TPU v7x, 128 devices: a whole 4x4x4 slice. The times are simulated.
128 devices in a mesh: fs: 16 (over z, x), tp: 8 (over y, core).
Axes of the slice: x: 4, y: 4, z: 4, core: 2. Of those that a mesh axis runs over, the one named last changes fastest.
Arguments:
- tokens: bfloat16 [12288, 2048], P('fs', 'tp'), may hold values from -6 to 6
- mix_gain: float32 [2048], replicated, may hold values from 0.1 to 1.9
- outer_gate: bfloat16 [2048, 2048], P('fs', 'tp'), may hold values from -0.125 to 0.125
- inner_gate: bfloat16 [2048, 2048], P('fs', 'tp'), may hold values from -0.125 to 0.125
- signal_in: bfloat16 [2048, 2048], P('fs', 'tp'), may hold values from -0.125 to 0.125
- mix_taps: float32 [3, 2048], P(None, 'tp'), may hold values from -3 to 3
- mix_bias: float32 [2048], P('tp'), may hold values from -3 to 3
- mix_out: bfloat16 [2048, 2048], P('tp', 'fs'), may hold values from -0.1875 to 0.1875
- ffn_gain: float32 [2048], replicated, may hold values from 0.1 to 1.9
- up_gate: bfloat16 [2048, 5632], P('fs', 'tp'), may hold values from -0.125 to 0.125
- up_value: bfloat16 [2048, 5632], P('fs', 'tp'), may hold values from -0.125 to 0.125
- ffn_taps: float32 [2, 3, 5632], P(None, None, 'tp'), may hold values from -3 to 3
- ffn_bias: float32 [2, 5632], P(None, 'tp'), may hold values from -3 to 3
- down_proj: bfloat16 [5632, 2048], P('tp', 'fs'), may hold values from -0.109375 to 0.109375
Outputs:
- layer_out: bfloat16 [12288, 2048], P('fs', 'tp')
All inputs are finite; a program needn't handle non-finite values.
Results may differ from a plain program's by a relative error of at most 0.023.
Values may be sent and summed in bfloat16 or wider, within the bound.
A program may use at most 64 MiB of HBM per device.

v0:
```python
import jax
import jax.numpy as jnp
from jax import lax
from jax.sharding import PartitionSpec as P

EPS = 1e-06


def joined_along(tiles, dim):
    lengths = list(tiles.shape[1:])
    lengths[dim] *= tiles.shape[0]
    return jnp.moveaxis(tiles, 0, dim).reshape(lengths)


def from_everyone(value, axis):
    devices = lax.axis_size(axis)
    return lax.all_to_all(
        jnp.broadcast_to(value[None], (devices, *value.shape)), axis, 0, 0, tiled=True
    )


def gather_directly(value, axis, dim):
    return joined_along(from_everyone(value, axis), dim)


def side_by_side(arrays, axis, dim, along):
    widths = [a.shape[along] for a in arrays]
    both = jnp.concatenate(arrays, axis=along)
    out = lax.all_gather(both, axis, axis=dim, tiled=True)
    return tuple(jnp.split(out, [sum(widths[:k]) for k in range(1, len(widths))], axis=along))


def gather_rows(column_part):
    return lax.all_gather(column_part, "tp", axis=1, tiled=True)


def rms_rows(values, gain):
    floats = values.astype(jnp.float32)
    scaled = floats * lax.rsqrt(jnp.mean(floats * floats, axis=-1, keepdims=True) + EPS) * gain
    return scaled.astype(jnp.bfloat16)


def causal_taps(signal, taps, bias):
    first = jnp.pad(signal, ((1, 0), (0, 0)))[:-1]
    second = jnp.pad(signal, ((2, 0), (0, 0)))[:-2]
    return taps[2] * signal + taps[1] * first + taps[0] * second + bias


def project_out(active, weight):
    return jnp.dot(active, gather_directly(weight, "fs", 1), preferred_element_type=jnp.float32)


def share_cols(term):
    return lax.psum_scatter(
        term.astype(jnp.bfloat16), "tp", scatter_dimension=1, tiled=True
    ).astype(jnp.float32)


def fold_products(normed, pieces):
    return tuple((jnp.dot(normed, piece, preferred_element_type=jnp.float32) for piece in pieces))


def on_device(
    tokens,
    mix_gain,
    outer_gate,
    inner_gate,
    signal_in,
    mix_taps,
    mix_bias,
    mix_out,
    ffn_gain,
    up_gate,
    up_value,
    ffn_taps,
    ffn_bias,
    down_proj,
):
    whole_gate, whole_value = side_by_side((up_gate, up_value), "fs", 0, 1)
    full_rows = gather_rows(tokens)
    normed = rms_rows(full_rows, mix_gain)
    outer, inner, signal = fold_products(
        normed, side_by_side((outer_gate, inner_gate, signal_in), "fs", 0, 1)
    )
    outer = outer.astype(jnp.bfloat16).astype(jnp.float32)
    inner = inner.astype(jnp.bfloat16).astype(jnp.float32)
    signal = signal.astype(jnp.bfloat16).astype(jnp.float32)
    gated = (outer * causal_taps(inner * signal, mix_taps, mix_bias)).astype(jnp.bfloat16)
    mix_term = project_out(gated, mix_out)
    state_cols = (tokens.astype(jnp.float32) + share_cols(mix_term)).astype(jnp.bfloat16)
    state_rows = gather_rows(state_cols)
    normed_two = rms_rows(state_rows, ffn_gain)
    gate_pre = jnp.dot(normed_two, whole_gate, preferred_element_type=jnp.float32)
    value_pre = jnp.dot(normed_two, whole_value, preferred_element_type=jnp.float32)
    gate_pre = gate_pre.astype(jnp.bfloat16).astype(jnp.float32)
    value_pre = value_pre.astype(jnp.bfloat16).astype(jnp.float32)
    gate_conv = causal_taps(gate_pre, ffn_taps[0], ffn_bias[0])
    value_conv = causal_taps(value_pre, ffn_taps[1], ffn_bias[1])
    active = (jax.nn.silu(gate_conv) * value_conv).astype(jnp.bfloat16)
    fed = share_cols(project_out(active, down_proj))
    return (state_cols.astype(jnp.float32) + fed).astype(jnp.bfloat16)


def solution(mesh):
    return jax.shard_map(
        on_device,
        mesh=mesh,
        in_specs=(
            P("fs", "tp"),
            P(),
            P("fs", "tp"),
            P("fs", "tp"),
            P("fs", "tp"),
            P(None, "tp"),
            P("tp"),
            P("tp", "fs"),
            P(),
            P("fs", "tp"),
            P("fs", "tp"),
            P(None, None, "tp"),
            P(None, "tp"),
            P("tp", "fs"),
        ),
        out_specs=P("fs", "tp"),
        check_vma=False,
    )
```

profile of v0, /device:TPU:1, one launch (start us, length us, event | category | flops | bytes accessed | tf_op | source)
XLA Modules:
  0.0 307.8 jit_solution(15107050874407716556)
XLA Ops:
  6.5 0.0 all-gather.5.cloned.1.call-start
  6.5 0.7 all-gather.5.cloned.1.call-update
  7.3 0.0 all-gather.7.cloned.1.call-start
  7.3 1.6 pad_maximum_fusion.1
  8.9 0.0 all-gather.7.cloned.1.call-update
  8.9 0.9 copy.16
  9.9 0.0 copy-start.11
  9.9 1.1 broadcast_in_dim.4
  11.0 8.5 %all-to-all-start = ((bf16[16,256,128]{1,2,0:T(8,128)(2,1)}), bf16[16,256,128]{1,2,0:T(8,128)(2,1)}, u32[]{:S(2)}, u32[]{:S(2)}) async-start(bf16[16,256,128]{1,2,0:T(8,128)(2,1)} %broadcast_in_dim.4), calls=%async_computation | async-start | bytes 2097152 | tf_op jit(solution)/shard_map/all_to_all | solution.py:17
  19.5 0.0 reduce-scatter.3.cloned.1.call-start
  19.5 0.0 copy-done.9
  19.5 24.2 %all-gather.5.cloned.1.call-done = bf16[768,2048]{1,0:T(8,128)(2,1)} async-done(((bf16[768,256]{1,0:T(8,128)(2,1)}), bf16[768,2048]{1,0:T(8,128)(2,1)}) %all-gather.5.cloned.1.call-update) | async-done | bytes 3145744 | tf_op jit(solution)/shard_map/all_gather | solution.py:34
  43.8 2.7 fusion
  46.5 47.2 %all-gather.7.cloned.1.call-done = bf16[2048,768]{1,0:T(8,128)(2,1)} async-done(((bf16[128,768]{1,0:T(8,128)(2,1)}), bf16[2048,768]{1,0:T(8,128)(2,1)}) %all-gather.7.cloned.1.call-update) | async-done | bytes 3145744 | tf_op jit(solution)/shard_map/all_gather | solution.py:29
  93.8 0.0 copy-done.11
  93.8 0.0 copy-done.1
  93.8 2.2 fusion.38
  96.0 0.0 copy-start.13
  96.0 3.2 %fusion.37 = f32[768,256]{1,0:T(8,128)} fusion(f32[768,256]{1,0:T(8,128)S(1)} %fusion.38, bf16[2048,768]{1,0:T(8,128)(2,1)} %all-gather.7.cloned.1.call-done, bf16[768,2048]{1,0:T(8,128)(2,1)S(1)} %copy-done.1, f32[2048]{0:T(1024)S(1)} %copy-done.11, f32[768]{0:T(1024)S(1)} %add_rsqrt_fusion.1), kind=kOutput, calls=%fused_computation.40 | convolution fusion | flops 812187648 | bytes 5778432 | tf_op jit(solution)/shard_map/dot_general | solution.py:60
  99.2 0.0 all-to-all-done
  99.2 0.0 copy-done.13
  99.2 7.5 %convolution_convert_fusion.1 = bf16[768,2048]{1,0:T(8,128)(2,1)} fusion(bf16[256,2048]{0,1:T(8,128)(2,1)} %bitcast.4, bf16[2048,768]{1,0:T(8,128)(2,1)} %all-gather.7.cloned.1.call-done, f32[768,256]{1,0:T(8,128)} %fusion.37, f32[256]{0:T(256)S(1)} %copy-done.13, f32[256]{0:T(256)S(1)} %bitcast.16, f32[256]{0:T(256)S(1)} %bitcast.17, f32[256]{0:T(256)S(1)} %bitcast.15, ...), kind=kOutput, calls=%fused_computation.11 | convolution fusion | flops 1620443136 | bytes 9190400 | tf_op jit(solution)/shard_map/dot_general | solution.py:50
  106.7 0.0 reduce-scatter.3.cloned.1.call-update
  106.8 0.0 all-gather.9.cloned.1.call-start
  106.8 32.3 %reduce-scatter.3.cloned.1.call-done = bf16[768,256]{1,0:T(8,128)(2,1)} async-done(((bf16[768,2048]{1,0:T(8,128)(2,1)}), bf16[768,256]{1,0:T(8,128)(2,1)}) %reduce-scatter.3.cloned.1.call-update) | async-done | bytes 393232 | tf_op jit(solution)/shard_map/reduce_scatter | solution.py:54
  139.1 0.0 copy-done.3
  139.1 1.8 add_convert_fusion.1
  141.0 0.0 all-gather.9.cloned.1.call-update
  141.0 0.0 all-gather.11.cloned.1.call-start
  141.0 0.0 copy-done.4
  141.0 0.0 copy-done.5
  141.1 0.8 pad_maximum_fusion
  141.8 0.0 all-gather.11.cloned.1.call-update
  141.9 2.2 broadcast_in_dim.5
  144.1 7.0 %all-to-all-start.1 = ((bf16[16,704,128]{2,1,0:T(8,128)(2,1)}), bf16[16,704,128]{2,1,0:T(8,128)(2,1)}, u32[]{:S(2)}, u32[]{:S(2)}) async-start(bf16[16,704,128]{2,1,0:T(8,128)(2,1)} %broadcast_in_dim.5), calls=%async_computation.2 | async-start | bytes 5767168 | tf_op jit(solution)/shard_map/all_to_all | solution.py:17
  151.1 0.2 reduce-scatter.5.cloned.1.call-start
  151.3 0.1 slice_reduce_fusion.7
  151.4 23.1 %all-gather.9.cloned.1.call-done = bf16[768,2048]{1,0:T(8,128)(2,1)} async-done(((bf16[768,256]{1,0:T(8,128)(2,1)}), bf16[768,2048]{1,0:T(8,128)(2,1)}) %all-gather.9.cloned.1.call-update) | async-done | bytes 3145744 | tf_op jit(solution)/shard_map/all_gather | solution.py:34
  174.5 2.7 fusion.3
  177.2 65.7 %all-gather.11.cloned.1.call-done = bf16[2048,1408]{0,1:T(8,128)(2,1)} async-done(((bf16[128,1408]{0,1:T(8,128)(2,1)}), bf16[2048,1408]{0,1:T(8,128)(2,1)}) %all-gather.11.cloned.1.call-update) | async-done | bytes 5767184 | tf_op jit(solution)/shard_map/all_gather | solution.py:29
  243.0 0.0 copy-done.2
  243.0 5.8 %fusion.27 = f32[768,704]{0,1:T(8,128)} fusion(bf16[2048,1408]{0,1:T(8,128)(2,1)} %all-gather.11.cloned.1.call-done, bf16[768,2048]{1,0:T(8,128)(2,1)S(1)} %copy-done.2, f32[2048]{0:T(1024)S(1)} %copy-done.12, f32[768]{0:T(1024)S(1)} %add_rsqrt_fusion), kind=kOutput, calls=%fused_computation.35 | convolution fusion | flops 2221965312 | bytes 8203264 | tf_op jit(solution)/shard_map/dot_general | solution.py:93
  248.8 3.9 %fusion.33 = f32[768,704]{0,1:T(8,128)} fusion(bf16[2048,1408]{0,1:T(8,128)(2,1)S(1)} %copy-done.10, bf16[768,2048]{1,0:T(8,128)(2,1)S(1)} %copy-done.2, f32[2048]{0:T(1024)S(1)} %copy-done.12, f32[768]{0:T(1024)S(1)} %add_rsqrt_fusion), kind=kOutput, calls=%fused_computation.37 | convolution fusion | flops 2221965312 | bytes 8204288 | tf_op jit(solution)/shard_map/dot_general | solution.py:94
  252.7 0.0 all-to-all-done.1
  252.7 12.6 %convolution_convert_fusion = bf16[768,2048]{1,0:T(8,128)(2,1)} fusion(f32[768,704]{0,1:T(8,128)} %fusion.33, f32[768,704]{0,1:T(8,128)} %fusion.27, f32[704]{0:T(1024)S(1)} %get-tuple-element.12, f32[704]{0:T(1024)S(1)} %get-tuple-element.9, f32[704]{0:T(1024)S(1)} %get-tuple-element.10, f32[704]{0:T(1024)S(1)} %get-tuple-element.6, ...), kind=kOutput, calls=%fused_computation.10 | convolution fusion | flops 2225897472 | bytes 10377216 | tf_op jit(solution)/shard_map/dot_general | solution.py:50
  265.3 0.0 reduce-scatter.5.cloned.1.call-update
  265.3 33.7 %reduce-scatter.5.cloned.1.call-done = bf16[768,256]{1,0:T(8,128)(2,1)} async-done(((bf16[768,2048]{1,0:T(8,128)(2,1)}), bf16[768,256]{1,0:T(8,128)(2,1)}) %reduce-scatter.5.cloned.1.call-update) | async-done | bytes 393232 | tf_op jit(solution)/shard_map/reduce_scatter | solution.py:54
  299.1 1.8 add_convert_fusion
  (22 shorter events, 0.1 us)
Async XLA Ops:
  6.5 13.0 %copy-start.9 = (f32[3,256]{1,0:T(4,128)S(1)}, f32[3,256]{1,0:T(4,128)}, u32[]{:S(2)}) copy-start(f32[3,256]{1,0:T(4,128)} %param.19) | copy-start | bytes 9220
  6.5 37.2 %all-gather.5.cloned.1.call-start = ((), (), s32[]{:S(2)}) async-start(), calls=%async_computation.4 | async-start | bytes 3538944 | tf_op jit(solution)/shard_map/all_gather | solution.py:34
  7.3 86.5 %all-gather.7.cloned.1.call-start = ((), (), s32[]{:S(2)}) async-start(), calls=%async_computation.5 | async-start | bytes 3342336 | tf_op jit(solution)/shard_map/all_gather | solution.py:29
  9.9 83.9 %copy-start.11 = (f32[2048]{0:T(1024)S(1)}, f32[2048]{0:T(1024)}, u32[]{:S(2)}) copy-start(f32[2048]{0:T(1024)} %param.15) | copy-start | bytes 24580
  11.0 88.2 %all-to-all-start = ((bf16[16,256,128]{1,2,0:T(8,128)(2,1)}), bf16[16,256,128]{1,2,0:T(8,128)(2,1)}, u32[]{:S(2)}, u32[]{:S(2)}) async-start(bf16[16,256,128]{1,2,0:T(8,128)(2,1)} %broadcast_in_dim.4), calls=%async_computation | async-start | bytes 2097152 | tf_op jit(solution)/shard_map/all_to_all | solution.py:17
  19.5 119.7 %reduce-scatter.3.cloned.1.call-start = ((), (), s32[]{:S(2)}) async-start(), calls=%async_computation.6 | async-start | bytes 3538944 | tf_op jit(solution)/shard_map/reduce_scatter | solution.py:54
  43.8 50.0 %copy-start.1 = (bf16[768,2048]{1,0:T(8,128)(2,1)S(1)}, bf16[768,2048]{1,0:T(8,128)(2,1)}, u32[]{:S(2)}) copy-start(bf16[768,2048]{1,0:T(8,128)(2,1)} %all-gather.5.cloned.1.call-done) | copy-start | bytes 9437188
  96.0 3.2 %copy-start.13 = (f32[256]{0:T(256)S(1)}, f32[256]{0:T(256)}, u32[]{:S(2)}) copy-start(f32[256]{0:T(256)} %param.20) | copy-start | bytes 3076
  106.7 32.4 %copy-start.3 = (bf16[768,256]{1,0:T(8,128)(2,1)S(1)}, bf16[768,256]{1,0:T(8,128)(2,1)}, u32[]{:S(2)}) copy-start(bf16[768,256]{1,0:T(8,128)(2,1)} %param.14) | copy-start | bytes 1179652
  106.7 34.3 %copy-start.4 = (bf16[128,704]{0,1:T(8,128)(2,1)S(1)}, bf16[128,704]{0,1:T(8,128)(2,1)}, u32[]{:S(2)}) copy-start(bf16[128,704]{0,1:T(8,128)(2,1)} %param.24) | copy-start | bytes 540676
  106.7 34.3 %copy-start.5 = (bf16[128,704]{0,1:T(8,128)(2,1)S(1)}, bf16[128,704]{0,1:T(8,128)(2,1)}, u32[]{:S(2)}) copy-start(bf16[128,704]{0,1:T(8,128)(2,1)} %param.23) | copy-start | bytes 540676
  106.7 35.1 %copy-start.6 = (bf16[704,128]{1,0:T(8,128)(2,1)S(1)}, bf16[704,128]{1,0:T(8,128)(2,1)}, u32[]{:S(2)}) copy-start(bf16[704,128]{1,0:T(8,128)(2,1)} %param.27) | copy-start | bytes 540676
  106.8 67.7 %all-gather.9.cloned.1.call-start = ((), (), s32[]{:S(2)}) async-start(), calls=%async_computation.7 | async-start | bytes 3538944 | tf_op jit(solution)/shard_map/all_gather | solution.py:34
  141.0 102.0 %all-gather.11.cloned.1.call-start = ((), (), s32[]{:S(2)}) async-start(), calls=%async_computation.8 | async-start | bytes 6127616 | tf_op jit(solution)/shard_map/all_gather | solution.py:29
  144.1 7.2 %copy-start.8 = (f32[2,704]{1,0:T(2,128)S(1)}, f32[2,704]{1,0:T(2,128)}, u32[]{:S(2)}) copy-start(f32[2,704]{1,0:T(2,128)} %param.26) | copy-start | bytes 16900
  144.1 7.2 %copy-start.7 = (f32[2,3,704]{2,0,1:T(2,128)S(1)}, f32[2,3,704]{2,0,1:T(2,128)}, u32[]{:S(2)}) copy-start(f32[2,3,704]{2,0,1:T(2,128)} %param.25) | copy-start | bytes 50692
  144.1 98.9 %copy-start.12 = (f32[2048]{0:T(1024)S(1)}, f32[2048]{0:T(1024)}, u32[]{:S(2)}) copy-start(f32[2048]{0:T(1024)} %param.22) | copy-start | bytes 24580
  144.1 108.6 %all-to-all-start.1 = ((bf16[16,704,128]{2,1,0:T(8,128)(2,1)}), bf16[16,704,128]{2,1,0:T(8,128)(2,1)}, u32[]{:S(2)}, u32[]{:S(2)}) async-start(bf16[16,704,128]{2,1,0:T(8,128)(2,1)} %broadcast_in_dim.5), calls=%async_computation.2 | async-start | bytes 5767168 | tf_op jit(solution)/shard_map/all_to_all | solution.py:17
  151.1 148.0 %reduce-scatter.5.cloned.1.call-start = ((), (), s32[]{:S(2)}) async-start(), calls=%async_computation.9 | async-start | bytes 3538944 | tf_op jit(solution)/shard_map/reduce_scatter | solution.py:54
  174.5 68.5 %copy-start.2 = (bf16[768,2048]{1,0:T(8,128)(2,1)S(1)}, bf16[768,2048]{1,0:T(8,128)(2,1)}, u32[]{:S(2)}) copy-start(bf16[768,2048]{1,0:T(8,128)(2,1)} %all-gather.9.cloned.1.call-done) | copy-start | bytes 9437188
  243.0 5.8 %copy-start.10 = (bf16[2048,1408]{0,1:T(8,128)(2,1)S(1)}, bf16[2048,1408]{0,1:T(8,128)(2,1)}, u32[]{:S(2)}) copy-start(bf16[2048,1408]{0,1:T(8,128)(2,1)} %all-gather.11.cloned.1.call-done) | copy-start | bytes 17301508
  265.3 33.8 %copy-start = (bf16[768,256]{1,0:T(8,128)(2,1)S(1)}, bf16[768,256]{1,0:T(8,128)(2,1)}, u32[]{:S(2)}) copy-start(bf16[768,256]{1,0:T(8,128)(2,1)} %add_convert_fusion.1) | copy-start | bytes 1179652
Sparse Core Ops, SparseCore 0:
  9.0 34.7 all-gather.4
  45.9 47.8 all-gather.6
  106.9 32.2 reduce-scatter.2
  141.1 33.3 all-gather.8
  176.4 66.4 all-gather.10
  265.5 33.5 reduce-scatter.4
where the time goes:
time: 311 us; the launch traced here: 308 us
  waiting for transfers between devices  227 us (73%)
  matrix products  35.3 us (11%)
  starting transfers between devices  15.8 us (5%)
  between operations  13.6 us (4%)
  other arithmetic  11.5 us (4%)
  local copies, waits for them, and re-layouts  4.38 us (1%)
    all_gather x2, waiting for transfers between devices, side_by_side(): out = lax.all_gather(both, axis, axis=dim, tiled=True)  113 us
    reduce_scatter x2, waiting for transfers between devices, share_cols(): lax.psum_scatter(term.astype(jnp.bfloat16), 'tp', scatter_dimension=1, ti...  66.1 us
    all_gather x2, waiting for transfers between devices, gather_rows(): return lax.all_gather(column_part, 'tp', axis=1, tiled=True)  47.3 us
    dot_general x2, matrix products, project_out(): jnp.dot(active, gather_directly(weight, 'fs', 1), preferred_element_type=...  20.1 us
    all_to_all x2, starting transfers between devices, from_everyone(): lax.all_to_all(jnp.broadcast_to(value[None], (devices, *value.shape)), ax...  15.4 us
  transfers between devices with their start and end apart: 8, of which 6 were waited for; matrix products, arithmetic and copies ran while one was open for 9% of the time, Pallas kernels for 0%

commit v1 on v0

v1 whole, which is shorter than its diff:
```python
import jax
import jax.numpy as jnp
from jax import lax
from jax.experimental import pallas as pl
from jax.experimental.pallas import tpu as pltpu
from jax.sharding import PartitionSpec as P

EPS = 1e-06
MESH = pl.DeviceIdType.MESH
BF16 = jnp.bfloat16
F32 = jnp.float32
SEQ = 768
D = 2048
CHUNKS = 3
R = SEQ // CHUNKS
H = R // 2
COPIES = 256
LOCALS = 9


def at(value, step):
    return pl.multiple_of(value, step)


def kernel(
    tokens,
    mix_gain,
    outer_gate,
    inner_gate,
    signal_in,
    mix_taps,
    mix_bias,
    mix_out,
    ffn_gain,
    up_gate,
    up_value,
    ffn_taps,
    ffn_bias,
    down_proj,
    out,
    rows,
    rows2,
    normed,
    projw,
    mixw,
    upw,
    downw,
    gstage,
    vstage,
    outer_s,
    mi,
    gated,
    pre,
    act,
    taps_s,
    keep,
    psend,
    precv,
    ssend,
    d2,
    fin,
    send_sem,
    recv_sem,
    local_sem,
):
    f = lax.axis_index("fs")
    t = lax.axis_index("tp")
    z, x = f // 4, f % 4
    y, c = t // 2, t % 2

    def near(v, i):
        return (v + i + 4) % 4

    xp, xm = (4 * z + near(x, 1), t), (4 * z + near(x, -1), t)
    zp, zm = (4 * near(z, 1) + x, t), (4 * near(z, -1) + x, t)
    yp, ym = (f, 2 * near(y, 1) + c), (f, 2 * near(y, -1) + c)
    pc = (f, 2 * y + 1 - c)

    ids = {}
    sent = []

    def ident(key):
        if key not in ids:
            ids[key] = len(ids)
        return ids[key]

    def descriptor(src, dst, key, dev):
        i = ident(key)
        return pltpu.make_async_remote_copy(
            src_ref=src,
            dst_ref=dst,
            send_sem=send_sem.at[i],
            recv_sem=recv_sem.at[i],
            device_id=dev,
            device_id_type=MESH,
        )

    def send(src, dst, key, dev):
        copy = descriptor(src, dst, key, dev)
        copy.start()
        sent.append(copy)

    def arrive(dst, key):
        descriptor(dst, dst, key, pc).wait_recv()


    def proj_slice(g, h, q):
        start, size = (h * 64, 64) if q is None else (h * 64 + q * 32, 32)
        return projw.at[pl.ds(at(g * 128 + start, 32), size), :]

    def up_slice(g, h, q):
        start, size = (h * 64, 64) if q is None else (h * 64 + q * 32, 32)
        return upw.at[pl.ds(at(g * 128 + start, 32), size), :]

    def mix_slice(g, h, q):
        start, size = (h * 128, 128) if q is None else (h * 128 + q * 64, 64)
        return mixw.at[pl.ds(start, size), pl.ds(at(g * 128, 128), 128)]

    def down_slice(g, h, q):
        start, size = (h * 352, 352) if q is None else (h * 352 + q * 176, 176)
        return downw.at[pl.ds(start, size), pl.ds(at(g * 128, 128), 128)]

    class Gather:
        def __init__(self, name, view):
            self.name, self.view = name, view

        def blk(self, h, i, j, q=None):
            g = 4 * near(z, j) + near(x, i) if h == 0 else 4 * near(z, i) + near(x, j)
            return self.view(g, h, q)

        def dev(self, h, which):
            first = {"np": xp, "nm": xm, "fp": zp, "fm": zm}
            second = {"np": zp, "nm": zm, "fp": xp, "fm": xm}
            return (first if h == 0 else second)[which]

        def put(self, h, i, j, which, tag, q=None):
            ref = self.blk(h, i, j, q)
            send(ref, ref, (self.name, h, tag), self.dev(h, which))

        def get(self, h, i, j, tag, q=None):
            arrive(self.blk(h, i, j, q), (self.name, h, tag))

        def r0(self):
            for h in (0, 1):
                self.put(h, 0, 0, "np", "np")
                self.put(h, 0, 0, "nm", "nm")

        def r1(self):
            for h in (0, 1):
                self.put(h, 0, 0, "fp", "fp0")
                self.put(h, 0, 0, "fm", "fm0")

        def r2(self):
            for h in (0, 1):
                self.get(h, -1, 0, "np")
                self.put(h, -1, 0, "np", "qp", 0)
                self.get(h, 1, 0, "nm")
                self.put(h, 1, 0, "nm", "qm", 1)
            for h in (0, 1):
                self.put(h, -1, 0, "fp", "fp1")
                self.put(h, -1, 0, "fm", "fm1")
                self.put(h, 1, 0, "fp", "fp2")
                self.put(h, 1, 0, "fm", "fm2")

        def r3(self):
            for h in (0, 1):
                self.get(h, 2, 0, "qp", 0)
                self.get(h, 2, 0, "qm", 1)
                self.put(h, 2, 0, "fp", "fp3")
                self.put(h, 2, 0, "fm", "fm3")

        def r4a(self):
            for h in (0, 1):
                self.get(h, 0, -1, "fp0")
                self.put(h, 0, -1, "fp", "gp0")
                self.get(h, 0, 1, "fm0")

        def r4b(self):
            for h in (0, 1):
                self.get(h, -1, -1, "fp1")
                self.get(h, -1, 1, "fm1")
                self.put(h, -1, 1, "fm", "gm1")
                self.get(h, 1, -1, "fp2")
                self.put(h, 1, -1, "fp", "gp2")
                self.get(h, 1, 1, "fm2")

        def r4c(self):
            for h in (0, 1):
                self.get(h, 2, -1, "fp3")
                self.get(h, 2, 1, "fm3")
                self.put(h, 2, 1, "fm", "gm3")

        def end(self):
            for h in (0, 1):
                self.get(h, 0, 2, "gp0")
                self.get(h, 1, 2, "gp2")
                self.get(h, -1, 2, "gm1")
                self.get(h, 2, 2, "gm3")

    proj = Gather("p", proj_slice)
    mix = Gather("m", mix_slice)
    up = Gather("u", up_slice)
    down = Gather("d", down_slice)


    class Rows:
        def __init__(self, name, buf, row, size):
            self.name, self.buf, self.row, self.size = name, buf, row, size

        def view(self, dy, other, half=None):
            col = 256 * (2 * near(y, dy) + (1 - c if other else c))
            start, size = self.row, self.size
            if half is not None:
                size = size // 2
                start = start + half * size
            return self.buf.at[pl.ds(start, size), pl.ds(at(col, 256), 256)]

        def put(self, dy, tag, dev, half=None):
            ref = self.view(dy, False, half)
            send(ref, ref, (self.name, tag), dev)

        def get(self, dy, tag, other=False, half=None):
            arrive(self.view(dy, other, half), (self.name, tag))

        def own(self):
            self.put(0, "ap", yp)
            self.put(0, "am", ym)
            self.put(0, "c0", pc)

        def forward(self):
            self.get(-1, "ap")
            self.put(-1, "bp", yp, 0)
            self.get(1, "am")
            self.put(1, "bm", ym, 1)
            self.put(-1, "c1", pc)
            self.put(1, "c2", pc)

        def across(self):
            self.get(2, "bp", False, 0)
            self.put(2, "c3", pc, 0)
            self.get(2, "bm", False, 1)
            self.put(2, "c4", pc, 1)

        def end(self):
            self.get(0, "c0", True)
            self.get(-1, "c1", True)
            self.get(1, "c2", True)
            self.get(2, "c3", True, 0)
            self.get(2, "c4", True, 1)


    ORDER = (2, 1, 3, 0)

    class Sums:
        def __init__(self, phase, r):
            self.name, self.r = ("s", phase, r), r
            n = phase * CHUNKS + r
            self.psend, self.precv = psend.at[n], precv.at[n]
            self.ssend, self.d2, self.fin = ssend.at[n], d2.at[n], fin.at[n]
            self.keep = keep.at[r]

        def terms(self, lhs, weight):
            for k, dy in enumerate(ORDER):
                col = at(256 * (2 * near(y, dy) + 1 - c), 256)
                term = jnp.dot(lhs[...], weight[:, pl.ds(col, 256)], preferred_element_type=F32)
                self.psend[k] = term.astype(BF16)
                send(self.psend.at[k], self.precv.at[k], (self.name, "p", k), pc)
            for k, dy in enumerate(ORDER):
                col = at(256 * (2 * near(y, dy) + c), 256)
                self.keep[k] = jnp.dot(lhs[...], weight[:, pl.ds(col, 256)], preferred_element_type=F32)

        def pairs(self):
            for k in range(4):
                arrive(self.precv.at[k], (self.name, "p", k))
                total = self.keep[k] + self.precv[k].astype(F32)
                if k == 0:
                    self.ssend[0] = total.astype(BF16)
                    send(self.ssend.at[0, pl.ds(0, H)], self.d2.at[0], (self.name, "dp"), yp)
                    send(self.ssend.at[0, pl.ds(H, H)], self.d2.at[1], (self.name, "dm"), ym)
                elif k == 1:
                    self.ssend[1, H:] = total[H:].astype(BF16)
                    send(self.ssend.at[1, pl.ds(H, H)], self.fin.at[0, pl.ds(H, H)], (self.name, "ep"), yp)
                    self.keep[1, :H] = total[:H]
                elif k == 2:
                    self.ssend[2, :H] = total[:H].astype(BF16)
                    send(self.ssend.at[2, pl.ds(0, H)], self.fin.at[1, pl.ds(0, H)], (self.name, "em"), ym)
                    self.keep[2, H:] = total[H:]
                else:
                    self.keep[3] = total

        def pass_on(self):
            arrive(self.d2.at[0], (self.name, "dp"))
            self.ssend[1, :H] = (self.keep[1, :H] + self.d2[0].astype(F32)).astype(BF16)
            send(self.ssend.at[1, pl.ds(0, H)], self.fin.at[0, pl.ds(0, H)], (self.name, "fp"), yp)
            arrive(self.d2.at[1], (self.name, "dm"))
            self.ssend[2, H:] = (self.keep[2, H:] + self.d2[1].astype(F32)).astype(BF16)
            send(self.ssend.at[2, pl.ds(H, H)], self.fin.at[1, pl.ds(H, H)], (self.name, "fm"), ym)

        def total(self):
            arrive(self.fin.at[0, pl.ds(H, H)], (self.name, "ep"))
            arrive(self.fin.at[1, pl.ds(0, H)], (self.name, "em"))
            arrive(self.fin.at[0, pl.ds(0, H)], (self.name, "fp"))
            arrive(self.fin.at[1, pl.ds(H, H)], (self.name, "fm"))
            return self.keep[3] + self.fin[0].astype(F32) + self.fin[1].astype(F32)


    def norm(src, gain, start, count):
        def body(i, carry):
            r = at(start + i * 32, 32)
            v = src[pl.ds(r, 32), :].astype(F32)
            mean = jnp.sum(v * v, axis=1, keepdims=True) * (1.0 / D)
            normed[pl.ds(r, 32), :] = (v * lax.rsqrt(mean + EPS) * gain[...]).astype(BF16)
            return carry

        lax.fori_loop(0, count // 32, body, 0)

    def project(r):
        rows_r = pl.ds(r * R, R)
        outer_s[...] = jnp.dot(normed[rows_r, :], projw[:, 0:256], preferred_element_type=F32)
        inner = jnp.dot(normed[rows_r, :], projw[:, 256:512], preferred_element_type=F32)
        mi[pl.ds(8 + r * R, R), :] = inner
        signal = jnp.dot(normed[rows_r, :], projw[:, 512:768], preferred_element_type=F32)
        mi[pl.ds(8 + r * R, R), :] = mi[pl.ds(8 + r * R, R), :] * signal
        conv = (
            mix_taps[2:3, :] * mi[pl.ds(8 + r * R, R), :]
            + mix_taps[1:2, :] * mi[pl.ds(7 + r * R, R), :]
            + mix_taps[0:1, :] * mi[pl.ds(6 + r * R, R), :]
            + mix_bias[...]
        )
        gated[r] = (outer_s[...] * conv).astype(BF16)

    def expand(r):
        for n in range(6):
            width = 256 if n < 5 else 128
            pre[pl.ds(8 + r * R, R), pl.ds(n * 256, width)] = jnp.dot(
                normed[pl.ds(r * R, R), :], upw[:, n * 256 : n * 256 + width], preferred_element_type=F32
            )

    def conv_cols(r, col, which, j):
        lanes = pl.ds(col, 128)
        taps = taps_s[:, pl.ds(128 * j, 128)]
        a = 4 * which
        return (
            taps[a + 2 : a + 3] * pre[pl.ds(8 + r * R, R), lanes]
            + taps[a + 1 : a + 2] * pre[pl.ds(7 + r * R, R), lanes]
            + taps[a : a + 1] * pre[pl.ds(6 + r * R, R), lanes]
            + taps[a + 3 : a + 4]
        )

    def activate(r):
        for j in range(5):
            g = conv_cols(r, 128 * j, 0, j)
            v = conv_cols(r, 640 + 128 * j, 1, j)
            act[r, :, pl.ds(128 * j, 128)] = (g / (1.0 + jnp.exp(-g)) * v).astype(BF16)
        g = conv_cols(r, 1280, 0, 5)
        v = pltpu.roll(conv_cols(r, 1280, 1, 5), 64, 1)
        lane = lax.broadcasted_iota(jnp.int32, (R, 128), 1)
        last = jnp.where(lane < 64, g / (1.0 + jnp.exp(-g)) * v, 0.0)
        act[r, :, pl.ds(640, 128)] = last.astype(BF16)


    own_cols = pl.ds(at(256 * t, 256), 256)
    own_rows = pl.ds(at(128 * f, 128), 128)
    own_block = pl.ds(at(128 * f, 128), 128)
    moves = [
        (tokens, rows.at[:, own_cols]),
        (outer_gate, projw.at[own_rows, pl.ds(0, 256)]),
        (inner_gate, projw.at[own_rows, pl.ds(256, 256)]),
        (signal_in, projw.at[own_rows, pl.ds(512, 256)]),
        (mix_out, mixw.at[:, own_block]),
        (up_gate, gstage),
        (up_value, vstage),
        (down_proj, downw.at[pl.ds(0, 704), own_block]),
    ]
    local = [pltpu.make_async_copy(src, dst, local_sem.at[i]) for i, (src, dst) in enumerate(moves)]
    for copy in local:
        copy.start()

    barrier = pltpu.get_barrier_semaphore()
    for dev in (xp, xm, zp, zm, yp, ym, pc):
        pl.semaphore_signal(barrier, inc=1, device_id=dev, device_id_type=MESH)
    mi[0:8, :] = jnp.zeros((8, 256), F32)
    pre[0:8, :] = jnp.zeros((8, 1408), F32)
    downw[704:768, :] = jnp.zeros((64, D), BF16)
    taps_s[...] = jnp.zeros((8, 768), F32)
    for which in (0, 1):
        taps_s[4 * which : 4 * which + 3, 0:704] = ffn_taps[which]
        taps_s[4 * which + 3 : 4 * which + 4, 0:704] = ffn_bias[which : which + 1]
    tail = taps_s[4:8, 640:768]
    taps_s[4:8, 640:768] = pltpu.roll(tail, 64, 1)
    pl.semaphore_wait(barrier, 7)

    tok = Rows("t", rows, 0, SEQ)
    hid = [Rows(("h", r), rows2, r * R, R) for r in range(CHUNKS)]
    one = [Sums(0, r) for r in range(CHUNKS)]
    two = [Sums(1, r) for r in range(CHUNKS)]

    local[0].wait()
    tok.own()
    for copy in local[1:4]:
        copy.wait()
    proj.r0()
    proj.r1()
    local[4].wait()
    mix.r0()
    mix.r1()
    for copy in local[5:8]:
        copy.wait()
    upw[own_rows, 0:640] = gstage[:, 0:640]
    upw[own_rows, 640:1280] = vstage[:, 0:640]
    upw[own_rows, 1280:1408] = jnp.concatenate([gstage[:, 640:704], vstage[:, 640:704]], axis=1)

    proj.r2()
    proj.r4a()
    proj.r3()
    mix.r2()
    tok.forward()
    proj.r4b()
    mix.r4a()
    mix.r3()
    up.r0()
    up.r1()
    proj.r4c()
    mix.r4b()
    tok.across()
    mix.r4c()
    tok.end()
    norm(rows, mix_gain, 0, SEQ)
    proj.end()
    up.r2()
    project(0)
    mix.end()
    one[0].terms(gated.at[0], mixw)
    up.r4a()
    project(1)
    one[0].pairs()
    one[1].terms(gated.at[1], mixw)
    up.r3()
    down.r0()
    project(2)
    one[1].pairs()
    one[0].pass_on()
    one[2].terms(gated.at[2], mixw)
    one[2].pairs()
    one[1].pass_on()
    down.r1()

    def hidden(r):
        rr = pl.ds(r * R, R)
        total = rows[rr, own_cols].astype(F32) + one[r].total()
        rows2[rr, own_cols] = total.astype(BF16)
        hid[r].own()

    up.r4b()
    hidden(0)
    one[2].pass_on()
    hidden(1)
    hid[0].forward()
    down.r2()
    hidden(2)
    hid[1].forward()
    hid[0].across()
    up.r4c()
    hid[0].end()
    norm(rows2, ffn_gain, 0, R)
    hid[2].forward()
    hid[1].across()
    down.r4a()
    down.r3()
    hid[1].end()
    norm(rows2, ffn_gain, R, R)
    hid[2].across()
    down.r4b()
    hid[2].end()
    norm(rows2, ffn_gain, 2 * R, R)
    up.end()
    expand(0)
    down.r4c()
    activate(0)
    down.end()
    two[0].terms(act.at[0], downw)
    expand(1)
    two[0].pairs()
    activate(1)
    two[1].terms(act.at[1], downw)
    two[0].pass_on()
    expand(2)
    two[1].pairs()
    activate(2)
    two[1].pass_on()
    two[2].terms(act.at[2], downw)
    two[2].pairs()

    def finish(r):
        rr = pl.ds(r * R, R)
        out[rr, :] = (rows2[rr, own_cols].astype(F32) + two[r].total()).astype(BF16)

    finish(0)
    two[2].pass_on()
    finish(1)
    finish(2)
    for copy in sent:
        copy.wait_send()


def on_device(
    tokens,
    mix_gain,
    outer_gate,
    inner_gate,
    signal_in,
    mix_taps,
    mix_bias,
    mix_out,
    ffn_gain,
    up_gate,
    up_value,
    ffn_taps,
    ffn_bias,
    down_proj,
):
    hbm = pl.BlockSpec(memory_space=pl.ANY)
    vmem = pl.BlockSpec(memory_space=pltpu.VMEM)
    n = 2 * CHUNKS
    return pl.pallas_call(
        kernel,
        out_shape=jax.ShapeDtypeStruct((SEQ, 256), BF16),
        in_specs=[hbm, vmem, hbm, hbm, hbm, vmem, vmem, hbm, vmem, hbm, hbm, vmem, vmem, hbm],
        out_specs=vmem,
        scratch_shapes=[
            pltpu.VMEM((SEQ, D), BF16),
            pltpu.VMEM((SEQ, D), BF16),
            pltpu.VMEM((SEQ, D), BF16),
            pltpu.VMEM((D, 768), BF16),
            pltpu.VMEM((256, D), BF16),
            pltpu.VMEM((D, 1408), BF16),
            pltpu.VMEM((768, D), BF16),
            pltpu.VMEM((128, 704), BF16),
            pltpu.VMEM((128, 704), BF16),
            pltpu.VMEM((R, 256), F32),
            pltpu.VMEM((8 + SEQ, 256), F32),
            pltpu.VMEM((CHUNKS, R, 256), BF16),
            pltpu.VMEM((8 + SEQ, 1408), F32),
            pltpu.VMEM((CHUNKS, R, 768), BF16),
            pltpu.VMEM((8, 768), F32),
            pltpu.VMEM((CHUNKS, 4, R, 256), F32),
            pltpu.VMEM((n, 4, R, 256), BF16),
            pltpu.VMEM((n, 4, R, 256), BF16),
            pltpu.VMEM((n, 3, R, 256), BF16),
            pltpu.VMEM((n, 2, H, 256), BF16),
            pltpu.VMEM((n, 2, R, 256), BF16),
            pltpu.SemaphoreType.DMA((COPIES,)),
            pltpu.SemaphoreType.DMA((COPIES,)),
            pltpu.SemaphoreType.DMA((LOCALS,)),
        ],
        compiler_params=pltpu.CompilerParams(
            collective_id=0, has_side_effects=True, vmem_limit_bytes=62 * 1024 * 1024
        ),
    )(
        tokens,
        mix_gain.reshape(1, D),
        outer_gate,
        inner_gate,
        signal_in,
        mix_taps,
        mix_bias.reshape(1, 256),
        mix_out,
        ffn_gain.reshape(1, D),
        up_gate,
        up_value,
        ffn_taps,
        ffn_bias,
        down_proj,
    )


def solution(mesh):
    return jax.shard_map(
        on_device,
        mesh=mesh,
        in_specs=(
            P("fs", "tp"),
            P(),
            P("fs", "tp"),
            P("fs", "tp"),
            P("fs", "tp"),
            P(None, "tp"),
            P("tp"),
            P("tp", "fs"),
            P(),
            P("fs", "tp"),
            P("fs", "tp"),
            P(None, None, "tp"),
            P(None, "tp"),
            P("tp", "fs"),
        ),
        out_specs=P("fs", "tp"),
        check_vma=False,
    )
```

time: 311 us -> 115 us (0.37)
  waiting for transfers between devices: 227 us -> 0 us
  Pallas kernels: 0 us -> 107 us
  matrix products: 35.3 us -> 0 us
  starting transfers between devices: 15.8 us -> 0 us
  between operations: 13.6 us -> 0.01 us
  other arithmetic: 11.5 us -> 0 us
    all_gather x4 -> x0, waiting for transfers between devices: 160 us -> none  [the longest x2 113 us: side_by_side(): out = lax.all_gather(both, axis, axis=dim, tiled=True)]
    pallas_call x0 -> x1, Pallas kernels: none -> 107 us  [on_device(): pl.pallas_call(kernel, out_shape=jax.ShapeDtypeStruct((SEQ, 256), BF16),...]
    reduce_scatter x2 -> x0, waiting for transfers between devices: 66.1 us -> none  [share_cols(): lax.psum_scatter(term.astype(jnp.bfloat16), 'tp', scatter_dimension=1, ti...]
    dot_general x6 -> x0, matrix products: 35.3 us -> none  [the longest x2 20.1 us: project_out(): jnp.dot(active, gather_directly(weight, 'fs', 1), preferred_element_type=...]
    all_to_all x2 -> x0, starting transfers between devices: 15.4 us -> none  [from_everyone(): lax.all_to_all(jnp.broadcast_to(value[None], (devices, *value.shape)), ax...]
    reduce_sum x2 -> x0, other arithmetic: 5.44 us -> none  [rms_rows(): jnp.mean(floats * floats, axis=-1, keepdims=True) + EPS]
    unnamed x29 -> x6, local copies, waits for them, and re-layouts: 1 us -> 5.7 us
    convert_element_type x2 -> x0, other arithmetic: 3.67 us -> none  [the longest x1 1.84 us: on_device(): return (state_cols.astype(jnp.float32) + fed).astype(jnp.bfloat16)]
  transfers between devices with their start and end apart: 8 -> 0, of which waited for: 6 -> 0; matrix products, arithmetic and copies ran while one was open for 9% -> 0% of each run, Pallas kernels for 0% -> 0%
where the time goes in v1:
time: 115 us; the launch traced here: 113 us
  Pallas kernels  107 us (93%)
  local copies, waits for them, and re-layouts  5.7 us (5%)
    pallas_call x1, Pallas kernels, on_device(): pl.pallas_call(kernel, out_shape=jax.ShapeDtypeStruct((SEQ, 256), BF16),...  107 us
    unnamed x6, local copies, waits for them, and re-layouts  5.7 us

profile of v1, /device:TPU:1, one launch (start us, length us, event | category | flops | bytes accessed | tf_op | source)
XLA Modules:
  0.0 113.1 jit_solution(11884487584710303544)
XLA Ops:
  0.0 1.3 %copy.17.ffn_taps = f32[2,3,704]{2,1,0:T(4,128)} copy(f32[2,3,704]{2,0,1:T(2,128)} %param.25) | data formatting | bytes 33792 | tf_op args[11]
  1.3 0.0 copy-start
  1.3 1.8 %copy.15.up_gate = bf16[128,704]{1,0:T(8,128)(2,1)} copy(bf16[128,704]{0,1:T(8,128)(2,1)} %param.23) | data formatting | bytes 360448 | tf_op args[9]
  3.1 0.0 copy-done
  3.1 0.8 copy.16.up_value
  3.9 107.4 %shard_map.136 = bf16[768,256]{1,0:T(8,128)(2,1)} custom-call(bf16[768,256]{1,0:T(8,128)(2,1)} %tokens.1, f32[1,2048]{1,0:T(1,128)} %bitcast.3, bf16[128,256]{1,0:T(8,128)(2,1)} %outer_gate.1, bf16[128,256]{1,0:T(8,128)(2,1)} %inner_gate.1, bf16[128,256]{1,0:T(8,128)(2,1)} %signal_in.1, f32[3,256]{1,0:T(4,128)} %mix_taps.1, f32[1,256]{1,0:T(1,128)} %bitcast.5, ...), custom_call_target="tpu_custom_call" | custom-call | tf_op jit(solution)/shard_map/pallas_call | solution.py:525
  111.3 1.8 %copy.19 = bf16[768,256]{1,0:T(8,128)(2,1)} copy(bf16[768,256]{1,0:T(8,128)(2,1)} %shard_map.136) | data formatting | bytes 786432
Async XLA Ops:
  1.3 1.8 %copy-start = (bf16[128,704]{0,1:T(8,128)(2,1)S(1)}, bf16[128,704]{0,1:T(8,128)(2,1)}, u32[]{:S(2)}) copy-start(bf16[128,704]{0,1:T(8,128)(2,1)} %param.24) | copy-start | bytes 540676

commit v2 on v1

--- a/solution.py
+++ b/solution.py
@@ -14,8 +14,36 @@
 CHUNKS = 3
 R = SEQ // CHUNKS
 H = R // 2
-COPIES = 256
-LOCALS = 9
+COPIES = 288
+LOCALS = 8
+
+PLAN = (
+    "place_t", "place_p", "p0.nm", "p1.nm", "place_m", "m0.np", "m1.np", "t0.own", "t1.own", "t2.own", "p0.np",
+    "p1.np", "lay_up", "m0.nm", "m1.nm", "place_d", "m1.fm0", "m0.fm0", "m1.fp0", "m0.fp0", "p1.fm0", "p0.fm0",
+    "p1.fp0", "p0.fp0", "m1.fm1", "m0.fm1", "m0.qp", "m1.qp", "m1.fp1", "m0.fp1", "p0.qm", "p1.qm", "t0.fp",
+    "t0.fm", "p0.qp", "p1.qp", "m0.qm", "m1.qm", "m1.fm2", "m0.fm2", "m1.gp0", "m0.gp0", "p1.fm2", "p0.fm2",
+    "m1.fp2", "m0.fp2", "p1.fp2", "p0.fp2", "t1.fp", "t1.fm", "m1.gm1", "m0.gm1", "p1.fm1", "p0.fm1", "p1.gp0",
+    "p0.gp0", "t2.fp", "t2.fm", "m1.fm3", "m0.fm3", "m1.fp3", "m0.fp3", "t0.xp", "t0.xm", "p1.fm3", "p0.fm3",
+    "m1.gp2", "m0.gp2", "p1.fp3", "p0.fp3", "t0.end", "norm0", "t1.xp", "t1.xm", "u0.nm", "u1.nm", "t2.xp", "t2.xm",
+    "p1.fp1", "p0.fp1", "t1.end", "norm1", "t2.end", "m1.gm3", "m0.gm3", "norm2", "p1.gm1", "p0.gm1", "p1.gp2",
+    "p0.gp2", "p1.gm3", "p0.gm3", "u0.np", "u1.np", "m.end", "u0.qm", "u1.qm", "u1.fp2", "u0.fp2", "u1.fm2",
+    "u0.fm2", "u1.fp0", "u0.fp0", "v0.nm", "v1.nm", "v0.np", "v1.np", "p.end", "project0", "u0.fm1", "u1.fm1",
+    "one0.terms", "u0.qp", "u1.qp", "project1", "u1.gp0", "u0.gp0", "u0.fm0", "u1.fm0", "one1.terms", "one0.pairs",
+    "u0.fp1", "u1.fp1", "d0.nm", "d1.nm", "project2", "u0.fm3", "u1.fm3", "u0.fp3", "u1.fp3", "one2.terms",
+    "one1.pairs", "u1.gm1", "u0.gm1", "v0.qp", "v1.qp", "one0.pass", "u1.gp2", "u0.gp2", "v0.qm", "v1.qm",
+    "one2.pairs", "v1.fp2", "v0.fp2", "v1.fm2", "v0.fm2", "one1.pass", "v1.fp0", "v0.fp0", "u1.gm3", "u0.gm3",
+    "hidden0", "h0.own", "v1.fm3", "v0.fm3", "v1.fp3", "v0.fp3", "one2.pass", "v1.fm1", "v0.fm1", "d0.np", "d1.np",
+    "u.end", "hidden1", "h1.own", "v1.fm0", "v0.fm0", "v1.gp0", "v0.gp0", "v1.gm3", "v0.gm3", "v1.fp1", "v0.fp1",
+    "h0.fp", "h0.fm", "hidden2", "h2.own", "v1.gm1", "v0.gm1", "d0.qp", "d1.qp", "v1.gp2", "v0.gp2", "d0.qm",
+    "d1.qm", "h1.fp", "h1.fm", "d1.fm2", "d0.fm2", "d1.fp2", "d0.fp2", "h0.xp", "h0.xm", "d1.fm1", "d0.fm1",
+    "d1.fp0", "d0.fp0", "h0.end", "norm20", "v.end", "h2.fp", "h2.fm", "d0.fm3", "d1.fm3", "d0.fp3", "d1.fp3",
+    "expand0", "h1.xp", "h1.xm", "d1.fm0", "d0.fm0", "activate0", "d0.fp1", "d1.fp1", "h1.end", "norm21", "h2.xp",
+    "h2.xm", "d1.gp0", "d0.gp0", "d1.gm1", "d0.gm1", "expand1", "h2.end", "d0.gm3", "d1.gm3", "d1.gp2", "d0.gp2",
+    "activate1", "norm22", "expand2", "activate2", "d.end", "two.other0", "two.own0", "two.other1", "two0.pair0",
+    "two.own1", "two1.pair0", "two2.pair0", "two.other2", "two0.pair1", "two1.pair1", "two.own2", "two2.pair1",
+    "two.other3", "two0.pair2", "two1.pair2", "two.own3", "two2.pair2", "two0.pass", "two0.pair3", "two1.pair3",
+    "two2.pair3", "two1.pass", "two2.pass", "finish0", "finish1", "finish2",
+)
 
 
 def at(value, step):
@@ -59,6 +87,7 @@
     ssend,
     d2,
     fin,
+    out_s,
     send_sem,
     recv_sem,
     local_sem,
@@ -108,9 +137,13 @@
         start, size = (h * 64, 64) if q is None else (h * 64 + q * 32, 32)
         return projw.at[pl.ds(at(g * 128 + start, 32), size), :]
 
-    def up_slice(g, h, q):
+    def gate_slice(g, h, q):
         start, size = (h * 64, 64) if q is None else (h * 64 + q * 32, 32)
-        return upw.at[pl.ds(at(g * 128 + start, 32), size), :]
+        return upw.at[pl.ds(at(g * 128 + start, 32), size), pl.ds(0, 640)]
+
+    def value_slice(g, h, q):
+        start, size = (h * 64, 64) if q is None else (h * 64 + q * 32, 32)
+        return upw.at[pl.ds(at(g * 128 + start, 32), size), pl.ds(640, 768)]
 
     def mix_slice(g, h, q):
         start, size = (h * 128, 128) if q is None else (h * 128 + q * 64, 64)
@@ -120,87 +153,62 @@
         start, size = (h * 352, 352) if q is None else (h * 352 + q * 176, 176)
         return downw.at[pl.ds(start, size), pl.ds(at(g * 128, 128), 128)]
 
+    ROUTE = {
+        "np": ((0, 0, None), (-1, 0, None), "np", ()),
+        "nm": ((0, 0, None), (1, 0, None), "nm", ()),
+        "qp": ((-1, 0, 0), (2, 0, 0), "np", ("np",)),
+        "qm": ((1, 0, 1), (2, 0, 1), "nm", ("nm",)),
+        "fp0": ((0, 0, None), (0, -1, None), "fp", ()),
+        "fm0": ((0, 0, None), (0, 1, None), "fm", ()),
+        "fp1": ((-1, 0, None), (-1, -1, None), "fp", ("np",)),
+        "fm1": ((-1, 0, None), (-1, 1, None), "fm", ("np",)),
+        "fp2": ((1, 0, None), (1, -1, None), "fp", ("nm",)),
+        "fm2": ((1, 0, None), (1, 1, None), "fm", ("nm",)),
+        "fp3": ((2, 0, None), (2, -1, None), "fp", ("qp", "qm")),
+        "fm3": ((2, 0, None), (2, 1, None), "fm", ("qp", "qm")),
+        "gp0": ((0, -1, None), (0, 2, None), "fp", ("fp0",)),
+        "gm1": ((-1, 1, None), (-1, 2, None), "fm", ("fm1",)),
+        "gp2": ((1, -1, None), (1, 2, None), "fp", ("fp2",)),
+        "gm3": ((2, 1, None), (2, 2, None), "fm", ("fm3",)),
+    }
+    LINKS = (
+        {"np": xp, "nm": xm, "fp": zp, "fm": zm},
+        {"np": zp, "nm": zm, "fp": xp, "fm": xm},
+    )
+
     class Gather:
         def __init__(self, name, view):
-            self.name, self.view = name, view
-
-        def blk(self, h, i, j, q=None):
+            self.name, self.view, self.got = name, view, set()
+
+        def blk(self, h, where):
+            i, j, q = where
             g = 4 * near(z, j) + near(x, i) if h == 0 else 4 * near(z, i) + near(x, j)
             return self.view(g, h, q)
 
-        def dev(self, h, which):
-            first = {"np": xp, "nm": xm, "fp": zp, "fm": zm}
-            second = {"np": zp, "nm": zm, "fp": xp, "fm": xm}
-            return (first if h == 0 else second)[which]
-
-        def put(self, h, i, j, which, tag, q=None):
-            ref = self.blk(h, i, j, q)
-            send(ref, ref, (self.name, h, tag), self.dev(h, which))
-
-        def get(self, h, i, j, tag, q=None):
-            arrive(self.blk(h, i, j, q), (self.name, h, tag))
-
-        def r0(self):
-            for h in (0, 1):
-                self.put(h, 0, 0, "np", "np")
-                self.put(h, 0, 0, "nm", "nm")
-
-        def r1(self):
-            for h in (0, 1):
-                self.put(h, 0, 0, "fp", "fp0")
-                self.put(h, 0, 0, "fm", "fm0")
-
-        def r2(self):
-            for h in (0, 1):
-                self.get(h, -1, 0, "np")
-                self.put(h, -1, 0, "np", "qp", 0)
-                self.get(h, 1, 0, "nm")
-                self.put(h, 1, 0, "nm", "qm", 1)
-            for h in (0, 1):
-                self.put(h, -1, 0, "fp", "fp1")
-                self.put(h, -1, 0, "fm", "fm1")
-                self.put(h, 1, 0, "fp", "fp2")
-                self.put(h, 1, 0, "fm", "fm2")
-
-        def r3(self):
-            for h in (0, 1):
-                self.get(h, 2, 0, "qp", 0)
-                self.get(h, 2, 0, "qm", 1)
-                self.put(h, 2, 0, "fp", "fp3")
-                self.put(h, 2, 0, "fm", "fm3")
-
-        def r4a(self):
-            for h in (0, 1):
-                self.get(h, 0, -1, "fp0")
-                self.put(h, 0, -1, "fp", "gp0")
-                self.get(h, 0, 1, "fm0")
-
-        def r4b(self):
-            for h in (0, 1):
-                self.get(h, -1, -1, "fp1")
-                self.get(h, -1, 1, "fm1")
-                self.put(h, -1, 1, "fm", "gm1")
-                self.get(h, 1, -1, "fp2")
-                self.put(h, 1, -1, "fp", "gp2")
-                self.get(h, 1, 1, "fm2")
-
-        def r4c(self):
-            for h in (0, 1):
-                self.get(h, 2, -1, "fp3")
-                self.get(h, 2, 1, "fm3")
-                self.put(h, 2, 1, "fm", "gm3")
+        def get(self, h, tag):
+            if (h, tag) not in self.got:
+                self.got.add((h, tag))
+                arrive(self.blk(h, ROUTE[tag][1]), (self.name, h, tag))
+
+        def put(self, h, tag):
+            leaves, _, link, needs = ROUTE[tag]
+            for need in needs:
+                self.get(h, need)
+            ref = self.blk(h, leaves)
+            send(ref, ref, (self.name, h, tag), LINKS[h][link])
 
         def end(self):
-            for h in (0, 1):
-                self.get(h, 0, 2, "gp0")
-                self.get(h, 1, 2, "gp2")
-                self.get(h, -1, 2, "gm1")
-                self.get(h, 2, 2, "gm3")
-
-    proj = Gather("p", proj_slice)
-    mix = Gather("m", mix_slice)
-    up = Gather("u", up_slice)
-    down = Gather("d", down_slice)
+            for tag in ROUTE:
+                for h in (0, 1):
+                    self.get(h, tag)
+
+    gathers = {
+        "p": Gather("p", proj_slice),
+        "m": Gather("m", mix_slice),
+        "u": Gather("u", gate_slice),
+        "v": Gather("v", value_slice),
+        "d": Gather("d", down_slice),
+    }
 
 
     class Rows:
@@ -227,17 +235,21 @@
             self.put(0, "am", ym)
             self.put(0, "c0", pc)
 
-        def forward(self):
+        def fp(self):
             self.get(-1, "ap")
             self.put(-1, "bp", yp, 0)
+            self.put(-1, "c1", pc)
+
+        def fm(self):
             self.get(1, "am")
             self.put(1, "bm", ym, 1)
-            self.put(-1, "c1", pc)
             self.put(1, "c2", pc)
 
-        def across(self):
+        def xp(self):
             self.get(2, "bp", False, 0)
             self.put(2, "c3", pc, 0)
+
+        def xm(self):
             self.get(2, "bm", False, 1)
             self.put(2, "c4", pc, 1)
 
@@ -259,34 +271,31 @@
             self.ssend, self.d2, self.fin = ssend.at[n], d2.at[n], fin.at[n]
             self.keep = keep.at[r]
 
-        def terms(self, lhs, weight):
-            for k, dy in enumerate(ORDER):
-                col = at(256 * (2 * near(y, dy) + 1 - c), 256)
-                term = jnp.dot(lhs[...], weight[:, pl.ds(col, 256)], preferred_element_type=F32)
-                self.psend[k] = term.astype(BF16)
-                send(self.psend.at[k], self.precv.at[k], (self.name, "p", k), pc)
-            for k, dy in enumerate(ORDER):
-                col = at(256 * (2 * near(y, dy) + c), 256)
-                self.keep[k] = jnp.dot(lhs[...], weight[:, pl.ds(col, 256)], preferred_element_type=F32)
+        def other(self, k, term):
+            self.psend[k] = term.astype(BF16)
+            send(self.psend.at[k], self.precv.at[k], (self.name, "p", k), pc)
+
+        def pair(self, k):
+            arrive(self.precv.at[k], (self.name, "p", k))
+            total = self.keep[k] + self.precv[k].astype(F32)
+            if k == 0:
+                self.ssend[0] = total.astype(BF16)
+                send(self.ssend.at[0, pl.ds(0, H)], self.d2.at[0], (self.name, "dp"), yp)
+                send(self.ssend.at[0, pl.ds(H, H)], self.d2.at[1], (self.name, "dm"), ym)
+            elif k == 1:
+                self.ssend[1, H:] = total[H:].astype(BF16)
+                send(self.ssend.at[1, pl.ds(H, H)], self.fin.at[0, pl.ds(H, H)], (self.name, "ep"), yp)
+                self.keep[1, :H] = total[:H]
+            elif k == 2:
+                self.ssend[2, :H] = total[:H].astype(BF16)
+                send(self.ssend.at[2, pl.ds(0, H)], self.fin.at[1, pl.ds(0, H)], (self.name, "em"), ym)
+                self.keep[2, H:] = total[H:]
+            else:
+                self.keep[3] = total
 
         def pairs(self):
             for k in range(4):
-                arrive(self.precv.at[k], (self.name, "p", k))
-                total = self.keep[k] + self.precv[k].astype(F32)
-                if k == 0:
-                    self.ssend[0] = total.astype(BF16)
-                    send(self.ssend.at[0, pl.ds(0, H)], self.d2.at[0], (self.name, "dp"), yp)
-                    send(self.ssend.at[0, pl.ds(H, H)], self.d2.at[1], (self.name, "dm"), ym)
-                elif k == 1:
-                    self.ssend[1, H:] = total[H:].astype(BF16)
-                    send(self.ssend.at[1, pl.ds(H, H)], self.fin.at[0, pl.ds(H, H)], (self.name, "ep"), yp)
-                    self.keep[1, :H] = total[:H]
-                elif k == 2:
-                    self.ssend[2, :H] = total[:H].astype(BF16)
-                    send(self.ssend.at[2, pl.ds(0, H)], self.fin.at[1, pl.ds(0, H)], (self.name, "em"), ym)
-                    self.keep[2, H:] = total[H:]
-                else:
-                    self.keep[3] = total
+                self.pair(k)
 
         def pass_on(self):
             arrive(self.d2.at[0], (self.name, "dp"))
@@ -303,6 +312,25 @@
             arrive(self.fin.at[1, pl.ds(H, H)], (self.name, "fm"))
             return self.keep[3] + self.fin[0].astype(F32) + self.fin[1].astype(F32)
 
+
+    def columns(k, side):
+        return pl.ds(at(256 * (2 * near(y, ORDER[k]) + side), 256), 256)
+
+    def mix_terms(r):
+        for k in range(4):
+            one[r].other(k, jnp.dot(gated[r], mixw[:, columns(k, 1 - c)], preferred_element_type=F32))
+        for k in range(4):
+            one[r].keep[k] = jnp.dot(gated[r], mixw[:, columns(k, c)], preferred_element_type=F32)
+
+    def down_other(k):
+        term = jnp.dot(act[...], downw[:, columns(k, 1 - c)], preferred_element_type=F32)
+        for r in range(CHUNKS):
+            two[r].other(k, term[r * R : (r + 1) * R])
+
+    def down_own(k):
+        term = jnp.dot(act[...], downw[:, columns(k, c)], preferred_element_type=F32)
+        for r in range(CHUNKS):
+            two[r].keep[k] = term[r * R : (r + 1) * R]
 
     def norm(src, gain, start, count):
         def body(i, carry):
@@ -351,12 +379,12 @@
         for j in range(5):
             g = conv_cols(r, 128 * j, 0, j)
             v = conv_cols(r, 640 + 128 * j, 1, j)
-            act[r, :, pl.ds(128 * j, 128)] = (g / (1.0 + jnp.exp(-g)) * v).astype(BF16)
+            act[pl.ds(r * R, R), pl.ds(128 * j, 128)] = (g / (1.0 + jnp.exp(-g)) * v).astype(BF16)
         g = conv_cols(r, 1280, 0, 5)
         v = pltpu.roll(conv_cols(r, 1280, 1, 5), 64, 1)
         lane = lax.broadcasted_iota(jnp.int32, (R, 128), 1)
         last = jnp.where(lane < 64, g / (1.0 + jnp.exp(-g)) * v, 0.0)
-        act[r, :, pl.ds(640, 128)] = last.astype(BF16)
+        act[pl.ds(r * R, R), pl.ds(640, 128)] = last.astype(BF16)
 
 
     own_cols = pl.ds(at(256 * t, 256), 256)
@@ -384,123 +412,82 @@
     downw[704:768, :] = jnp.zeros((64, D), BF16)
     taps_s[...] = jnp.zeros((8, 768), F32)
     for which in (0, 1):
-        taps_s[4 * which : 4 * which + 3, 0:704] = ffn_taps[which]
+        for k in range(3):
+            taps_s[4 * which + k : 4 * which + k + 1, 0:704] = ffn_taps[k, which : which + 1]
         taps_s[4 * which + 3 : 4 * which + 4, 0:704] = ffn_bias[which : which + 1]
     tail = taps_s[4:8, 640:768]
     taps_s[4:8, 640:768] = pltpu.roll(tail, 64, 1)
     pl.semaphore_wait(barrier, 7)
 
-    tok = Rows("t", rows, 0, SEQ)
+    tok = [Rows(("t", r), rows, r * R, R) for r in range(CHUNKS)]
     hid = [Rows(("h", r), rows2, r * R, R) for r in range(CHUNKS)]
     one = [Sums(0, r) for r in range(CHUNKS)]
     two = [Sums(1, r) for r in range(CHUNKS)]
 
-    local[0].wait()
-    tok.own()
-    for copy in local[1:4]:
-        copy.wait()
-    proj.r0()
-    proj.r1()
-    local[4].wait()
-    mix.r0()
-    mix.r1()
-    for copy in local[5:8]:
-        copy.wait()
-    upw[own_rows, 0:640] = gstage[:, 0:640]
-    upw[own_rows, 640:1280] = vstage[:, 0:640]
-    upw[own_rows, 1280:1408] = jnp.concatenate([gstage[:, 640:704], vstage[:, 640:704]], axis=1)
-
-    proj.r2()
-    proj.r4a()
-    proj.r3()
-    mix.r2()
-    tok.forward()
-    proj.r4b()
-    mix.r4a()
-    mix.r3()
-    up.r0()
-    up.r1()
-    proj.r4c()
-    mix.r4b()
-    tok.across()
-    mix.r4c()
-    tok.end()
-    norm(rows, mix_gain, 0, SEQ)
-    proj.end()
-    up.r2()
-    project(0)
-    mix.end()
-    one[0].terms(gated.at[0], mixw)
-    up.r4a()
-    project(1)
-    one[0].pairs()
-    one[1].terms(gated.at[1], mixw)
-    up.r3()
-    down.r0()
-    project(2)
-    one[1].pairs()
-    one[0].pass_on()
-    one[2].terms(gated.at[2], mixw)
-    one[2].pairs()
-    one[1].pass_on()
-    down.r1()
+    def place(lo, hi):
+        for copy in local[lo:hi]:
+            copy.wait()
+
+    def lay_up():
+        place(5, 7)
+        for j in range(5):
+            lanes = pl.ds(128 * j, 128)
+            upw[own_rows, lanes] = gstage[lanes, :].T
+            upw[own_rows, pl.ds(640 + 128 * j, 128)] = vstage[lanes, :].T
+        upw[own_rows, 1280:1408] = jnp.concatenate([gstage[640:704, :], vstage[640:704, :]], axis=0).T
 
     def hidden(r):
         rr = pl.ds(r * R, R)
         total = rows[rr, own_cols].astype(F32) + one[r].total()
         rows2[rr, own_cols] = total.astype(BF16)
-        hid[r].own()
-
-    up.r4b()
-    hidden(0)
-    one[2].pass_on()
-    hidden(1)
-    hid[0].forward()
-    down.r2()
-    hidden(2)
-    hid[1].forward()
-    hid[0].across()
-    up.r4c()
-    hid[0].end()
-    norm(rows2, ffn_gain, 0, R)
-    hid[2].forward()
-    hid[1].across()
-    down.r4a()
-    down.r3()
-    hid[1].end()
-    norm(rows2, ffn_gain, R, R)
-    hid[2].across()
-    down.r4b()
-    hid[2].end()
-    norm(rows2, ffn_gain, 2 * R, R)
-    up.end()
-    expand(0)
-    down.r4c()
-    activate(0)
-    down.end()
-    two[0].terms(act.at[0], downw)
-    expand(1)
-    two[0].pairs()
-    activate(1)
-    two[1].terms(act.at[1], downw)
-    two[0].pass_on()
-    expand(2)
-    two[1].pairs()
-    activate(2)
-    two[1].pass_on()
-    two[2].terms(act.at[2], downw)
-    two[2].pairs()
 
     def finish(r):
         rr = pl.ds(r * R, R)
-        out[rr, :] = (rows2[rr, own_cols].astype(F32) + two[r].total()).astype(BF16)
-
-    finish(0)
-    two[2].pass_on()
-    finish(1)
-    finish(2)
+        out_s[rr, :] = (rows2[rr, own_cols].astype(F32) + two[r].total()).astype(BF16)
+        pltpu.make_async_copy(out_s.at[rr, :], out.at[rr, :], local_sem.at[LOCALS + r]).start()
+
+    steps = {
+        "place_t": (place, 0, 1),
+        "place_p": (place, 1, 4),
+        "place_m": (place, 4, 5),
+        "lay_up": (lay_up,),
+        "place_d": (place, 7, 8),
+    }
+    for r in range(CHUNKS):
+        steps[f"norm{r}"] = (norm, rows, mix_gain, r * R, R)
+        steps[f"project{r}"] = (project, r)
+        steps[f"one{r}.terms"] = (mix_terms, r)
+        steps[f"one{r}.pairs"] = (one[r].pairs,)
+        steps[f"one{r}.pass"] = (one[r].pass_on,)
+        steps[f"hidden{r}"] = (hidden, r)
+        steps[f"norm2{r}"] = (norm, rows2, ffn_gain, r * R, R)
+        steps[f"expand{r}"] = (expand, r)
+        steps[f"activate{r}"] = (activate, r)
+        steps[f"two{r}.pass"] = (two[r].pass_on,)
+        steps[f"finish{r}"] = (finish, r)
+        for name, part in (("t", tok[r]), ("h", hid[r])):
+            for tag in ("own", "fp", "fm", "xp", "xm", "end"):
+                steps[f"{name}{r}.{tag}"] = (getattr(part, tag),)
+        for k in range(4):
+            steps[f"two{r}.pair{k}"] = (two[r].pair, k)
+    for k in range(4):
+        steps[f"two.other{k}"] = (down_other, k)
+        steps[f"two.own{k}"] = (down_own, k)
+    for name, part in gathers.items():
+        steps[f"{name}.end"] = (part.end,)
+        for h in (0, 1):
+            for tag in ROUTE:
+                steps[f"{name}{h}.{tag}"] = (part.put, h, tag)
+    for name in PLAN:
+        step, *given = steps.pop(name)
+        with jax.named_scope(name):
+            step(*given)
+    assert not steps
     for copy in sent:
         copy.wait_send()
+    for r in range(CHUNKS):
+        rr = pl.ds(r * R, R)
+        pltpu.make_async_copy(out_s.at[rr, :], out.at[rr, :], local_sem.at[LOCALS + r]).wait()
 
 
 def on_device(
@@ -526,7 +513,7 @@
         kernel,
         out_shape=jax.ShapeDtypeStruct((SEQ, 256), BF16),
         in_specs=[hbm, vmem, hbm, hbm, hbm, vmem, vmem, hbm, vmem, hbm, hbm, vmem, vmem, hbm],
-        out_specs=vmem,
+        out_specs=hbm,
         scratch_shapes=[
             pltpu.VMEM((SEQ, D), BF16),
             pltpu.VMEM((SEQ, D), BF16),
@@ -535,13 +522,13 @@
             pltpu.VMEM((256, D), BF16),
             pltpu.VMEM((D, 1408), BF16),
             pltpu.VMEM((768, D), BF16),
-            pltpu.VMEM((128, 704), BF16),
-            pltpu.VMEM((128, 704), BF16),
+            pltpu.VMEM((704, 128), BF16),
+            pltpu.VMEM((704, 128), BF16),
             pltpu.VMEM((R, 256), F32),
             pltpu.VMEM((8 + SEQ, 256), F32),
             pltpu.VMEM((CHUNKS, R, 256), BF16),
             pltpu.VMEM((8 + SEQ, 1408), F32),
-            pltpu.VMEM((CHUNKS, R, 768), BF16),
+            pltpu.VMEM((SEQ, 768), BF16),
             pltpu.VMEM((8, 768), F32),
             pltpu.VMEM((CHUNKS, 4, R, 256), F32),
             pltpu.VMEM((n, 4, R, 256), BF16),
@@ -549,9 +536,10 @@
             pltpu.VMEM((n, 3, R, 256), BF16),
             pltpu.VMEM((n, 2, H, 256), BF16),
             pltpu.VMEM((n, 2, R, 256), BF16),
+            pltpu.VMEM((SEQ, 256), BF16),
             pltpu.SemaphoreType.DMA((COPIES,)),
             pltpu.SemaphoreType.DMA((COPIES,)),
-            pltpu.SemaphoreType.DMA((LOCALS,)),
+            pltpu.SemaphoreType.DMA((LOCALS + CHUNKS,)),
         ],
         compiler_params=pltpu.CompilerParams(
             collective_id=0, has_side_effects=True, vmem_limit_bytes=62 * 1024 * 1024
@@ -566,9 +554,9 @@
         mix_bias.reshape(1, 256),
         mix_out,
         ffn_gain.reshape(1, D),
-        up_gate,
-        up_value,
-        ffn_taps,
+        up_gate.T,
+        up_value.T,
+        jnp.transpose(ffn_taps, (1, 0, 2)),
         ffn_bias,
         down_proj,
     )

time: 115 us -> 100 us (0.87); the launches traced: 113 us -> 100 us
  Pallas kernels: 107 us -> 98.3 us
  local copies, waits for them, and re-layouts: 5.7 us -> 1.77 us
    pallas_call x1, Pallas kernels: 107 us -> 98.3 us  [on_device(): pl.pallas_call(kernel, out_shape=jax.ShapeDtypeStruct((SEQ, 256), BF16),...]
    unnamed x6 -> x1, local copies, waits for them, and re-layouts: 5.7 us -> 1.77 us
where the time goes in v2:
time: 100 us
  Pallas kernels  98.3 us (98%)
  local copies, waits for them, and re-layouts  1.77 us (2%)
    pallas_call x1, Pallas kernels, on_device(): pl.pallas_call(kernel, out_shape=jax.ShapeDtypeStruct((SEQ, 256), BF16),...  98.3 us

profile of v2, /device:TPU:1, one launch (start us, length us, event | category | flops | bytes accessed | tf_op | source)
XLA Modules:
  0.0 100.1 jit_solution(14142675763152959348)
XLA Ops:
  0.0 98.3 %shard_map.136 = bf16[768,256]{1,0:T(8,128)(2,1)} custom-call(bf16[768,256]{1,0:T(8,128)(2,1)} %tokens.1, f32[1,2048]{1,0:T(1,128)} %bitcast.9, bf16[128,256]{1,0:T(8,128)(2,1)} %outer_gate.1, bf16[128,256]{1,0:T(8,128)(2,1)} %inner_gate.1, bf16[128,256]{1,0:T(8,128)(2,1)} %signal_in.1, f32[3,256]{1,0:T(4,128)} %mix_taps.1, f32[1,256]{1,0:T(1,128)} %bitcast.11, ...), custom_call_target="tpu_custom_call" | custom-call | tf_op jit(solution)/shard_map/pallas_call | solution.py:512
  98.3 1.8 %copy.16 = bf16[768,256]{1,0:T(8,128)(2,1)} copy(bf16[768,256]{1,0:T(8,128)(2,1)} %shard_map.136) | data formatting | bytes 786432

commit v3 on v0

v3 whole, which is shorter than its diff:
```python
import jax
import jax.numpy as jnp
from jax import lax
from jax.experimental import pallas as pl
from jax.experimental.pallas import tpu as pltpu
from jax.sharding import PartitionSpec as P

EPS = 1e-06
MESH = pl.DeviceIdType.MESH
BF16 = jnp.bfloat16
F32 = jnp.float32
SEQ = 768
D = 2048
CHUNKS = 4
R = SEQ // CHUNKS
PIECES = 3
Q = SEQ // PIECES
RECEIVES = 162
GROUPS = 12
NP, NM, QP, QM, FP0, FM0, FP1, FM1, FP2, FM2, FP3, FM3, GP0, GM1, GP2, GM3 = range(16)
ROUTE = {
    NP: ((0, 0, None), (-1, 0, None), 0, (), False),
    NM: ((0, 0, None), (1, 0, None), 1, (), False),
    QP: ((-1, 0, 0), (2, 0, 0), 0, (NP,), False),
    QM: ((1, 0, 1), (2, 0, 1), 1, (NM,), False),
    FP0: ((0, 0, None), (0, -1, None), 2, (), False),
    FM0: ((0, 0, None), (0, 1, None), 3, (), True),
    FP1: ((-1, 0, None), (-1, -1, None), 2, (NP,), True),
    FM1: ((-1, 0, None), (-1, 1, None), 3, (NP,), False),
    FP2: ((1, 0, None), (1, -1, None), 2, (NM,), False),
    FM2: ((1, 0, None), (1, 1, None), 3, (NM,), True),
    FP3: ((2, 0, None), (2, -1, None), 2, (QP,), True),
    FM3: ((2, 0, None), (2, 1, None), 3, (QP,), False),
    GP0: ((0, -1, None), (0, 2, None), 2, (FP0,), True),
    GM1: ((-1, 1, None), (-1, 2, None), 3, (FM1,), True),
    GP2: ((1, -1, None), (1, 2, None), 2, (FP2,), True),
    GM3: ((2, 1, None), (2, 2, None), 3, (FM3,), True),
}
ORDER = (2, 1, 3, 0)


def at(value, step):
    return pl.multiple_of(value, step)


def kernel(
    tokens,
    mix_gain,
    outer_gate,
    inner_gate,
    signal_in,
    mix_taps,
    mix_bias,
    mix_out,
    ffn_gain,
    up_gate,
    up_value,
    ffn_taps,
    ffn_bias,
    down_proj,
    out,
    rows,
    rows2,
    normed,
    projw,
    mixw,
    upw,
    downw,
    downw2,
    gstage,
    vstage,
    dstage,
    outer_s,
    mi,
    gated,
    pre,
    act,
    taps_s,
    keep1,
    psend1,
    precv1,
    ssend1,
    mid1,
    fin1,
    keep2,
    psend2,
    precv2,
    ssend2,
    mid2,
    fin2,
    send_sem,
    recv_sem,
    local_sem,
):
    f = lax.axis_index("fs")
    t = lax.axis_index("tp")
    z, x = f // 4, f % 4
    y, c = t // 2, t % 2

    def near(v, i):
        return (v + i + 4) % 4

    xp, xm = (4 * z + near(x, 1), t), (4 * z + near(x, -1), t)
    zp, zm = (4 * near(z, 1) + x, t), (4 * near(z, -1) + x, t)
    yp, ym = (f, 2 * near(y, 1) + c), (f, 2 * near(y, -1) + c)
    pc = (f, 2 * y + 1 - c)

    ids = {}

    def copy_of(src, dst, key, group, dev):
        return pltpu.make_async_remote_copy(
            src_ref=src,
            dst_ref=dst,
            send_sem=send_sem.at[group],
            recv_sem=recv_sem.at[ids.setdefault(key, len(ids))],
            device_id=dev,
            device_id_type=MESH,
        )

    def send(src, dst, key, group, dev):
        copy_of(src, dst, key, group, dev).start()

    def arrive(dst, key):
        copy_of(dst, dst, key, 0, pc).wait_recv()

    def all_sent(src, group):
        copy_of(src, src, (0, 0, NP), group, pc).wait_send()


    def by_rows(buf, lanes, depth):
        def view(g, h, q):
            start, size = (h * depth // 2, depth // 2) if q is None else (h * depth // 2 + q * depth // 4, depth // 4)
            return buf.at[pl.ds(at(g * depth + start, depth // 4), size), lanes]

        return view

    def by_columns(buf, depth):
        def view(g, h, q):
            start, size = (h * depth // 2, depth // 2) if q is None else (h * depth // 2 + q * depth // 4, depth // 4)
            return buf.at[pl.ds(start, size), pl.ds(at(g * 128, 128), 128)]

        return view

    LINKS = ((xp, xm, zp, zm), (zp, zm, xp, xm))

    class Gather:
        def __init__(self, group, view, sent, rest):
            self.group, self.view, self.got = group, view, set()
            self.sent, self.rest = sent, rest

        def blk(self, h, where):
            i, j, q = where
            g = 4 * near(z, j) + near(x, i) if h == 0 else 4 * near(z, i) + near(x, j)
            return self.view(g, h, q)

        def key(self, h, tag):
            if ROUTE[tag][4]:
                return (self.group, 0, -1)
            return (self.group, h, QP if tag == QM else tag)

        def get(self, h, tag):
            if (h, tag) not in self.got:
                self.got.add((h, tag))
                i, j, _ = ROUTE[tag][1]
                arrive(self.blk(h, (i, j, None)), self.key(h, tag))

        def put(self, h, tag):
            leaves, _, link, needs, _ = ROUTE[tag]
            for need in needs:
                self.get(h, need)
            ref = self.blk(h, leaves)
            i, j, q = leaves
            send(ref, ref, self.key(h, tag), self.group, LINKS[h][link])

        def end(self):
            for tag in (NP, NM, QP, FP0, FM1, FP2, FM3):
                for h in (0, 1):
                    self.get(h, tag)
            arrive(self.rest, (self.group, 0, -1))

    main, second = pl.ds(0, 640), pl.ds(640, 768)
    every = pl.ds(0, 768)
    gp = Gather(0, by_rows(projw, every, 128), projw.at[pl.ds(0, 1920), :], projw.at[pl.ds(0, 1024), :])
    gm = Gather(1, by_columns(mixw, 256), mixw.at[:, pl.ds(0, 1920)], mixw.at[:, pl.ds(0, 1024)])
    gu = Gather(2, by_rows(upw, main, 128), upw.at[pl.ds(0, 1920), main], upw.at[pl.ds(0, 1024), main])
    gv = Gather(3, by_rows(upw, second, 128), upw.at[pl.ds(0, 1920), second], upw.at[pl.ds(0, 1024), second])
    gd = Gather(4, by_rows(downw, every, 64), downw.at[pl.ds(0, 960), :], downw.at[pl.ds(0, 512), :])
    ge = Gather(5, by_rows(downw2, main, 64), downw2.at[pl.ds(0, 960), :], downw2.at[pl.ds(0, 512), :])


    class Rows:
        def __init__(self, group, buf, r):
            self.group, self.buf, self.r = group, buf, r

        def view(self, dy, half=None):
            start, size = self.r * R, R
            if half is not None:
                size = size // 2
                start = start + half * size
            return self.buf.at[pl.ds(start, size), pl.ds(at(256 * (2 * near(y, dy) + c), 256), 256)]

        def put(self, dy, tag, dev, half=None):
            ref = self.view(dy, half)
            send(ref, ref, (self.group, self.r, tag), self.group, dev)

        def get(self, dy, tag, half=None):
            arrive(self.view(dy, half), (self.group, self.r, tag))

        def own(self):
            self.put(0, 0, yp)
            self.put(0, 1, ym)
            self.put(0, 4, pc)

        def fp(self):
            self.get(-1, 0)
            self.put(-1, 2, yp, 0)
            self.put(-1, 4, pc)

        def fm(self):
            self.get(1, 1)
            self.put(1, 3, ym, 1)
            self.put(1, 4, pc)

        def xp(self):
            self.get(2, 2, 0)
            self.put(2, 4, pc, 0)

        def xm(self):
            self.get(2, 3, 1)
            self.put(2, 4, pc, 1)

        def end(self):
            arrive(self.buf.at[pl.ds(self.r * R, R), pl.ds(0, 1024)], (self.group, self.r, 4))

    tok = [Rows(6, rows, r) for r in range(CHUNKS)]
    hid = [Rows(7, rows2, r) for r in range(CHUNKS)]


    class Sums:
        def __init__(self, group, r, start, size, keep, mine, leave, mid, fin):
            self.group, self.r, self.start, self.size = group, r, start, size
            self.keep, self.mine, self.leave, self.mid, self.fin = keep, mine, leave, mid, fin

        def pair(self, k):
            n, half = self.size, self.size // 2
            mine = pl.ds(self.start, n)
            total = self.keep[k, mine] + self.mine[k, mine].astype(F32)
            key, keys = (self.group, self.r, 2), (self.group, self.r, 3)
            if k == 0:
                self.leave[0] = total.astype(BF16)
                send(self.leave.at[0, pl.ds(0, half)], self.mid.at[0], key, self.group, yp)
                send(self.leave.at[0, pl.ds(half, half)], self.mid.at[1], key, self.group, ym)
            elif k == 1:
                self.leave[1, half:] = total[half:].astype(BF16)
                part = pl.ds(half, half)
                send(self.leave.at[1, part], self.fin.at[0, part], keys, self.group, yp)
                self.keep[k, pl.ds(self.start, half)] = total[:half]
            elif k == 2:
                self.leave[2, :half] = total[:half].astype(BF16)
                part = pl.ds(0, half)
                send(self.leave.at[2, part], self.fin.at[1, part], keys, self.group, ym)
                self.keep[k, pl.ds(self.start + half, half)] = total[half:]
            else:
                self.keep[k, mine] = total

        def pass_on(self):
            half = self.size // 2
            low, high = pl.ds(0, half), pl.ds(half, half)
            keys = (self.group, self.r, 3)
            arrive(self.mid, (self.group, self.r, 2))
            self.leave[1, low] = (self.keep[1, pl.ds(self.start, half)] + self.mid[0].astype(F32)).astype(BF16)
            send(self.leave.at[1, low], self.fin.at[0, low], keys, self.group, yp)
            self.leave[2, high] = (self.keep[2, pl.ds(self.start + half, half)] + self.mid[1].astype(F32)).astype(BF16)
            send(self.leave.at[2, high], self.fin.at[1, high], keys, self.group, ym)

        def total(self):
            arrive(self.fin, (self.group, self.r, 3))
            return self.keep[3, pl.ds(self.start, self.size)] + self.fin[0].astype(F32) + self.fin[1].astype(F32)

    one = [
        Sums(9, r, 0, R, keep1.at[r], precv1.at[r], ssend1.at[r], mid1.at[r], fin1.at[r]) for r in range(CHUNKS)
    ]
    two, tri = (
        [
            Sums(11, n * PIECES + r, r * Q, Q, keep2.at[n], precv2.at[n], ssend2.at[n, r], mid2.at[n, r], fin2.at[n, r])
            for r in range(PIECES)
        ]
        for n in (0, 1)
    )

    def columns(k, side):
        return pl.ds(at(256 * (2 * near(y, ORDER[k]) + side), 256), 256)

    def mix_terms(r):
        for k in range(4):
            term = jnp.dot(gated[r], mixw[:, columns(k, 1 - c)], preferred_element_type=F32)
            psend1[r, k] = term.astype(BF16)
            send(psend1.at[r, k], precv1.at[r, k], (8, r), 8, pc)
        for k in range(4):
            keep1[r, k] = jnp.dot(gated[r], mixw[:, columns(k, c)], preferred_element_type=F32)

    def pairs(r):
        arrive(precv1.at[r], (8, r))
        for k in range(4):
            one[r].pair(k)

    def across(a, b):
        return lax.dot_general(a, b, (((1,), (1,)), ((), ())), preferred_element_type=F32)

    def down_terms(n, k):
        lines = pl.ds(at(256 * near(y, ORDER[k]), 256), 256)
        if n == 0:
            term = across(act[:, 0:768], downw[lines, :])
        else:
            term = across(act[:, 0:640], downw2[lines, :]) + across(act[:, 768:896], downw[lines, 640:768])
        low, high = term[:, 0:128], term[:, 128:256]
        psend2[n, k] = jnp.where(c == 0, high, low).astype(BF16)
        send(psend2.at[n, k], precv2.at[n, k], (10, n, k), 10, pc)
        keep2[n, k] = jnp.where(c == 0, low, high)

    def pair_all(n, k):
        arrive(precv2.at[n, k], (10, n, k))
        for r in range(PIECES):
            (two, tri)[n][r].pair(k)


    def norm(src, gain, r):
        def body(i, carry):
            lines = pl.ds(at(r * R + i * 32, 32), 32)
            v = src[lines, :].astype(F32)
            mean = jnp.sum(v * v, axis=1, keepdims=True) * (1.0 / D)
            normed[lines, :] = (v * lax.rsqrt(mean + EPS) * gain[...]).astype(BF16)
            return carry

        lax.fori_loop(0, R // 32, body, 0)

    def project(r):
        lines, here = pl.ds(r * R, R), pl.ds(8 + r * R, R)
        outer_s[...] = jnp.dot(normed[lines, :], projw[:, 0:256], preferred_element_type=F32)
        mi[here, :] = jnp.dot(normed[lines, :], projw[:, 256:512], preferred_element_type=F32)
        signal = jnp.dot(normed[lines, :], projw[:, 512:768], preferred_element_type=F32)
        mi[here, :] = mi[here, :] * signal
        conv = (
            mix_taps[2:3, :] * mi[here, :]
            + mix_taps[1:2, :] * mi[pl.ds(7 + r * R, R), :]
            + mix_taps[0:1, :] * mi[pl.ds(6 + r * R, R), :]
            + mix_bias[...]
        )
        gated[r] = (outer_s[...] * conv).astype(BF16)

    def expand(r):
        for n in range(6):
            width = 256 if n < 5 else 128
            pre[pl.ds(8 + r * R, R), pl.ds(n * 256, width)] = jnp.dot(
                normed[pl.ds(r * R, R), :], upw[:, n * 256 : n * 256 + width], preferred_element_type=F32
            )

    def conv_cols(r, col, which, j):
        lanes = pl.ds(col, 128)
        taps = taps_s[:, pl.ds(128 * j, 128)]
        a = 4 * which
        return (
            taps[a + 2 : a + 3] * pre[pl.ds(8 + r * R, R), lanes]
            + taps[a + 1 : a + 2] * pre[pl.ds(7 + r * R, R), lanes]
            + taps[a : a + 1] * pre[pl.ds(6 + r * R, R), lanes]
            + taps[a + 3 : a + 4]
        )

    def activate(r):
        lines = pl.ds(r * R, R)
        for j in range(5):
            g = conv_cols(r, 128 * j, 0, j)
            v = conv_cols(r, 640 + 128 * j, 1, j)
            act[lines, pl.ds(128 * j, 128)] = (g / (1.0 + jnp.exp(-g)) * v).astype(BF16)
        g = conv_cols(r, 1280, 0, 5)
        v = pltpu.roll(conv_cols(r, 1280, 1, 5), 64, 1)
        lane = lax.broadcasted_iota(jnp.int32, (R, 128), 1)
        last = jnp.where(lane < 64, g / (1.0 + jnp.exp(-g)) * v, 0.0)
        act[lines, 640:768] = last.astype(BF16)
        act[lines, 768:896] = pltpu.roll(last, 64, 1).astype(BF16)


    own_cols = pl.ds(at(256 * t, 256), 256)
    own_rows = pl.ds(at(128 * f, 128), 128)
    own_lines = pl.ds(at(64 * f, 64), 64)
    moves = [
        (tokens, rows.at[:, own_cols]),
        (outer_gate, projw.at[own_rows, pl.ds(0, 256)]),
        (inner_gate, projw.at[own_rows, pl.ds(256, 256)]),
        (signal_in, projw.at[own_rows, pl.ds(512, 256)]),
        (mix_out, mixw.at[:, own_rows]),
        (up_gate, gstage),
        (up_value, vstage),
        (down_proj, dstage),
    ]
    local = [pltpu.make_async_copy(src, dst, local_sem.at[i]) for i, (src, dst) in enumerate(moves)]
    for copy in local:
        copy.start()

    barrier = pltpu.get_barrier_semaphore()
    for dev in (xp, xm, zp, zm, yp, ym, pc):
        pl.semaphore_signal(barrier, inc=1, device_id=dev, device_id_type=MESH)

    def place(lo, hi):
        for copy in local[lo:hi]:
            copy.wait()

    def lay_up():
        place(5, 7)
        for j in range(5):
            lanes = pl.ds(128 * j, 128)
            upw[own_rows, lanes] = gstage[lanes, :].T
            upw[own_rows, pl.ds(640 + 128 * j, 128)] = vstage[lanes, :].T
        upw[own_rows, 1280:1408] = jnp.concatenate([gstage[640:704, :], vstage[640:704, :]], axis=0).T

    def lay_down():
        place(7, 8)
        for j in range(5):
            lanes = pl.ds(128 * j, 128)
            turned = dstage[lanes, :].T
            downw[own_lines, lanes] = turned[0:64]
            downw2[own_lines, lanes] = turned[64:128]
        tail = dstage[640:704, :].astype(F32)
        both = jnp.concatenate([tail, pltpu.roll(tail, 64, 1)], axis=0).T
        downw[own_lines, 640:768] = both[0:64].astype(BF16)

    def hidden(r):
        lines = pl.ds(r * R, R)
        rows2[lines, own_cols] = (rows[lines, own_cols].astype(F32) + one[r].total()).astype(BF16)

    def finish(r):
        lines = pl.ds(r * Q, Q)
        state = rows2[lines, own_cols].astype(F32)
        a, b = two[r].total(), tri[r].total()
        lane = lax.broadcasted_iota(jnp.int32, (Q, 128), 1)
        first = jnp.where(lane < 64, a, pltpu.roll(b, 64, 1))
        last = jnp.where(lane < 64, pltpu.roll(a, 64, 1), b)
        out[lines, 0:128] = (state[:, 0:128] + first).astype(BF16)
        out[lines, 128:256] = (state[:, 128:256] + last).astype(BF16)

    mi[0:8, :] = jnp.zeros((8, 256), F32)
    pre[0:8, :] = jnp.zeros((8, 1408), F32)
    taps_s[...] = jnp.zeros((8, 768), F32)
    for which in (0, 1):
        for k in range(3):
            taps_s[4 * which + k : 4 * which + k + 1, 0:704] = ffn_taps[k, which : which + 1]
        taps_s[4 * which + 3 : 4 * which + 4, 0:704] = ffn_bias[which : which + 1]
    taps_s[4:8, 640:768] = pltpu.roll(taps_s[4:8, 640:768], 64, 1)
    pl.semaphore_wait(barrier, 7)

    place(0, 1)
    place(1, 4)
    tok[0].own()
    tok[1].own()
    tok[2].own()
    tok[3].own()
    place(4, 5)
    gm.put(0, NM)
    gm.put(1, NM)
    gm.put(0, NP)
    gm.put(1, NP)
    gp.put(0, NM)
    gp.put(1, NM)
    gp.put(0, NP)
    gp.put(1, NP)
    lay_up()
    lay_down()
    gm.put(1, FM0)
    gm.put(0, FM0)
    gm.put(1, FP0)
    gm.put(0, FP0)
    gp.put(1, FM0)
    gp.put(0, FM0)
    gp.put(1, FP0)
    gp.put(0, FP0)
    tok[0].fp()
    tok[0].fm()
    gm.put(0, QM)
    gm.put(1, QM)
    gm.put(0, QP)
    gm.put(1, QP)
    gp.put(0, QM)
    gp.put(1, QM)
    gp.put(0, QP)
    gp.put(1, QP)
    gm.put(1, FM1)
    gm.put(0, FM1)
    gm.put(1, FP1)
    gm.put(0, FP1)
    tok[1].fp()
    tok[1].fm()
    gp.put(1, FM1)
    gp.put(0, FM1)
    gp.put(1, FP1)
    gp.put(0, FP1)
    tok[2].fp()
    tok[2].fm()
    gm.put(1, FM2)
    gm.put(0, FM2)
    gm.put(1, FP3)
    gm.put(0, FP3)
    gp.put(1, FM2)
    gp.put(0, FM2)
    gp.put(1, FP3)
    gp.put(0, FP3)
    tok[3].fp()
    tok[3].fm()
    tok[0].xp()
    tok[0].xm()
    gm.put(1, FM3)
    gm.put(0, FM3)
    gm.put(1, FP2)
    gm.put(0, FP2)
    gp.put(1, FM3)
    gp.put(0, FM3)
    gp.put(1, FP2)
    gp.put(0, FP2)
    tok[1].xp()
    tok[1].xm()
    tok[0].end()
    norm(rows, mix_gain, 0)
    tok[2].xp()
    tok[2].xm()
    tok[1].end()
    norm(rows, mix_gain, 1)
    gm.put(1, GM1)
    gm.put(0, GM1)
    gm.put(1, GP0)
    gm.put(0, GP0)
    tok[3].xp()
    tok[3].xm()
    tok[2].end()
    norm(rows, mix_gain, 2)
    gm.put(1, GM3)
    gm.put(0, GM3)
    gm.put(1, GP2)
    gm.put(0, GP2)
    gp.put(1, GM1)
    gp.put(0, GM1)
    gp.put(1, GP0)
    gp.put(0, GP0)
    tok[3].end()
    norm(rows, mix_gain, 3)
    gp.put(1, GM3)
    gp.put(0, GM3)
    gp.put(1, GP2)
    gp.put(0, GP2)
    gm.end()
    gu.put(0, NM)
    gu.put(1, NM)
    gu.put(0, NP)
    gu.put(1, NP)
    gu.put(1, FM0)
    gu.put(0, FM0)
    gu.put(1, FP0)
    gu.put(0, FP0)
    gp.end()
    project(0)
    gv.put(0, NM)
    gv.put(1, NM)
    gv.put(0, NP)
    gv.put(1, NP)
    mix_terms(0)
    project(1)
    gu.put(0, QP)
    gu.put(1, QP)
    gu.put(0, QM)
    gu.put(1, QM)
    mix_terms(1)
    pairs(0)
    gu.put(0, FM1)
    gu.put(1, FM1)
    gu.put(0, FP1)
    gu.put(1, FP1)
    project(2)
    gu.put(0, FM2)
    gu.put(1, FM2)
    gu.put(0, FP2)
    gu.put(1, FP2)
    mix_terms(2)
    pairs(1)
    project(3)
    gu.put(0, FP3)
    gu.put(1, FP3)
    gu.put(0, FM3)
    gu.put(1, FM3)
    mix_terms(3)
    one[0].pass_on()
    pairs(2)
    gv.put(0, QP)
    gv.put(1, QP)
    gu.put(0, GM1)
    gu.put(1, GM1)
    gu.put(0, GP0)
    gu.put(1, GP0)
    one[1].pass_on()
    pairs(3)
    gv.put(0, QM)
    gv.put(1, QM)
    gv.put(0, FM1)
    gv.put(1, FM1)
    gu.put(0, GP2)
    gu.put(1, GP2)
    hidden(0)
    hid[0].own()
    one[2].pass_on()
    gv.put(0, FP1)
    gv.put(1, FP1)
    gu.put(0, GM3)
    gu.put(1, GM3)
    hidden(1)
    hid[1].own()
    gv.put(0, FM0)
    gv.put(1, FM0)
    gv.put(0, FP3)
    gv.put(1, FP3)
    one[3].pass_on()
    gv.put(0, FM2)
    gv.put(1, FM2)
    gv.put(0, FP0)
    gv.put(1, FP0)
    gu.end()
    hid[0].fp()
    hid[0].fm()
    gv.put(0, FM3)
    gv.put(1, FM3)
    gv.put(0, FP2)
    gv.put(1, FP2)
    hidden(2)
    hid[2].own()
    gd.put(1, NM)
    gd.put(0, NM)
    gd.put(1, NP)
    gd.put(0, NP)
    hid[1].fp()
    hid[1].fm()
    gv.put(0, GM1)
    gv.put(1, GM1)
    gv.put(0, GP0)
    gv.put(1, GP0)
    hidden(3)
    hid[3].own()
    hid[0].xp()
    hid[0].xm()
    gv.put(0, GM3)
    gv.put(1, GM3)
    gv.put(0, GP2)
    gv.put(1, GP2)
    hid[0].end()
    norm(rows2, ffn_gain, 0)
    hid[2].fp()
    hid[2].fm()
    gd.put(1, QM)
    gd.put(0, QM)
    gd.put(1, QP)
    gd.put(0, QP)
    gd.put(0, FM1)
    gd.put(1, FM1)
    gd.put(0, FP1)
    gd.put(1, FP1)
    hid[1].xp()
    hid[1].xm()
    gd.put(0, FM0)
    gd.put(1, FM0)
    gd.put(0, FP0)
    gd.put(1, FP0)
    hid[1].end()
    norm(rows2, ffn_gain, 1)
    gd.put(1, FM2)
    gd.put(0, FM2)
    gd.put(1, FP2)
    gd.put(0, FP2)
    hid[3].fp()
    hid[3].fm()
    gv.end()
    expand(0)
    hid[2].xp()
    hid[2].xm()
    gd.put(1, FP3)
    gd.put(0, FP3)
    gd.put(1, FM3)
    gd.put(0, FM3)
    activate(0)
    ge.put(0, NM)
    ge.put(1, NM)
    ge.put(0, NP)
    ge.put(1, NP)
    expand(1)
    hid[3].xp()
    hid[3].xm()
    hid[2].end()
    gd.put(0, GM1)
    gd.put(1, GM1)
    gd.put(0, GP0)
    gd.put(1, GP0)
    activate(1)
    gd.put(1, GP2)
    gd.put(0, GP2)
    ge.put(0, FM0)
    ge.put(1, FM0)
    norm(rows2, ffn_gain, 2)
    hid[3].end()
    gd.put(1, GM3)
    gd.put(0, GM3)
    ge.put(0, FP0)
    ge.put(1, FP0)
    norm(rows2, ffn_gain, 3)
    ge.put(0, QP)
    ge.put(1, QP)
    ge.put(0, QM)
    ge.put(1, QM)
    expand(2)
    ge.put(0, FM1)
    ge.put(1, FM1)
    ge.put(0, FP1)
    ge.put(1, FP1)
    ge.put(0, FM2)
    ge.put(1, FM2)
    ge.put(0, FP2)
    ge.put(1, FP2)
    activate(2)
    expand(3)
    ge.put(1, FP3)
    ge.put(0, FP3)
    ge.put(0, FM3)
    ge.put(1, FM3)
    ge.put(1, GP0)
    ge.put(0, GP0)
    activate(3)
    gd.end()
    down_terms(0, 0)
    ge.put(0, GM1)
    ge.put(1, GM1)
    down_terms(0, 1)
    ge.put(0, GP2)
    ge.put(1, GP2)
    down_terms(0, 2)
    pair_all(0, 0)
    ge.put(0, GM3)
    ge.put(1, GM3)
    down_terms(0, 3)
    pair_all(0, 1)
    pair_all(0, 2)
    pair_all(0, 3)
    two[0].pass_on()
    ge.end()
    down_terms(1, 0)
    two[1].pass_on()
    down_terms(1, 1)
    two[2].pass_on()
    down_terms(1, 2)
    pair_all(1, 0)
    down_terms(1, 3)
    pair_all(1, 1)
    pair_all(1, 2)
    pair_all(1, 3)
    tri[0].pass_on()
    tri[1].pass_on()
    tri[2].pass_on()
    finish(0)
    finish(1)
    finish(2)
    for gather in (gp, gm, gu, gv, gd, ge):
        all_sent(gather.sent, gather.group)
    all_sent(rows.at[:, pl.ds(0, 1792)], 6)
    all_sent(rows2.at[:, pl.ds(0, 1792)], 7)
    all_sent(psend1, 8)
    all_sent(ssend1, 9)
    all_sent(psend2, 10)
    all_sent(ssend2, 11)
    assert len(ids) == RECEIVES, len(ids)


def on_device(
    tokens,
    mix_gain,
    outer_gate,
    inner_gate,
    signal_in,
    mix_taps,
    mix_bias,
    mix_out,
    ffn_gain,
    up_gate,
    up_value,
    ffn_taps,
    ffn_bias,
    down_proj,
):
    hbm = pl.BlockSpec(memory_space=pltpu.HBM)
    vmem = pl.BlockSpec(memory_space=pltpu.VMEM)
    return pl.pallas_call(
        kernel,
        out_shape=jax.ShapeDtypeStruct((SEQ, 256), BF16),
        in_specs=[hbm, vmem, hbm, hbm, hbm, vmem, vmem, hbm, vmem, hbm, hbm, vmem, vmem, hbm],
        out_specs=vmem,
        scratch_shapes=[
            pltpu.VMEM((SEQ, D), BF16),
            pltpu.VMEM((SEQ, D), BF16),
            pltpu.VMEM((SEQ, D), BF16),
            pltpu.VMEM((D, 768), BF16),
            pltpu.VMEM((256, D), BF16),
            pltpu.VMEM((D, 1408), BF16),
            pltpu.VMEM((1024, 768), BF16),
            pltpu.VMEM((1024, 640), BF16),
            pltpu.VMEM((704, 128), BF16),
            pltpu.VMEM((704, 128), BF16),
            pltpu.VMEM((704, 128), BF16),
            pltpu.VMEM((R, 256), F32),
            pltpu.VMEM((8 + SEQ, 256), F32),
            pltpu.VMEM((CHUNKS, R, 256), BF16),
            pltpu.VMEM((8 + SEQ, 1408), F32),
            pltpu.VMEM((SEQ, 896), BF16),
            pltpu.VMEM((8, 768), F32),
            pltpu.VMEM((CHUNKS, 4, R, 256), F32),
            pltpu.VMEM((CHUNKS, 4, R, 256), BF16),
            pltpu.VMEM((CHUNKS, 4, R, 256), BF16),
            pltpu.VMEM((CHUNKS, 3, R, 256), BF16),
            pltpu.VMEM((CHUNKS, 2, R // 2, 256), BF16),
            pltpu.VMEM((CHUNKS, 2, R, 256), BF16),
            pltpu.VMEM((2, 4, SEQ, 128), F32),
            pltpu.VMEM((2, 4, SEQ, 128), BF16),
            pltpu.VMEM((2, 4, SEQ, 128), BF16),
            pltpu.VMEM((2, PIECES, 3, Q, 128), BF16),
            pltpu.VMEM((2, PIECES, 2, Q // 2, 128), BF16),
            pltpu.VMEM((2, PIECES, 2, Q, 128), BF16),
            pltpu.SemaphoreType.DMA((GROUPS,)),
            pltpu.SemaphoreType.DMA((RECEIVES,)),
            pltpu.SemaphoreType.DMA((8,)),
        ],
        compiler_params=pltpu.CompilerParams(
            collective_id=0, has_side_effects=True, vmem_limit_bytes=56 * 1024 * 1024
        ),
    )(
        tokens,
        mix_gain.reshape(1, D),
        outer_gate,
        inner_gate,
        signal_in,
        mix_taps,
        mix_bias.reshape(1, 256),
        mix_out,
        ffn_gain.reshape(1, D),
        up_gate.T,
        up_value.T,
        jnp.transpose(ffn_taps, (1, 0, 2)),
        ffn_bias,
        down_proj,
    )


def solution(mesh):
    return jax.shard_map(
        on_device,
        mesh=mesh,
        in_specs=(
            P("fs", "tp"),
            P(),
            P("fs", "tp"),
            P("fs", "tp"),
            P("fs", "tp"),
            P(None, "tp"),
            P("tp"),
            P("tp", "fs"),
            P(),
            P("fs", "tp"),
            P("fs", "tp"),
            P(None, None, "tp"),
            P(None, "tp"),
            P("tp", "fs"),
        ),
        out_specs=P("fs", "tp"),
        check_vma=False,
    )
```

time: 311 us -> 94.9 us (0.31)
  waiting for transfers between devices: 227 us -> 0 us
  Pallas kernels: 0 us -> 92.9 us
  matrix products: 35.3 us -> 0 us
  starting transfers between devices: 15.8 us -> 0 us
  between operations: 13.6 us -> 0.01 us
  other arithmetic: 11.5 us -> 0 us
    all_gather x4 -> x0, waiting for transfers between devices: 160 us -> none  [the longest x2 113 us: side_by_side(): out = lax.all_gather(both, axis, axis=dim, tiled=True)]
    pallas_call x0 -> x1, Pallas kernels: none -> 92.9 us  [on_device(): pl.pallas_call(kernel, out_shape=jax.ShapeDtypeStruct((SEQ, 256), BF16),...]
    reduce_scatter x2 -> x0, waiting for transfers between devices: 66.1 us -> none  [share_cols(): lax.psum_scatter(term.astype(jnp.bfloat16), 'tp', scatter_dimension=1, ti...]
    dot_general x6 -> x0, matrix products: 35.3 us -> none  [the longest x2 20.1 us: project_out(): jnp.dot(active, gather_directly(weight, 'fs', 1), preferred_element_type=...]
    all_to_all x2 -> x0, starting transfers between devices: 15.4 us -> none  [from_everyone(): lax.all_to_all(jnp.broadcast_to(value[None], (devices, *value.shape)), ax...]
    reduce_sum x2 -> x0, other arithmetic: 5.44 us -> none  [rms_rows(): jnp.mean(floats * floats, axis=-1, keepdims=True) + EPS]
    convert_element_type x2 -> x0, other arithmetic: 3.67 us -> none  [the longest x1 1.84 us: on_device(): return (state_cols.astype(jnp.float32) + fed).astype(jnp.bfloat16)]
    broadcast_in_dim x2 -> x0, local copies, waits for them, and re-layouts: 3.31 us -> none  [from_everyone(): jnp.broadcast_to(value[None], (devices, *value.shape))]
  transfers between devices with their start and end apart: 8 -> 0, of which waited for: 6 -> 0; matrix products, arithmetic and copies ran while one was open for 9% -> 0% of each run, Pallas kernels for 0% -> 0%
where the time goes in v3:
time: 94.9 us; the launch traced here: 94.7 us
  Pallas kernels  92.9 us (98%)
  local copies, waits for them, and re-layouts  1.77 us (2%)
    pallas_call x1, Pallas kernels, on_device(): pl.pallas_call(kernel, out_shape=jax.ShapeDtypeStruct((SEQ, 256), BF16),...  92.9 us

profile of v3, /device:TPU:1, one launch (start us, length us, event | category | flops | bytes accessed | tf_op | source)
XLA Modules:
  0.0 94.7 jit_solution(9799602404994040979)
XLA Ops:
  0.0 92.9 %shard_map.136 = bf16[768,256]{1,0:T(8,128)(2,1)} custom-call(bf16[768,256]{1,0:T(8,128)(2,1)} %tokens.1, f32[1,2048]{1,0:T(1,128)} %bitcast.9, bf16[128,256]{1,0:T(8,128)(2,1)} %outer_gate.1, bf16[128,256]{1,0:T(8,128)(2,1)} %inner_gate.1, bf16[128,256]{1,0:T(8,128)(2,1)} %signal_in.1, f32[3,256]{1,0:T(4,128)} %mix_taps.1, f32[1,256]{1,0:T(1,128)} %bitcast.11, ...), custom_call_target="tpu_custom_call" | custom-call | tf_op jit(solution)/shard_map/pallas_call | solution.py:792
  92.9 1.8 %copy.16 = bf16[768,256]{1,0:T(8,128)(2,1)} copy(bf16[768,256]{1,0:T(8,128)(2,1)} %shard_map.136) | data formatting | bytes 786432

commit v4 on v3

--- a/solution.py
+++ b/solution.py
@@ -15,7 +15,7 @@
 R = SEQ // CHUNKS
 PIECES = 3
 Q = SEQ // PIECES
-RECEIVES = 162
+RECEIVES = 120
 GROUPS = 12
 NP, NM, QP, QM, FP0, FM0, FP1, FM1, FP2, FM2, FP3, FM3, GP0, GM1, GP2, GM3 = range(16)
 ROUTE = {
@@ -59,6 +59,13 @@
     ffn_bias,
     down_proj,
     out,
+    mix_gain_v,
+    ffn_gain_v,
+    mix_taps_v,
+    mix_bias_v,
+    ffn_taps_v,
+    ffn_bias_v,
+    scale_s,
     rows,
     rows2,
     normed,
@@ -124,19 +131,26 @@
         copy_of(dst, dst, key, 0, pc).wait_recv()
 
     def all_sent(src, group):
-        copy_of(src, src, (0, 0, NP), group, pc).wait_send()
-
+        copy_of(src, src, (0, NP), group, pc).wait_send()
+
+
+    def part(h, q, depth):
+        if h is None:
+            return 0, depth
+        if q is None:
+            return h * depth // 2, depth // 2
+        return h * depth // 2 + q * depth // 4, depth // 4
 
     def by_rows(buf, lanes, depth):
         def view(g, h, q):
-            start, size = (h * depth // 2, depth // 2) if q is None else (h * depth // 2 + q * depth // 4, depth // 4)
+            start, size = part(h, q, depth)
             return buf.at[pl.ds(at(g * depth + start, depth // 4), size), lanes]
 
         return view
 
     def by_columns(buf, depth):
         def view(g, h, q):
-            start, size = (h * depth // 2, depth // 2) if q is None else (h * depth // 2 + q * depth // 4, depth // 4)
+            start, size = part(h, q, depth)
             return buf.at[pl.ds(start, size), pl.ds(at(g * 128, 128), 128)]
 
         return view
@@ -153,30 +167,25 @@
             g = 4 * near(z, j) + near(x, i) if h == 0 else 4 * near(z, i) + near(x, j)
             return self.view(g, h, q)
 
-        def key(self, h, tag):
-            if ROUTE[tag][4]:
-                return (self.group, 0, -1)
-            return (self.group, h, QP if tag == QM else tag)
-
-        def get(self, h, tag):
-            if (h, tag) not in self.got:
-                self.got.add((h, tag))
-                i, j, _ = ROUTE[tag][1]
-                arrive(self.blk(h, (i, j, None)), self.key(h, tag))
+        def key(self, tag):
+            return (self.group, -1 if ROUTE[tag][4] else QP if tag == QM else tag)
+
+        def get(self, tag):
+            if tag not in self.got:
+                self.got.add(tag)
+                arrive(self.view(f, None, None), self.key(tag))
 
         def put(self, h, tag):
             leaves, _, link, needs, _ = ROUTE[tag]
             for need in needs:
-                self.get(h, need)
+                self.get(need)
             ref = self.blk(h, leaves)
-            i, j, q = leaves
-            send(ref, ref, self.key(h, tag), self.group, LINKS[h][link])
+            send(ref, ref, self.key(tag), self.group, LINKS[h][link])
 
         def end(self):
             for tag in (NP, NM, QP, FP0, FM1, FP2, FM3):
-                for h in (0, 1):
-                    self.get(h, tag)
-            arrive(self.rest, (self.group, 0, -1))
+                self.get(tag)
+            arrive(self.rest, (self.group, -1))
 
     main, second = pl.ds(0, 640), pl.ds(640, 768)
     every = pl.ds(0, 768)
@@ -324,15 +333,25 @@
             (two, tri)[n][r].pair(k)
 
 
-    def norm(src, gain, r):
+    def norm(r):
         def body(i, carry):
             lines = pl.ds(at(r * R + i * 32, 32), 32)
-            v = src[lines, :].astype(F32)
+            v = rows[lines, :].astype(F32)
             mean = jnp.sum(v * v, axis=1, keepdims=True) * (1.0 / D)
-            normed[lines, :] = (v * lax.rsqrt(mean + EPS) * gain[...]).astype(BF16)
+            normed[lines, :] = (v * lax.rsqrt(mean + EPS) * mix_gain_v[...]).astype(BF16)
             return carry
 
         lax.fori_loop(0, R // 32, body, 0)
+
+    def scale(r):
+        def body(i, carry):
+            lines = pl.ds(at(r * R + i * (R // 2), R // 2), R // 2)
+            v = rows2[lines, :].astype(F32)
+            mean = jnp.sum(v * v, axis=1, keepdims=True) * (1.0 / D)
+            scale_s[lines, :] = lax.rsqrt(mean + EPS)
+            return carry
+
+        lax.fori_loop(0, 2, body, 0)
 
     def project(r):
         lines, here = pl.ds(r * R, R), pl.ds(8 + r * R, R)
@@ -341,19 +360,19 @@
         signal = jnp.dot(normed[lines, :], projw[:, 512:768], preferred_element_type=F32)
         mi[here, :] = mi[here, :] * signal
         conv = (
-            mix_taps[2:3, :] * mi[here, :]
-            + mix_taps[1:2, :] * mi[pl.ds(7 + r * R, R), :]
-            + mix_taps[0:1, :] * mi[pl.ds(6 + r * R, R), :]
-            + mix_bias[...]
+            mix_taps_v[2:3, :] * mi[here, :]
+            + mix_taps_v[1:2, :] * mi[pl.ds(7 + r * R, R), :]
+            + mix_taps_v[0:1, :] * mi[pl.ds(6 + r * R, R), :]
+            + mix_bias_v[...]
         )
         gated[r] = (outer_s[...] * conv).astype(BF16)
 
     def expand(r):
+        lines = pl.ds(r * R, R)
         for n in range(6):
             width = 256 if n < 5 else 128
-            pre[pl.ds(8 + r * R, R), pl.ds(n * 256, width)] = jnp.dot(
-                normed[pl.ds(r * R, R), :], upw[:, n * 256 : n * 256 + width], preferred_element_type=F32
-            )
+            term = jnp.dot(rows2[lines, :], upw[:, n * 256 : n * 256 + width], preferred_element_type=F32)
+            pre[pl.ds(8 + r * R, R), pl.ds(n * 256, width)] = term * scale_s[lines, :]
 
     def conv_cols(r, col, which, j):
         lanes = pl.ds(col, 128)
@@ -392,6 +411,12 @@
         (up_gate, gstage),
         (up_value, vstage),
         (down_proj, dstage),
+        (mix_gain, mix_gain_v),
+        (ffn_gain, ffn_gain_v),
+        (mix_taps, mix_taps_v),
+        (mix_bias, mix_bias_v),
+        (ffn_taps, ffn_taps_v),
+        (ffn_bias, ffn_bias_v),
     ]
     local = [pltpu.make_async_copy(src, dst, local_sem.at[i]) for i, (src, dst) in enumerate(moves)]
     for copy in local:
@@ -405,13 +430,28 @@
         for copy in local[lo:hi]:
             copy.wait()
 
+    def small():
+        place(8, 14)
+        taps_s[...] = jnp.zeros((8, 768), F32)
+        for which in (0, 1):
+            for k in range(3):
+                taps_s[4 * which + k : 4 * which + k + 1, 0:704] = ffn_taps_v[k, which : which + 1]
+            taps_s[4 * which + 3 : 4 * which + 4, 0:704] = ffn_bias_v[which : which + 1]
+        taps_s[4:8, 640:768] = pltpu.roll(taps_s[4:8, 640:768], 64, 1)
+
     def lay_up():
+        small()
         place(5, 7)
+        gain = ffn_gain_v[:, own_rows]
+
+        def gained(block):
+            return (block.astype(F32) * gain).astype(BF16).T
+
         for j in range(5):
             lanes = pl.ds(128 * j, 128)
-            upw[own_rows, lanes] = gstage[lanes, :].T
-            upw[own_rows, pl.ds(640 + 128 * j, 128)] = vstage[lanes, :].T
-        upw[own_rows, 1280:1408] = jnp.concatenate([gstage[640:704, :], vstage[640:704, :]], axis=0).T
+            upw[own_rows, lanes] = gained(gstage[lanes, :])
+            upw[own_rows, pl.ds(640 + 128 * j, 128)] = gained(vstage[lanes, :])
+        upw[own_rows, 1280:1408] = gained(jnp.concatenate([gstage[640:704, :], vstage[640:704, :]], axis=0))
 
     def lay_down():
         place(7, 8)
@@ -440,304 +480,298 @@
 
     mi[0:8, :] = jnp.zeros((8, 256), F32)
     pre[0:8, :] = jnp.zeros((8, 1408), F32)
-    taps_s[...] = jnp.zeros((8, 768), F32)
-    for which in (0, 1):
-        for k in range(3):
-            taps_s[4 * which + k : 4 * which + k + 1, 0:704] = ffn_taps[k, which : which + 1]
-        taps_s[4 * which + 3 : 4 * which + 4, 0:704] = ffn_bias[which : which + 1]
-    taps_s[4:8, 640:768] = pltpu.roll(taps_s[4:8, 640:768], 64, 1)
     pl.semaphore_wait(barrier, 7)
 
     place(0, 1)
     place(1, 4)
+    gp.put(0, NP)
+    gp.put(1, NP)
+    gp.put(0, NM)
+    gp.put(1, NM)
     tok[0].own()
     tok[1].own()
     tok[2].own()
     tok[3].own()
     place(4, 5)
+    lay_up()
+    lay_down()
+    gm.put(0, NP)
+    gm.put(1, NP)
     gm.put(0, NM)
     gm.put(1, NM)
-    gm.put(0, NP)
-    gm.put(1, NP)
-    gp.put(0, NM)
-    gp.put(1, NM)
-    gp.put(0, NP)
-    gp.put(1, NP)
-    lay_up()
-    lay_down()
+    gm.put(1, FP0)
+    gm.put(0, FP0)
     gm.put(1, FM0)
     gm.put(0, FM0)
-    gm.put(1, FP0)
-    gm.put(0, FP0)
+    gp.put(1, FP0)
+    gp.put(0, FP0)
     gp.put(1, FM0)
     gp.put(0, FM0)
-    gp.put(1, FP0)
-    gp.put(0, FP0)
     tok[0].fp()
     tok[0].fm()
+    gp.put(0, QP)
+    gp.put(1, QP)
+    gp.put(0, QM)
+    gp.put(1, QM)
+    gm.put(1, FP2)
+    gm.put(0, FP2)
     gm.put(0, QM)
     gm.put(1, QM)
+    gm.put(1, FM1)
+    gm.put(0, FM1)
+    tok[1].fp()
+    tok[1].fm()
     gm.put(0, QP)
     gm.put(1, QP)
-    gp.put(0, QM)
-    gp.put(1, QM)
-    gp.put(0, QP)
-    gp.put(1, QP)
-    gm.put(1, FM1)
-    gm.put(0, FM1)
+    gp.put(1, FP2)
+    gp.put(0, FP2)
+    gp.put(1, FM1)
+    gp.put(0, FM1)
+    tok[2].fp()
+    tok[2].fm()
     gm.put(1, FP1)
     gm.put(0, FP1)
-    tok[1].fp()
-    tok[1].fm()
-    gp.put(1, FM1)
-    gp.put(0, FM1)
-    gp.put(1, FP1)
-    gp.put(0, FP1)
-    tok[2].fp()
-    tok[2].fm()
-    gm.put(1, FM2)
-    gm.put(0, FM2)
-    gm.put(1, FP3)
-    gm.put(0, FP3)
-    gp.put(1, FM2)
-    gp.put(0, FM2)
+    gp.put(1, FM3)
+    gp.put(0, FM3)
     gp.put(1, FP3)
     gp.put(0, FP3)
     tok[3].fp()
     tok[3].fm()
+    gm.put(1, FM3)
+    gm.put(0, FM3)
     tok[0].xp()
     tok[0].xm()
-    gm.put(1, FM3)
-    gm.put(0, FM3)
-    gm.put(1, FP2)
-    gm.put(0, FP2)
-    gp.put(1, FM3)
-    gp.put(0, FM3)
-    gp.put(1, FP2)
-    gp.put(0, FP2)
-    tok[1].xp()
-    tok[1].xm()
-    tok[0].end()
-    norm(rows, mix_gain, 0)
-    tok[2].xp()
-    tok[2].xm()
-    tok[1].end()
-    norm(rows, mix_gain, 1)
+    gm.put(1, FP3)
+    gm.put(0, FP3)
     gm.put(1, GM1)
     gm.put(0, GM1)
     gm.put(1, GP0)
     gm.put(0, GP0)
+    gp.put(1, FM2)
+    gp.put(0, FM2)
+    tok[1].xp()
+    tok[1].xm()
+    gp.put(1, FP1)
+    gp.put(0, FP1)
+    tok[0].end()
+    norm(0)
+    tok[2].xp()
+    tok[2].xm()
+    tok[1].end()
+    norm(1)
+    gp.put(0, GM3)
+    gp.put(1, GM3)
     tok[3].xp()
     tok[3].xm()
-    tok[2].end()
-    norm(rows, mix_gain, 2)
-    gm.put(1, GM3)
-    gm.put(0, GM3)
     gm.put(1, GP2)
     gm.put(0, GP2)
+    tok[2].end()
+    norm(2)
+    gp.put(0, GP2)
+    gp.put(1, GP2)
+    tok[3].end()
+    gm.put(0, GM3)
+    gm.put(1, GM3)
+    norm(3)
+    gm.put(0, FM2)
+    gm.put(1, FM2)
+    gp.put(1, GP0)
+    gp.put(0, GP0)
     gp.put(1, GM1)
     gp.put(0, GM1)
-    gp.put(1, GP0)
-    gp.put(0, GP0)
-    tok[3].end()
-    norm(rows, mix_gain, 3)
-    gp.put(1, GM3)
-    gp.put(0, GM3)
-    gp.put(1, GP2)
-    gp.put(0, GP2)
-    gm.end()
+    gu.put(0, NP)
+    gu.put(1, NP)
     gu.put(0, NM)
     gu.put(1, NM)
-    gu.put(0, NP)
-    gu.put(1, NP)
-    gu.put(1, FM0)
-    gu.put(0, FM0)
+    gm.end()
+    gd.put(0, NP)
+    gd.put(1, NP)
+    gv.put(0, NM)
+    gv.put(1, NM)
     gu.put(1, FP0)
     gu.put(0, FP0)
     gp.end()
     project(0)
-    gv.put(0, NM)
-    gv.put(1, NM)
+    gu.put(0, FM0)
+    gu.put(1, FM0)
+    mix_terms(0)
+    gu.put(0, FP2)
+    gu.put(1, FP2)
+    project(1)
+    gu.put(0, FM1)
+    gu.put(1, FM1)
+    gu.put(0, QP)
+    gu.put(1, QP)
+    mix_terms(1)
+    gu.put(0, QM)
+    gu.put(1, QM)
     gv.put(0, NP)
     gv.put(1, NP)
-    mix_terms(0)
-    project(1)
-    gu.put(0, QP)
-    gu.put(1, QP)
-    gu.put(0, QM)
-    gu.put(1, QM)
-    mix_terms(1)
     pairs(0)
-    gu.put(0, FM1)
-    gu.put(1, FM1)
+    project(2)
+    gv.put(0, FM2)
+    gv.put(1, FM2)
+    mix_terms(2)
+    pairs(1)
+    gv.put(0, FP2)
+    gv.put(1, FP2)
+    project(3)
+    gu.put(0, FM2)
+    gu.put(1, FM2)
+    one[0].pass_on()
+    mix_terms(3)
+    pairs(2)
+    gu.put(0, FM3)
+    gu.put(1, FM3)
+    gu.put(0, FP3)
+    gu.put(1, FP3)
+    one[1].pass_on()
+    gv.put(0, QP)
+    gv.put(1, QP)
+    gv.put(1, FM1)
+    gv.put(0, FM1)
+    gu.put(0, GP0)
+    gu.put(1, GP0)
+    pairs(3)
+    hidden(0)
+    hid[0].own()
+    gv.put(0, QM)
+    gv.put(1, QM)
+    gu.put(0, GP2)
+    gu.put(1, GP2)
+    one[2].pass_on()
+    gu.put(1, GM3)
+    gu.put(0, GM3)
     gu.put(0, FP1)
     gu.put(1, FP1)
-    project(2)
-    gu.put(0, FM2)
-    gu.put(1, FM2)
-    gu.put(0, FP2)
-    gu.put(1, FP2)
-    mix_terms(2)
-    pairs(1)
-    project(3)
-    gu.put(0, FP3)
-    gu.put(1, FP3)
-    gu.put(0, FM3)
-    gu.put(1, FM3)
-    mix_terms(3)
-    one[0].pass_on()
-    pairs(2)
-    gv.put(0, QP)
-    gv.put(1, QP)
-    gu.put(0, GM1)
-    gu.put(1, GM1)
-    gu.put(0, GP0)
-    gu.put(1, GP0)
-    one[1].pass_on()
-    pairs(3)
-    gv.put(0, QM)
-    gv.put(1, QM)
-    gv.put(0, FM1)
-    gv.put(1, FM1)
-    gu.put(0, GP2)
-    gu.put(1, GP2)
-    hidden(0)
-    hid[0].own()
-    one[2].pass_on()
+    hidden(1)
+    hid[1].own()
+    gd.put(0, NM)
+    gd.put(1, NM)
+    one[3].pass_on()
     gv.put(0, FP1)
     gv.put(1, FP1)
-    gu.put(0, GM3)
-    gu.put(1, GM3)
-    hidden(1)
-    hid[1].own()
-    gv.put(0, FM0)
-    gv.put(1, FM0)
+    gv.put(1, GM1)
+    gv.put(0, GM1)
+    gv.put(0, FP0)
+    gv.put(1, FP0)
+    gv.put(1, FM3)
+    gv.put(0, FM3)
+    hid[0].fp()
+    hid[0].fm()
+    hidden(2)
+    hid[2].own()
     gv.put(0, FP3)
     gv.put(1, FP3)
-    one[3].pass_on()
-    gv.put(0, FM2)
-    gv.put(1, FM2)
-    gv.put(0, FP0)
-    gv.put(1, FP0)
-    gu.end()
-    hid[0].fp()
-    hid[0].fm()
-    gv.put(0, FM3)
-    gv.put(1, FM3)
-    gv.put(0, FP2)
-    gv.put(1, FP2)
-    hidden(2)
-    hid[2].own()
-    gd.put(1, NM)
-    gd.put(0, NM)
-    gd.put(1, NP)
-    gd.put(0, NP)
+    gv.put(1, FM0)
+    gv.put(0, FM0)
     hid[1].fp()
     hid[1].fm()
-    gv.put(0, GM1)
-    gv.put(1, GM1)
+    gv.put(0, GP2)
+    gv.put(1, GP2)
+    gu.put(1, GM1)
+    gu.put(0, GM1)
+    hidden(3)
+    hid[3].own()
+    gv.put(1, GM3)
+    gv.put(0, GM3)
+    hid[0].xp()
+    hid[0].xm()
     gv.put(0, GP0)
     gv.put(1, GP0)
-    hidden(3)
-    hid[3].own()
-    hid[0].xp()
-    hid[0].xm()
-    gv.put(0, GM3)
-    gv.put(1, GM3)
-    gv.put(0, GP2)
-    gv.put(1, GP2)
     hid[0].end()
-    norm(rows2, ffn_gain, 0)
+    scale(0)
+    gd.put(1, FM1)
+    gd.put(0, FM1)
     hid[2].fp()
     hid[2].fm()
-    gd.put(1, QM)
-    gd.put(0, QM)
     gd.put(1, QP)
     gd.put(0, QP)
-    gd.put(0, FM1)
-    gd.put(1, FM1)
     gd.put(0, FP1)
     gd.put(1, FP1)
+    gu.end()
+    gd.put(0, QM)
+    gd.put(1, QM)
     hid[1].xp()
     hid[1].xm()
-    gd.put(0, FM0)
-    gd.put(1, FM0)
-    gd.put(0, FP0)
-    gd.put(1, FP0)
-    hid[1].end()
-    norm(rows2, ffn_gain, 1)
+    ge.put(0, NM)
+    ge.put(1, NM)
+    gd.put(0, FP2)
+    gd.put(1, FP2)
     gd.put(1, FM2)
     gd.put(0, FM2)
-    gd.put(1, FP2)
-    gd.put(0, FP2)
+    hid[1].end()
+    scale(1)
+    ge.put(0, NP)
+    ge.put(1, NP)
+    gv.end()
     hid[3].fp()
     hid[3].fm()
-    gv.end()
     expand(0)
     hid[2].xp()
     hid[2].xm()
+    gd.put(0, FM3)
+    gd.put(1, FM3)
+    gd.put(0, FP3)
     gd.put(1, FP3)
-    gd.put(0, FP3)
-    gd.put(1, FM3)
-    gd.put(0, FM3)
     activate(0)
-    ge.put(0, NM)
-    ge.put(1, NM)
-    ge.put(0, NP)
-    ge.put(1, NP)
+    gd.put(0, GM1)
+    gd.put(1, GM1)
+    gd.put(0, FP0)
+    gd.put(1, FP0)
     expand(1)
     hid[3].xp()
     hid[3].xm()
     hid[2].end()
-    gd.put(0, GM1)
-    gd.put(1, GM1)
+    ge.put(0, FM1)
+    ge.put(1, FM1)
+    ge.put(0, QP)
+    ge.put(1, QP)
+    ge.put(0, FP2)
+    ge.put(1, QM)
+    ge.put(0, QM)
+    ge.put(1, FP2)
+    activate(1)
+    gd.put(0, FM0)
+    gd.put(1, FM0)
+    gd.put(0, GP2)
+    gd.put(1, GP2)
+    scale(2)
+    expand(2)
+    hid[3].end()
+    gd.put(0, GM3)
+    gd.put(1, GM3)
     gd.put(0, GP0)
     gd.put(1, GP0)
-    activate(1)
-    gd.put(1, GP2)
-    gd.put(0, GP2)
-    ge.put(0, FM0)
-    ge.put(1, FM0)
-    norm(rows2, ffn_gain, 2)
-    hid[3].end()
-    gd.put(1, GM3)
-    gd.put(0, GM3)
-    ge.put(0, FP0)
-    ge.put(1, FP0)
-    norm(rows2, ffn_gain, 3)
-    ge.put(0, QP)
-    ge.put(1, QP)
-    ge.put(0, QM)
-    ge.put(1, QM)
-    expand(2)
-    ge.put(0, FM1)
-    ge.put(1, FM1)
+    activate(2)
     ge.put(0, FP1)
     ge.put(1, FP1)
     ge.put(0, FM2)
     ge.put(1, FM2)
-    ge.put(0, FP2)
-    ge.put(1, FP2)
-    activate(2)
+    scale(3)
     expand(3)
-    ge.put(1, FP3)
-    ge.put(0, FP3)
     ge.put(0, FM3)
     ge.put(1, FM3)
-    ge.put(1, GP0)
-    ge.put(0, GP0)
+    ge.put(0, FP0)
+    ge.put(1, FP0)
     activate(3)
+    ge.put(0, GM1)
+    ge.put(1, GM1)
+    ge.put(0, GP2)
+    ge.put(1, GP2)
+    ge.put(0, FM0)
+    ge.put(1, FM0)
+    ge.put(0, FP3)
+    ge.put(1, FP3)
     gd.end()
     down_terms(0, 0)
-    ge.put(0, GM1)
-    ge.put(1, GM1)
     down_terms(0, 1)
-    ge.put(0, GP2)
-    ge.put(1, GP2)
     down_terms(0, 2)
     pair_all(0, 0)
     ge.put(0, GM3)
     ge.put(1, GM3)
+    ge.put(0, GP0)
+    ge.put(1, GP0)
     down_terms(0, 3)
     pair_all(0, 1)
     pair_all(0, 2)
@@ -791,10 +825,17 @@
     vmem = pl.BlockSpec(memory_space=pltpu.VMEM)
     return pl.pallas_call(
         kernel,
-        out_shape=jax.ShapeDtypeStruct((SEQ, 256), BF16),
-        in_specs=[hbm, vmem, hbm, hbm, hbm, vmem, vmem, hbm, vmem, hbm, hbm, vmem, vmem, hbm],
+        out_shape=pltpu.VMEM((SEQ, 256), BF16),
+        in_specs=[hbm] * 14,
         out_specs=vmem,
         scratch_shapes=[
+            pltpu.VMEM((1, D), F32),
+            pltpu.VMEM((1, D), F32),
+            pltpu.VMEM((3, 256), F32),
+            pltpu.VMEM((1, 256), F32),
+            pltpu.VMEM((3, 2, 704), F32),
+            pltpu.VMEM((2, 704), F32),
+            pltpu.VMEM((SEQ, 1), F32),
             pltpu.VMEM((SEQ, D), BF16),
             pltpu.VMEM((SEQ, D), BF16),
             pltpu.VMEM((SEQ, D), BF16),
@@ -826,7 +867,7 @@
             pltpu.VMEM((2, PIECES, 2, Q, 128), BF16),
             pltpu.SemaphoreType.DMA((GROUPS,)),
             pltpu.SemaphoreType.DMA((RECEIVES,)),
-            pltpu.SemaphoreType.DMA((8,)),
+            pltpu.SemaphoreType.DMA((14,)),
         ],
         compiler_params=pltpu.CompilerParams(
             collective_id=0, has_side_effects=True, vmem_limit_bytes=56 * 1024 * 1024

time: 94.9 us -> 91.4 us (0.963)
  Pallas kernels: 92.9 us -> 90.6 us
  local copies, waits for them, and re-layouts: 1.77 us -> 0.75 us
    pallas_call x1, Pallas kernels: 92.9 us -> 90.6 us  [on_device(): pl.pallas_call(kernel, out_shape=pltpu.VMEM((SEQ, 256), BF16), in_specs=[...]
    unnamed x1, local copies, waits for them, and re-layouts: 1.77 us -> 0.75 us
where the time goes in v4:
time: 91.4 us; the launch traced here: 91.3 us
  Pallas kernels  90.6 us (99%)
    pallas_call x1, Pallas kernels, on_device(): pl.pallas_call(kernel, out_shape=pltpu.VMEM((SEQ, 256), BF16), in_specs=[...  90.6 us

profile of v4, /device:TPU:1, one launch (start us, length us, event | category | flops | bytes accessed | tf_op | source)
XLA Modules:
  0.0 91.3 jit_solution(15786539968405447339)
XLA Ops:
  0.0 90.6 %shard_map.136 = bf16[768,256]{1,0:T(8,128)(2,1)S(1)} custom-call(bf16[768,256]{1,0:T(8,128)(2,1)} %tokens.1, f32[1,2048]{1,0:T(1,128)} %bitcast.9, bf16[128,256]{1,0:T(8,128)(2,1)} %outer_gate.1, bf16[128,256]{1,0:T(8,128)(2,1)} %inner_gate.1, bf16[128,256]{1,0:T(8,128)(2,1)} %signal_in.1, f32[3,256]{1,0:T(4,128)} %mix_taps.1, f32[1,256]{1,0:T(1,128)} %bitcast.11, ...), custom_call_target="tpu_custom_call" | custom-call | tf_op jit(solution)/shard_map/pallas_call | solution.py:826
  90.6 0.7 copy.16

commit v5 on v4

--- a/solution.py
+++ b/solution.py
@@ -15,27 +15,29 @@
 R = SEQ // CHUNKS
 PIECES = 3
 Q = SEQ // PIECES
-RECEIVES = 120
+RECEIVES = 116
 GROUPS = 12
 NP, NM, QP, QM, FP0, FM0, FP1, FM1, FP2, FM2, FP3, FM3, GP0, GM1, GP2, GM3 = range(16)
 ROUTE = {
-    NP: ((0, 0, None), (-1, 0, None), 0, (), False),
-    NM: ((0, 0, None), (1, 0, None), 1, (), False),
-    QP: ((-1, 0, 0), (2, 0, 0), 0, (NP,), False),
-    QM: ((1, 0, 1), (2, 0, 1), 1, (NM,), False),
-    FP0: ((0, 0, None), (0, -1, None), 2, (), False),
-    FM0: ((0, 0, None), (0, 1, None), 3, (), True),
-    FP1: ((-1, 0, None), (-1, -1, None), 2, (NP,), True),
-    FM1: ((-1, 0, None), (-1, 1, None), 3, (NP,), False),
-    FP2: ((1, 0, None), (1, -1, None), 2, (NM,), False),
-    FM2: ((1, 0, None), (1, 1, None), 3, (NM,), True),
-    FP3: ((2, 0, None), (2, -1, None), 2, (QP,), True),
-    FM3: ((2, 0, None), (2, 1, None), 3, (QP,), False),
-    GP0: ((0, -1, None), (0, 2, None), 2, (FP0,), True),
-    GM1: ((-1, 1, None), (-1, 2, None), 3, (FM1,), True),
-    GP2: ((1, -1, None), (1, 2, None), 2, (FP2,), True),
-    GM3: ((2, 1, None), (2, 2, None), 3, (FM3,), True),
+    NP: ((0, 0, None), 0, None),
+    NM: ((0, 0, None), 1, None),
+    QP: ((-1, 0, 0), 0, NP),
+    QM: ((1, 0, 1), 1, NM),
+    FP0: ((0, 0, None), 2, None),
+    FM0: ((0, 0, None), 3, None),
+    FP1: ((-1, 0, None), 2, NP),
+    FM1: ((-1, 0, None), 3, NP),
+    FP2: ((1, 0, None), 2, NM),
+    FM2: ((1, 0, None), 3, NM),
+    FP3: ((2, 0, None), 2, QP),
+    FM3: ((2, 0, None), 3, QP),
+    GP0: ((0, -1, None), 2, FP0),
+    GM1: ((-1, 1, None), 3, FM1),
+    GP2: ((1, -1, None), 2, FP2),
+    GM3: ((2, 1, None), 3, FM3),
 }
+WAITED = (NP, NM, QP, FP0, FM1, FP2, FM3)
+REST = -1
 ORDER = (2, 1, 3, 0)
 
 
@@ -135,8 +137,6 @@
 
 
     def part(h, q, depth):
-        if h is None:
-            return 0, depth
         if q is None:
             return h * depth // 2, depth // 2
         return h * depth // 2 + q * depth // 4, depth // 4
@@ -158,88 +158,88 @@
     LINKS = ((xp, xm, zp, zm), (zp, zm, xp, xm))
 
     class Gather:
-        def __init__(self, group, view, sent, rest):
-            self.group, self.view, self.got = group, view, set()
-            self.sent, self.rest = sent, rest
-
-        def blk(self, h, where):
-            i, j, q = where
+        def __init__(self, group, view, blocks):
+            self.group, self.view, self.blocks, self.got = group, view, blocks, set()
+
+        def get(self, key):
+            if key is not None and key not in self.got:
+                self.got.add(key)
+                arrive(self.blocks(1), (self.group, key))
+
+        def put(self, h, tag):
+            (i, j, q), link, needs = ROUTE[tag]
+            self.get(needs)
             g = 4 * near(z, j) + near(x, i) if h == 0 else 4 * near(z, i) + near(x, j)
-            return self.view(g, h, q)
-
-        def key(self, tag):
-            return (self.group, -1 if ROUTE[tag][4] else QP if tag == QM else tag)
-
-        def get(self, tag):
-            if tag not in self.got:
-                self.got.add(tag)
-                arrive(self.view(f, None, None), self.key(tag))
-
-        def put(self, h, tag):
-            leaves, _, link, needs, _ = ROUTE[tag]
-            for need in needs:
-                self.get(need)
-            ref = self.blk(h, leaves)
-            send(ref, ref, self.key(tag), self.group, LINKS[h][link])
+            ref = self.view(g, h, q)
+            key = QP if tag == QM else tag
+            send(ref, ref, (self.group, key if key in WAITED else REST), self.group, LINKS[h][link])
 
         def end(self):
-            for tag in (NP, NM, QP, FP0, FM1, FP2, FM3):
-                self.get(tag)
-            arrive(self.rest, (self.group, -1))
+            for key in WAITED:
+                self.get(key)
+            arrive(self.blocks(8), (self.group, REST))
+
+        def sent(self):
+            all_sent(self.blocks(15), self.group)
 
     main, second = pl.ds(0, 640), pl.ds(640, 768)
     every = pl.ds(0, 768)
-    gp = Gather(0, by_rows(projw, every, 128), projw.at[pl.ds(0, 1920), :], projw.at[pl.ds(0, 1024), :])
-    gm = Gather(1, by_columns(mixw, 256), mixw.at[:, pl.ds(0, 1920)], mixw.at[:, pl.ds(0, 1024)])
-    gu = Gather(2, by_rows(upw, main, 128), upw.at[pl.ds(0, 1920), main], upw.at[pl.ds(0, 1024), main])
-    gv = Gather(3, by_rows(upw, second, 128), upw.at[pl.ds(0, 1920), second], upw.at[pl.ds(0, 1024), second])
-    gd = Gather(4, by_rows(downw, every, 64), downw.at[pl.ds(0, 960), :], downw.at[pl.ds(0, 512), :])
-    ge = Gather(5, by_rows(downw2, main, 64), downw2.at[pl.ds(0, 960), :], downw2.at[pl.ds(0, 512), :])
+    gp = Gather(0, by_rows(projw, every, 128), lambda n: projw.at[pl.ds(0, 128 * n), :])
+    gm = Gather(1, by_columns(mixw, 256), lambda n: mixw.at[:, pl.ds(0, 128 * n)])
+    gu = Gather(2, by_rows(upw, main, 128), lambda n: upw.at[pl.ds(0, 128 * n), main])
+    gv = Gather(3, by_rows(upw, second, 128), lambda n: upw.at[pl.ds(0, 128 * n), second])
+    gd = Gather(4, by_rows(downw, every, 64), lambda n: downw.at[pl.ds(0, 64 * n), :])
+    ge = Gather(5, by_rows(downw2, main, 64), lambda n: downw2.at[pl.ds(0, 64 * n), :])
 
 
     class Rows:
         def __init__(self, group, buf, r):
-            self.group, self.buf, self.r = group, buf, r
-
-        def view(self, dy, half=None):
+            self.group, self.buf, self.r, self.got = group, buf, r, set()
+
+        def put(self, dy, key, dev, half=None):
             start, size = self.r * R, R
             if half is not None:
                 size = size // 2
                 start = start + half * size
-            return self.buf.at[pl.ds(start, size), pl.ds(at(256 * (2 * near(y, dy) + c), 256), 256)]
-
-        def put(self, dy, tag, dev, half=None):
-            ref = self.view(dy, half)
-            send(ref, ref, (self.group, self.r, tag), self.group, dev)
-
-        def get(self, dy, tag, half=None):
-            arrive(self.view(dy, half), (self.group, self.r, tag))
-
-        def own(self):
+            ref = self.buf.at[pl.ds(start, size), pl.ds(at(256 * (2 * near(y, dy) + c), 256), 256)]
+            send(ref, ref, (self.group, self.r, key), self.group, dev)
+
+        def get(self, key, blocks=1):
+            if key not in self.got:
+                self.got.add(key)
+                arrive(self.buf.at[pl.ds(self.r * R, R), pl.ds(0, 256 * blocks)], (self.group, self.r, key))
+
+        def own_p(self):
             self.put(0, 0, yp)
+
+        def own_m(self):
             self.put(0, 1, ym)
-            self.put(0, 4, pc)
-
-        def fp(self):
-            self.get(-1, 0)
+
+        def own_c(self):
+            self.put(0, 3, pc)
+
+        def on_p(self):
+            self.get(0)
             self.put(-1, 2, yp, 0)
-            self.put(-1, 4, pc)
-
-        def fm(self):
-            self.get(1, 1)
-            self.put(1, 3, ym, 1)
-            self.put(1, 4, pc)
-
-        def xp(self):
-            self.get(2, 2, 0)
-            self.put(2, 4, pc, 0)
-
-        def xm(self):
-            self.get(2, 3, 1)
-            self.put(2, 4, pc, 1)
+
+        def on_m(self):
+            self.get(1)
+            self.put(1, 2, ym, 1)
+
+        def on_cp(self):
+            self.get(0)
+            self.put(-1, 3, pc)
+
+        def on_cm(self):
+            self.get(1)
+            self.put(1, 3, pc)
+
+        def far_c(self):
+            self.get(2)
+            self.put(2, 3, pc)
 
         def end(self):
-            arrive(self.buf.at[pl.ds(self.r * R, R), pl.ds(0, 1024)], (self.group, self.r, 4))
+            self.get(3, 4)
 
     tok = [Rows(6, rows, r) for r in range(CHUNKS)]
     hid = [Rows(7, rows2, r) for r in range(CHUNKS)]
@@ -252,35 +252,48 @@
 
         def pair(self, k):
             n, half = self.size, self.size // 2
-            mine = pl.ds(self.start, n)
-            total = self.keep[k, mine] + self.mine[k, mine].astype(F32)
-            key, keys = (self.group, self.r, 2), (self.group, self.r, 3)
+            lines = pl.ds(self.start, n)
+            total = self.keep[k, lines] + self.mine[k, lines].astype(F32)
             if k == 0:
                 self.leave[0] = total.astype(BF16)
-                send(self.leave.at[0, pl.ds(0, half)], self.mid.at[0], key, self.group, yp)
-                send(self.leave.at[0, pl.ds(half, half)], self.mid.at[1], key, self.group, ym)
             elif k == 1:
                 self.leave[1, half:] = total[half:].astype(BF16)
-                part = pl.ds(half, half)
-                send(self.leave.at[1, part], self.fin.at[0, part], keys, self.group, yp)
                 self.keep[k, pl.ds(self.start, half)] = total[:half]
             elif k == 2:
                 self.leave[2, :half] = total[:half].astype(BF16)
-                part = pl.ds(0, half)
-                send(self.leave.at[2, part], self.fin.at[1, part], keys, self.group, ym)
                 self.keep[k, pl.ds(self.start + half, half)] = total[half:]
             else:
-                self.keep[k, mine] = total
+                self.keep[k, lines] = total
+
+        def go(self, k, half, dst, key, dev):
+            send(self.leave.at[k, half], dst, (self.group, self.r, key), self.group, dev)
+
+        def halves(self):
+            half = self.size // 2
+            return pl.ds(0, half), pl.ds(half, half)
+
+        def dp(self):
+            self.go(0, self.halves()[0], self.mid.at[0], 2, yp)
+
+        def dm(self):
+            self.go(0, self.halves()[1], self.mid.at[1], 2, ym)
+
+        def ep(self):
+            high = self.halves()[1]
+            self.go(1, high, self.fin.at[0, high], 3, yp)
+
+        def em(self):
+            low = self.halves()[0]
+            self.go(2, low, self.fin.at[1, low], 3, ym)
 
         def pass_on(self):
             half = self.size // 2
-            low, high = pl.ds(0, half), pl.ds(half, half)
-            keys = (self.group, self.r, 3)
+            low, high = self.halves()
             arrive(self.mid, (self.group, self.r, 2))
             self.leave[1, low] = (self.keep[1, pl.ds(self.start, half)] + self.mid[0].astype(F32)).astype(BF16)
-            send(self.leave.at[1, low], self.fin.at[0, low], keys, self.group, yp)
+            self.go(1, low, self.fin.at[0, low], 3, yp)
             self.leave[2, high] = (self.keep[2, pl.ds(self.start + half, half)] + self.mid[1].astype(F32)).astype(BF16)
-            send(self.leave.at[2, high], self.fin.at[1, high], keys, self.group, ym)
+            self.go(2, high, self.fin.at[1, high], 3, ym)
 
         def total(self):
             arrive(self.fin, (self.group, self.r, 3))
@@ -316,19 +329,25 @@
     def across(a, b):
         return lax.dot_general(a, b, (((1,), (1,)), ((), ())), preferred_element_type=F32)
 
-    def down_terms(n, k):
+    def down_terms(n, k, r):
         lines = pl.ds(at(256 * near(y, ORDER[k]), 256), 256)
+        here = pl.ds(r * Q, Q)
         if n == 0:
-            term = across(act[:, 0:768], downw[lines, :])
+            term = across(act[here, 0:768], downw[lines, :])
         else:
-            term = across(act[:, 0:640], downw2[lines, :]) + across(act[:, 768:896], downw[lines, 640:768])
+            term = across(act[here, 0:640], downw2[lines, :]) + across(act[here, 768:896], downw[lines, 640:768])
         low, high = term[:, 0:128], term[:, 128:256]
-        psend2[n, k] = jnp.where(c == 0, high, low).astype(BF16)
-        send(psend2.at[n, k], precv2.at[n, k], (10, n, k), 10, pc)
-        keep2[n, k] = jnp.where(c == 0, low, high)
+        psend2[n, k, here] = jnp.where(c == 0, high, low).astype(BF16)
+        send(psend2.at[n, k, here], precv2.at[n, k, here], (10, n, k, r if k == 0 else PIECES), 10, pc)
+        keep2[n, k, here] = jnp.where(c == 0, low, high)
+
+    def pair_first(n, r):
+        here = pl.ds(r * Q, Q)
+        arrive(precv2.at[n, 0, here], (10, n, 0, r))
+        (two, tri)[n][r].pair(0)
 
     def pair_all(n, k):
-        arrive(precv2.at[n, k], (10, n, k))
+        arrive(precv2.at[n, k], (10, n, k, PIECES))
         for r in range(PIECES):
             (two, tri)[n][r].pair(k)
 
@@ -367,12 +386,13 @@
         )
         gated[r] = (outer_s[...] * conv).astype(BF16)
 
-    def expand(r):
+    def expand(r, first, last):
         lines = pl.ds(r * R, R)
-        for n in range(6):
-            width = 256 if n < 5 else 128
-            term = jnp.dot(rows2[lines, :], upw[:, n * 256 : n * 256 + width], preferred_element_type=F32)
-            pre[pl.ds(8 + r * R, R), pl.ds(n * 256, width)] = term * scale_s[lines, :]
+        while first < last:
+            width = min(256, last - first)
+            term = jnp.dot(rows2[lines, :], upw[:, first : first + width], preferred_element_type=F32)
+            pre[pl.ds(8 + r * R, R), pl.ds(first, width)] = term * scale_s[lines, :]
+            first += width
 
     def conv_cols(r, col, which, j):
         lanes = pl.ds(col, 128)
@@ -482,320 +502,408 @@
     pre[0:8, :] = jnp.zeros((8, 1408), F32)
     pl.semaphore_wait(barrier, 7)
 
+    place(1, 4)
+    gp.put(1, NM)
+    gp.put(0, NM)
+    gp.put(1, NP)
+    gp.put(0, NP)
+    place(4, 5)
     place(0, 1)
-    place(1, 4)
-    gp.put(0, NP)
-    gp.put(1, NP)
-    gp.put(0, NM)
-    gp.put(1, NM)
-    tok[0].own()
-    tok[1].own()
-    tok[2].own()
-    tok[3].own()
-    place(4, 5)
+    gm.put(0, NP)
+    tok[2].own_p()
+    gm.put(0, NM)
+    gm.put(1, NP)
+    tok[2].own_m()
     lay_up()
-    lay_down()
-    gm.put(0, NP)
-    gm.put(1, NP)
-    gm.put(0, NM)
+    tok[0].own_p()
     gm.put(1, NM)
-    gm.put(1, FP0)
-    gm.put(0, FP0)
-    gm.put(1, FM0)
-    gm.put(0, FM0)
+    gp.put(0, FP0)
     gp.put(1, FP0)
-    gp.put(0, FP0)
     gp.put(1, FM0)
     gp.put(0, FM0)
-    tok[0].fp()
-    tok[0].fm()
+    tok[1].own_m()
     gp.put(0, QP)
+    gm.put(1, FP0)
+    tok[0].own_m()
     gp.put(1, QP)
+    gp.put(1, QM)
     gp.put(0, QM)
-    gp.put(1, QM)
+    gm.put(0, FM0)
+    tok[1].own_c()
+    gm.put(0, FP2)
+    gm.put(0, FP1)
+    tok[3].own_p()
+    gp.put(1, FP2)
+    tok[0].own_c()
+    gm.put(0, QP)
     gm.put(1, FP2)
-    gm.put(0, FP2)
+    gm.put(0, FM1)
+    gp.put(1, FM1)
+    tok[2].own_c()
+    tok[1].own_p()
+    gm.put(1, FP1)
+    gp.put(1, FM2)
+    gp.put(0, FP2)
+    lay_down()
+    tok[3].own_m()
+    gp.put(0, FM1)
+    tok[3].own_c()
+    gm.put(1, QP)
+    tok[0].on_cm()
+    gm.put(0, FP0)
+    tok[2].on_m()
+    gm.put(1, QM)
     gm.put(0, QM)
-    gm.put(1, QM)
+    gp.put(0, FP1)
+    tok[2].on_p()
+    gp.put(1, FP1)
+    gp.put(1, FM3)
+    gp.put(1, FP3)
+    gp.put(0, FM2)
+    tok[1].on_m()
+    gp.put(0, FM3)
+    tok[0].on_m()
+    gp.put(0, GP2)
+    gp.put(0, FP3)
+    gp.put(1, GP2)
+    gm.put(1, FM2)
+    tok[2].far_c()
+    gm.put(0, FM3)
+    tok[1].on_p()
+    tok[3].on_cm()
+    tok[0].on_cp()
+    tok[3].on_m()
+    gp.put(1, GM1)
     gm.put(1, FM1)
-    gm.put(0, FM1)
-    tok[1].fp()
-    tok[1].fm()
-    gm.put(0, QP)
-    gm.put(1, QP)
-    gp.put(1, FP2)
-    gp.put(0, FP2)
-    gp.put(1, FM1)
-    gp.put(0, FM1)
-    tok[2].fp()
-    tok[2].fm()
-    gm.put(1, FP1)
-    gm.put(0, FP1)
-    gp.put(1, FM3)
-    gp.put(0, FM3)
-    gp.put(1, FP3)
-    gp.put(0, FP3)
-    tok[3].fp()
-    tok[3].fm()
     gm.put(1, FM3)
-    gm.put(0, FM3)
-    tok[0].xp()
-    tok[0].xm()
-    gm.put(1, FP3)
+    tok[2].on_cp()
+    tok[0].on_p()
+    gp.put(0, GM1)
+    gp.put(0, GP0)
     gm.put(0, FP3)
-    gm.put(1, GM1)
-    gm.put(0, GM1)
-    gm.put(1, GP0)
-    gm.put(0, GP0)
-    gp.put(1, FM2)
-    gp.put(0, FM2)
-    tok[1].xp()
-    tok[1].xm()
-    gp.put(1, FP1)
-    gp.put(0, FP1)
-    tok[0].end()
-    norm(0)
-    tok[2].xp()
-    tok[2].xm()
-    tok[1].end()
-    norm(1)
+    tok[3].on_p()
+    tok[1].on_cp()
+    tok[2].on_cm()
+    tok[3].on_cp()
+    gm.put(0, GP2)
     gp.put(0, GM3)
     gp.put(1, GM3)
-    tok[3].xp()
-    tok[3].xm()
+    tok[1].on_cm()
+    gp.put(1, GP0)
+    tok[1].far_c()
+    tok[0].far_c()
+    gm.put(1, GP0)
+    tok[2].end()
+    gm.put(0, GP0)
+    gm.put(0, GM1)
+    gu.put(1, NP)
+    gm.put(1, GM1)
+    gm.put(1, FM0)
+    gm.put(1, FP3)
+    norm(2)
+    gm.put(1, GM3)
+    gm.put(0, FM2)
+    gv.put(1, NP)
+    tok[1].end()
+    gm.put(0, GM3)
+    gu.put(0, NM)
+    tok[0].end()
     gm.put(1, GP2)
-    gm.put(0, GP2)
-    tok[2].end()
-    norm(2)
-    gp.put(0, GP2)
-    gp.put(1, GP2)
-    tok[3].end()
-    gm.put(0, GM3)
-    gm.put(1, GM3)
-    norm(3)
-    gm.put(0, FM2)
-    gm.put(1, FM2)
-    gp.put(1, GP0)
-    gp.put(0, GP0)
-    gp.put(1, GM1)
-    gp.put(0, GM1)
+    tok[3].far_c()
+    norm(0)
     gu.put(0, NP)
-    gu.put(1, NP)
-    gu.put(0, NM)
+    gv.put(0, NP)
     gu.put(1, NM)
-    gm.end()
+    gu.put(0, FM0)
+    gv.put(0, FP0)
     gd.put(0, NP)
-    gd.put(1, NP)
-    gv.put(0, NM)
     gv.put(1, NM)
-    gu.put(1, FP0)
+    gv.put(1, FP0)
+    norm(1)
     gu.put(0, FP0)
     gp.end()
+    gv.put(0, NM)
     project(0)
-    gu.put(0, FM0)
+    project(1)
+    gm.end()
     gu.put(1, FM0)
+    gv.put(1, FM0)
     mix_terms(0)
+    tok[3].end()
+    mix_terms(1)
+    gu.put(1, QP)
+    gu.put(1, QM)
+    gd.put(1, NP)
+    gu.put(0, QP)
     gu.put(0, FP2)
+    gv.put(0, FM0)
+    project(2)
+    gu.put(0, QM)
+    pairs(0)
+    one[0].dp()
+    one[0].dm()
+    one[0].em()
+    gu.put(1, FP0)
+    one[0].ep()
+    mix_terms(2)
+    gu.put(0, FM1)
+    pairs(1)
+    one[1].dm()
+    gv.put(0, QP)
+    gu.put(1, FM1)
     gu.put(1, FP2)
-    project(1)
-    gu.put(0, FM1)
-    gu.put(1, FM1)
-    gu.put(0, QP)
-    gu.put(1, QP)
-    mix_terms(1)
-    gu.put(0, QM)
-    gu.put(1, QM)
-    gv.put(0, NP)
-    gv.put(1, NP)
-    pairs(0)
-    project(2)
+    one[1].dp()
+    norm(3)
+    one[1].ep()
+    gv.put(0, QM)
+    one[1].em()
+    gv.put(1, QM)
+    project(3)
+    gu.put(0, FM2)
+    gv.put(1, FM1)
+    pairs(2)
+    gv.put(1, QP)
+    one[2].dp()
+    one[2].dm()
+    mix_terms(3)
+    gv.put(0, GP0)
+    gd.put(1, NM)
+    gu.put(0, FM3)
+    gv.put(1, FP2)
+    one[0].pass_on()
+    gu.put(1, GP0)
+    one[2].ep()
+    one[1].pass_on()
+    gd.put(0, NM)
+    gu.put(1, FM3)
+    one[2].em()
+    one[2].pass_on()
+    pairs(3)
     gv.put(0, FM2)
     gv.put(1, FM2)
-    mix_terms(2)
-    pairs(1)
     gv.put(0, FP2)
-    gv.put(1, FP2)
-    project(3)
-    gu.put(0, FM2)
+    gu.put(0, GP2)
+    hidden(0)
+    one[3].dp()
+    one[3].ep()
+    gv.put(1, FM3)
+    hid[0].own_p()
+    gv.put(1, GP0)
+    gu.put(0, FP1)
+    gv.put(0, FM1)
+    one[3].dm()
+    hid[0].own_m()
+    hidden(1)
+    gu.put(1, GP2)
+    gv.put(0, FM3)
+    hid[1].own_c()
+    gd.put(1, QP)
+    gu.put(1, GM1)
+    one[3].em()
+    gv.put(1, FP3)
+    gv.put(0, FP3)
+    gu.put(0, GM3)
     gu.put(1, FM2)
-    one[0].pass_on()
-    mix_terms(3)
-    pairs(2)
-    gu.put(0, FM3)
-    gu.put(1, FM3)
+    gu.put(1, FP1)
+    one[3].pass_on()
+    hid[1].own_p()
     gu.put(0, FP3)
+    hid[0].own_c()
+    gu.put(1, GM3)
+    gd.put(1, QM)
+    gu.put(0, GP0)
+    gu.put(0, GM1)
+    hid[1].own_m()
     gu.put(1, FP3)
-    one[1].pass_on()
-    gv.put(0, QP)
-    gv.put(1, QP)
-    gv.put(1, FM1)
-    gv.put(0, FM1)
-    gu.put(0, GP0)
-    gu.put(1, GP0)
-    pairs(3)
-    hidden(0)
-    hid[0].own()
-    gv.put(0, QM)
-    gv.put(1, QM)
-    gu.put(0, GP2)
-    gu.put(1, GP2)
-    one[2].pass_on()
-    gu.put(1, GM3)
-    gu.put(0, GM3)
-    gu.put(0, FP1)
-    gu.put(1, FP1)
-    hidden(1)
-    hid[1].own()
-    gd.put(0, NM)
-    gd.put(1, NM)
-    one[3].pass_on()
+    hid[0].on_m()
+    gd.put(0, QP)
+    hidden(2)
+    hid[2].own_m()
+    gv.put(0, GP2)
+    hid[0].on_p()
     gv.put(0, FP1)
     gv.put(1, FP1)
+    gd.put(0, QM)
+    hid[0].on_cm()
+    hid[2].own_p()
+    hid[1].on_m()
+    hid[1].on_p()
+    gv.put(0, GM3)
+    hid[1].on_cp()
+    gv.put(1, GM3)
+    hidden(3)
+    gv.put(1, GP2)
     gv.put(1, GM1)
+    gd.put(1, FP2)
+    ge.put(0, NP)
     gv.put(0, GM1)
-    gv.put(0, FP0)
-    gv.put(1, FP0)
-    gv.put(1, FM3)
-    gv.put(0, FM3)
-    hid[0].fp()
-    hid[0].fm()
-    hidden(2)
-    hid[2].own()
-    gv.put(0, FP3)
-    gv.put(1, FP3)
-    gv.put(1, FM0)
-    gv.put(0, FM0)
-    hid[1].fp()
-    hid[1].fm()
-    gv.put(0, GP2)
-    gv.put(1, GP2)
-    gu.put(1, GM1)
-    gu.put(0, GM1)
-    hidden(3)
-    hid[3].own()
-    gv.put(1, GM3)
-    gv.put(0, GM3)
-    hid[0].xp()
-    hid[0].xm()
-    gv.put(0, GP0)
-    gv.put(1, GP0)
+    hid[0].far_c()
+    hid[3].own_c()
+    ge.put(1, NP)
+    gd.put(0, FP2)
+    hid[3].own_p()
+    hid[3].own_m()
+    gd.put(0, FP0)
+    ge.put(0, NM)
+    hid[0].on_cp()
+    gd.put(0, FM1)
+    gd.put(1, FP0)
+    hid[2].own_c()
+    hid[2].on_p()
+    gd.put(1, FM1)
+    ge.put(1, NM)
+    hid[1].on_cm()
     hid[0].end()
+    hid[2].on_cm()
+    gd.put(1, FM3)
+    hid[2].on_m()
+    gd.put(0, FP1)
+    gd.put(0, FP3)
     scale(0)
-    gd.put(1, FM1)
-    gd.put(0, FM1)
-    hid[2].fp()
-    hid[2].fm()
-    gd.put(1, QP)
-    gd.put(0, QP)
-    gd.put(0, FP1)
+    gd.put(0, FM3)
+    gd.put(1, FM2)
+    gu.end()
+    hid[1].far_c()
+    gd.put(1, FM0)
+    expand(0, 0, 640)
+    hid[3].on_p()
+    gd.put(0, FM2)
+    hid[3].on_cm()
+    gd.put(0, FM0)
     gd.put(1, FP1)
-    gu.end()
-    gd.put(0, QM)
-    gd.put(1, QM)
-    hid[1].xp()
-    hid[1].xm()
-    ge.put(0, NM)
-    ge.put(1, NM)
-    gd.put(0, FP2)
-    gd.put(1, FP2)
-    gd.put(1, FM2)
-    gd.put(0, FM2)
+    hid[2].on_cp()
+    hid[3].on_cp()
+    hid[3].on_m()
     hid[1].end()
     scale(1)
-    ge.put(0, NP)
-    ge.put(1, NP)
+    expand(1, 0, 640)
+    hid[2].far_c()
+    gd.put(1, FP3)
     gv.end()
-    hid[3].fp()
-    hid[3].fm()
-    expand(0)
-    hid[2].xp()
-    hid[2].xm()
-    gd.put(0, FM3)
-    gd.put(1, FM3)
-    gd.put(0, FP3)
-    gd.put(1, FP3)
+    expand(0, 640, 1408)
+    expand(1, 640, 1408)
     activate(0)
+    ge.put(0, QM)
+    ge.put(1, QM)
+    ge.put(1, QP)
     gd.put(0, GM1)
-    gd.put(1, GM1)
-    gd.put(0, FP0)
-    gd.put(1, FP0)
-    expand(1)
-    hid[3].xp()
-    hid[3].xm()
     hid[2].end()
-    ge.put(0, FM1)
-    ge.put(1, FM1)
+    gd.put(0, GP2)
     ge.put(0, QP)
-    ge.put(1, QP)
-    ge.put(0, FP2)
-    ge.put(1, QM)
-    ge.put(0, QM)
-    ge.put(1, FP2)
-    activate(1)
-    gd.put(0, FM0)
-    gd.put(1, FM0)
-    gd.put(0, GP2)
     gd.put(1, GP2)
     scale(2)
-    expand(2)
+    hid[3].far_c()
+    gd.put(1, GM1)
+    expand(2, 0, 640)
+    gd.put(1, GM3)
+    gd.put(1, GP0)
+    gd.put(0, GP0)
+    ge.put(1, FM1)
+    activate(1)
+    ge.put(0, FP2)
+    ge.put(0, FP0)
+    gd.put(0, GM3)
+    expand(2, 640, 1408)
+    ge.put(1, FP2)
     hid[3].end()
-    gd.put(0, GM3)
-    gd.put(1, GM3)
-    gd.put(0, GP0)
-    gd.put(1, GP0)
+    scale(3)
+    ge.put(0, FM1)
     activate(2)
-    ge.put(0, FP1)
-    ge.put(1, FP1)
-    ge.put(0, FM2)
-    ge.put(1, FM2)
-    scale(3)
-    expand(3)
     ge.put(0, FM3)
     ge.put(1, FM3)
-    ge.put(0, FP0)
+    ge.put(1, FM2)
+    ge.put(0, FM0)
     ge.put(1, FP0)
+    ge.put(0, FM2)
+    ge.put(1, FP3)
+    ge.put(1, FM0)
+    ge.put(0, FP1)
+    expand(3, 0, 640)
+    ge.put(1, FP1)
+    ge.put(0, FP3)
+    expand(3, 640, 1408)
     activate(3)
+    gd.end()
+    down_terms(0, 0, 1)
+    down_terms(0, 0, 2)
+    down_terms(0, 0, 0)
+    down_terms(0, 1, 0)
     ge.put(0, GM1)
     ge.put(1, GM1)
     ge.put(0, GP2)
     ge.put(1, GP2)
-    ge.put(0, FM0)
-    ge.put(1, FM0)
-    ge.put(0, FP3)
-    ge.put(1, FP3)
-    gd.end()
-    down_terms(0, 0)
-    down_terms(0, 1)
-    down_terms(0, 2)
-    pair_all(0, 0)
+    down_terms(0, 1, 1)
+    down_terms(0, 1, 2)
     ge.put(0, GM3)
+    down_terms(0, 2, 2)
     ge.put(1, GM3)
     ge.put(0, GP0)
+    pair_first(0, 1)
+    two[1].dp()
+    two[1].dm()
     ge.put(1, GP0)
-    down_terms(0, 3)
+    down_terms(0, 2, 1)
+    down_terms(0, 2, 0)
+    pair_first(0, 0)
+    two[0].dp()
+    pair_first(0, 2)
+    two[0].dm()
+    two[2].dp()
+    two[2].dm()
+    down_terms(0, 3, 1)
     pair_all(0, 1)
+    down_terms(0, 3, 2)
+    two[1].ep()
+    two[0].ep()
     pair_all(0, 2)
+    two[0].em()
+    two[1].em()
+    down_terms(0, 3, 0)
+    ge.end()
+    two[2].ep()
+    two[2].em()
+    two[1].pass_on()
+    down_terms(1, 0, 1)
+    down_terms(1, 0, 0)
+    down_terms(1, 0, 2)
+    down_terms(1, 1, 0)
+    two[0].pass_on()
+    down_terms(1, 1, 1)
+    two[2].pass_on()
     pair_all(0, 3)
-    two[0].pass_on()
-    ge.end()
-    down_terms(1, 0)
-    two[1].pass_on()
-    down_terms(1, 1)
-    two[2].pass_on()
-    down_terms(1, 2)
-    pair_all(1, 0)
-    down_terms(1, 3)
+    down_terms(1, 2, 1)
+    pair_first(1, 1)
+    down_terms(1, 1, 2)
+    tri[1].dm()
+    tri[1].dp()
+    down_terms(1, 2, 0)
+    pair_first(1, 2)
+    down_terms(1, 2, 2)
+    tri[2].dm()
+    pair_first(1, 0)
+    tri[0].dp()
+    down_terms(1, 3, 1)
+    tri[0].dm()
+    down_terms(1, 3, 0)
     pair_all(1, 1)
+    tri[0].ep()
     pair_all(1, 2)
+    tri[0].em()
+    tri[2].dp()
+    tri[2].ep()
+    down_terms(1, 3, 2)
+    tri[2].em()
+    tri[1].ep()
+    tri[1].em()
+    tri[1].pass_on()
     pair_all(1, 3)
     tri[0].pass_on()
-    tri[1].pass_on()
     tri[2].pass_on()
+    finish(1)
     finish(0)
-    finish(1)
     finish(2)
     for gather in (gp, gm, gu, gv, gd, ge):
-        all_sent(gather.sent, gather.group)
+        gather.sent()
     all_sent(rows.at[:, pl.ds(0, 1792)], 6)
     all_sent(rows2.at[:, pl.ds(0, 1792)], 7)
     all_sent(psend1, 8)

time: 91.4 us -> 91.6 us (level)
  no operation moved by 1% of the time
where the time goes in v5:
time: 91.6 us; the launch traced here: 91.5 us
  Pallas kernels  90.8 us (99%)
    pallas_call x1, Pallas kernels, on_device(): pl.pallas_call(kernel, out_shape=pltpu.VMEM((SEQ, 256), BF16), in_specs=[...  90.8 us

profile of v5, /device:TPU:1, one launch (start us, length us, event | category | flops | bytes accessed | tf_op | source)
XLA Modules:
  0.0 91.5 jit_solution(6984671401425603841)
XLA Ops:
  0.0 90.8 %shard_map.136 = bf16[768,256]{1,0:T(8,128)(2,1)S(1)} custom-call(bf16[768,256]{1,0:T(8,128)(2,1)} %tokens.1, f32[1,2048]{1,0:T(1,128)} %bitcast.9, bf16[128,256]{1,0:T(8,128)(2,1)} %outer_gate.1, bf16[128,256]{1,0:T(8,128)(2,1)} %inner_gate.1, bf16[128,256]{1,0:T(8,128)(2,1)} %signal_in.1, f32[3,256]{1,0:T(4,128)} %mix_taps.1, f32[1,256]{1,0:T(1,128)} %bitcast.11, ...), custom_call_target="tpu_custom_call" | custom-call | tf_op jit(solution)/shard_map/pallas_call | solution.py:934
  90.8 0.7 copy.16

commit v6 on v5

--- a/solution.py
+++ b/solution.py
@@ -15,7 +15,7 @@
 R = SEQ // CHUNKS
 PIECES = 3
 Q = SEQ // PIECES
-RECEIVES = 116
+RECEIVES = 112
 GROUPS = 12
 NP, NM, QP, QM, FP0, FM0, FP1, FM1, FP2, FM2, FP3, FM3, GP0, GM1, GP2, GM3 = range(16)
 ROUTE = {
@@ -68,6 +68,7 @@
     ffn_taps_v,
     ffn_bias_v,
     scale_s,
+    part_s,
     rows,
     rows2,
     normed,
@@ -329,25 +330,19 @@
     def across(a, b):
         return lax.dot_general(a, b, (((1,), (1,)), ((), ())), preferred_element_type=F32)
 
-    def down_terms(n, k, r):
+    def down_terms(n, k):
         lines = pl.ds(at(256 * near(y, ORDER[k]), 256), 256)
-        here = pl.ds(r * Q, Q)
         if n == 0:
-            term = across(act[here, 0:768], downw[lines, :])
+            term = across(act[:, 0:768], downw[lines, :])
         else:
-            term = across(act[here, 0:640], downw2[lines, :]) + across(act[here, 768:896], downw[lines, 640:768])
+            term = across(act[:, 0:640], downw2[lines, :]) + across(act[:, 768:896], downw[lines, 640:768])
         low, high = term[:, 0:128], term[:, 128:256]
-        psend2[n, k, here] = jnp.where(c == 0, high, low).astype(BF16)
-        send(psend2.at[n, k, here], precv2.at[n, k, here], (10, n, k, r if k == 0 else PIECES), 10, pc)
-        keep2[n, k, here] = jnp.where(c == 0, low, high)
-
-    def pair_first(n, r):
-        here = pl.ds(r * Q, Q)
-        arrive(precv2.at[n, 0, here], (10, n, 0, r))
-        (two, tri)[n][r].pair(0)
+        psend2[n, k] = jnp.where(c == 0, high, low).astype(BF16)
+        send(psend2.at[n, k], precv2.at[n, k], (10, n, k), 10, pc)
+        keep2[n, k] = jnp.where(c == 0, low, high)
 
     def pair_all(n, k):
-        arrive(precv2.at[n, k], (10, n, k, PIECES))
+        arrive(precv2.at[n, k], (10, n, k))
         for r in range(PIECES):
             (two, tri)[n][r].pair(k)
 
@@ -386,13 +381,12 @@
         )
         gated[r] = (outer_s[...] * conv).astype(BF16)
 
-    def expand(r, first, last):
+    def expand(r):
         lines = pl.ds(r * R, R)
-        while first < last:
-            width = min(256, last - first)
-            term = jnp.dot(rows2[lines, :], upw[:, first : first + width], preferred_element_type=F32)
-            pre[pl.ds(8 + r * R, R), pl.ds(first, width)] = term * scale_s[lines, :]
-            first += width
+        for n in range(6):
+            width = 256 if n < 5 else 128
+            term = jnp.dot(rows2[lines, :], upw[:, n * 256 : n * 256 + width], preferred_element_type=F32)
+            pre[pl.ds(8 + r * R, R), pl.ds(n * 256, width)] = term * scale_s[lines, :]
 
     def conv_cols(r, col, which, j):
         lanes = pl.ds(col, 128)
@@ -488,419 +482,402 @@
         lines = pl.ds(r * R, R)
         rows2[lines, own_cols] = (rows[lines, own_cols].astype(F32) + one[r].total()).astype(BF16)
 
+    def early(r):
+        lines = pl.ds(r * Q, Q)
+        state, a = rows2[lines, own_cols].astype(F32), two[r].total()
+        lane = lax.broadcasted_iota(jnp.int32, (Q, 128), 1)
+        part_s[lines, 0:128] = state[:, 0:128] + jnp.where(lane < 64, a, 0.0)
+        part_s[lines, 128:256] = state[:, 128:256] + jnp.where(lane < 64, pltpu.roll(a, 64, 1), 0.0)
+
     def finish(r):
-        lines = pl.ds(r * Q, Q)
-        state = rows2[lines, own_cols].astype(F32)
-        a, b = two[r].total(), tri[r].total()
+        lines, b = pl.ds(r * Q, Q), tri[r].total()
         lane = lax.broadcasted_iota(jnp.int32, (Q, 128), 1)
-        first = jnp.where(lane < 64, a, pltpu.roll(b, 64, 1))
-        last = jnp.where(lane < 64, pltpu.roll(a, 64, 1), b)
-        out[lines, 0:128] = (state[:, 0:128] + first).astype(BF16)
-        out[lines, 128:256] = (state[:, 128:256] + last).astype(BF16)
+        first, last = jnp.where(lane < 64, 0.0, pltpu.roll(b, 64, 1)), jnp.where(lane < 64, 0.0, b)
+        out[lines, 0:128] = (part_s[lines, 0:128] + first).astype(BF16)
+        out[lines, 128:256] = (part_s[lines, 128:256] + last).astype(BF16)
 
     mi[0:8, :] = jnp.zeros((8, 256), F32)
     pre[0:8, :] = jnp.zeros((8, 1408), F32)
     pl.semaphore_wait(barrier, 7)
 
     place(1, 4)
+    gp.put(0, NP)
     gp.put(1, NM)
+    gp.put(1, NP)
     gp.put(0, NM)
-    gp.put(1, NP)
-    gp.put(0, NP)
     place(4, 5)
     place(0, 1)
+    gm.put(1, FM0)
+    gm.put(0, NM)
     gm.put(0, NP)
+    lay_up()
+    tok[2].own_m()
+    gm.put(1, NP)
+    gm.put(0, FP0)
+    gm.put(1, NM)
+    gp.put(1, FM0)
+    gp.put(0, FP0)
+    tok[0].own_p()
+    tok[1].own_p()
+    gp.put(0, FM0)
+    gm.put(1, FP0)
+    gp.put(1, FP0)
+    tok[0].own_m()
+    tok[0].own_c()
+    tok[2].own_c()
     tok[2].own_p()
-    gm.put(0, NM)
-    gm.put(1, NP)
-    tok[2].own_m()
-    lay_up()
-    tok[0].own_p()
-    gm.put(1, NM)
-    gp.put(0, FP0)
-    gp.put(1, FP0)
-    gp.put(1, FM0)
-    gp.put(0, FM0)
+    tok[1].own_c()
+    gm.put(0, FM0)
+    gp.put(1, QP)
     tok[1].own_m()
+    tok[3].own_p()
+    gm.put(1, QP)
+    tok[0].on_p()
+    gm.put(1, FP1)
+    gp.put(1, QM)
+    gp.put(0, FM1)
+    gm.put(1, FM1)
+    gm.put(0, FP2)
+    gm.put(1, QM)
     gp.put(0, QP)
-    gm.put(1, FP0)
-    tok[0].own_m()
-    gp.put(1, QP)
-    gp.put(1, QM)
+    tok[3].own_m()
     gp.put(0, QM)
-    gm.put(0, FM0)
-    tok[1].own_c()
-    gm.put(0, FP2)
+    gp.put(0, FP2)
+    gm.put(1, FP2)
+    gm.put(0, QM)
+    tok[1].on_p()
+    tok[0].on_m()
+    tok[2].on_m()
+    gp.put(1, FP2)
+    gp.put(0, FM2)
+    gp.put(1, FM1)
+    gm.put(0, FM2)
+    gp.put(0, FP1)
+    gp.put(0, GP0)
+    tok[0].on_cm()
+    tok[0].on_cp()
+    gm.put(1, FM2)
+    gm.put(0, QP)
+    gp.put(1, FM3)
+    gp.put(0, FP3)
+    tok[1].on_cm()
+    gp.put(1, FP3)
+    tok[2].on_cp()
+    gp.put(1, GP0)
+    tok[3].own_c()
+    gm.put(0, GP0)
+    gm.put(0, FM1)
+    tok[3].on_cp()
+    gp.put(0, FM3)
+    gp.put(1, FM2)
+    gm.put(1, FM3)
+    tok[2].on_cm()
+    gm.put(1, GP2)
+    tok[3].on_m()
+    tok[3].on_p()
+    tok[0].far_c()
+    gp.put(1, GM1)
+    gm.put(0, FM3)
+    gm.put(0, GP2)
+    tok[2].on_p()
+    gp.put(1, GP2)
+    tok[3].on_cm()
+    gp.put(1, FP1)
+    gp.put(0, GM1)
+    gm.put(1, FP3)
+    tok[0].end()
+    tok[1].on_m()
+    lay_down()
+    norm(0)
+    tok[1].on_cp()
+    gp.put(0, GP2)
+    gp.put(1, GM3)
+    gp.put(0, GM3)
+    gm.put(0, GM1)
     gm.put(0, FP1)
-    tok[3].own_p()
-    gp.put(1, FP2)
-    tok[0].own_c()
-    gm.put(0, QP)
-    gm.put(1, FP2)
-    gm.put(0, FM1)
-    gp.put(1, FM1)
-    tok[2].own_c()
-    tok[1].own_p()
-    gm.put(1, FP1)
-    gp.put(1, FM2)
-    gp.put(0, FP2)
-    lay_down()
-    tok[3].own_m()
-    gp.put(0, FM1)
-    tok[3].own_c()
-    gm.put(1, QP)
-    tok[0].on_cm()
-    gm.put(0, FP0)
-    tok[2].on_m()
-    gm.put(1, QM)
-    gm.put(0, QM)
-    gp.put(0, FP1)
-    tok[2].on_p()
-    gp.put(1, FP1)
-    gp.put(1, FM3)
-    gp.put(1, FP3)
-    gp.put(0, FM2)
-    tok[1].on_m()
-    gp.put(0, FM3)
-    tok[0].on_m()
-    gp.put(0, GP2)
-    gp.put(0, FP3)
-    gp.put(1, GP2)
-    gm.put(1, FM2)
+    gm.put(1, GM3)
+    gm.put(0, FP3)
     tok[2].far_c()
-    gm.put(0, FM3)
-    tok[1].on_p()
-    tok[3].on_cm()
-    tok[0].on_cp()
-    tok[3].on_m()
-    gp.put(1, GM1)
-    gm.put(1, FM1)
-    gm.put(1, FM3)
-    tok[2].on_cp()
-    tok[0].on_p()
-    gp.put(0, GM1)
-    gp.put(0, GP0)
-    gm.put(0, FP3)
-    tok[3].on_p()
-    tok[1].on_cp()
-    tok[2].on_cm()
-    tok[3].on_cp()
-    gm.put(0, GP2)
-    gp.put(0, GM3)
-    gp.put(1, GM3)
-    tok[1].on_cm()
-    gp.put(1, GP0)
+    gm.put(1, GM1)
+    gm.put(1, GP0)
+    gv.put(0, NM)
+    tok[3].far_c()
+    gm.put(0, GM3)
+    gv.put(1, NP)
     tok[1].far_c()
-    tok[0].far_c()
-    gm.put(1, GP0)
+    gu.put(1, NP)
+    gv.put(0, NP)
+    gv.put(0, FP0)
+    gv.put(1, NM)
     tok[2].end()
-    gm.put(0, GP0)
-    gm.put(0, GM1)
-    gu.put(1, NP)
-    gm.put(1, GM1)
-    gm.put(1, FM0)
-    gm.put(1, FP3)
+    gd.put(1, NM)
+    gu.put(0, NM)
+    gu.put(1, NM)
+    gu.put(0, NP)
+    tok[1].end()
+    gu.put(0, FM0)
+    gu.put(1, FP0)
     norm(2)
-    gm.put(1, GM3)
-    gm.put(0, FM2)
-    gv.put(1, NP)
-    tok[1].end()
-    gm.put(0, GM3)
-    gu.put(0, NM)
-    tok[0].end()
-    gm.put(1, GP2)
-    tok[3].far_c()
-    norm(0)
-    gu.put(0, NP)
-    gv.put(0, NP)
-    gu.put(1, NM)
-    gu.put(0, FM0)
-    gv.put(0, FP0)
-    gd.put(0, NP)
-    gv.put(1, NM)
+    gd.put(0, NM)
     gv.put(1, FP0)
     norm(1)
-    gu.put(0, FP0)
     gp.end()
-    gv.put(0, NM)
     project(0)
-    project(1)
     gm.end()
-    gu.put(1, FM0)
-    gv.put(1, FM0)
     mix_terms(0)
     tok[3].end()
+    project(1)
+    gv.put(1, QM)
+    gv.put(0, QM)
+    gu.put(0, FP0)
+    gv.put(1, QP)
+    gd.put(1, NP)
+    gv.put(1, FM2)
     mix_terms(1)
+    gv.put(1, FM1)
+    gv.put(0, FM0)
+    pairs(0)
     gu.put(1, QP)
-    gu.put(1, QM)
-    gd.put(1, NP)
-    gu.put(0, QP)
-    gu.put(0, FP2)
-    gv.put(0, FM0)
-    project(2)
-    gu.put(0, QM)
-    pairs(0)
-    one[0].dp()
+    gu.put(1, FM0)
     one[0].dm()
     one[0].em()
-    gu.put(1, FP0)
+    one[0].dp()
+    gv.put(0, QP)
+    gu.put(0, QP)
+    project(2)
     one[0].ep()
+    gv.put(0, FP2)
     mix_terms(2)
-    gu.put(0, FM1)
+    gu.put(0, FM2)
     pairs(1)
     one[1].dm()
-    gv.put(0, QP)
-    gu.put(1, FM1)
     gu.put(1, FP2)
+    gu.put(1, FM2)
+    one[1].ep()
+    one[1].em()
+    gu.put(0, QM)
+    gu.put(0, FP2)
     one[1].dp()
     norm(3)
-    one[1].ep()
-    gv.put(0, QM)
-    one[1].em()
-    gv.put(1, QM)
+    one[0].pass_on()
+    gv.put(1, FP3)
+    gu.put(1, GP0)
+    gu.put(1, QM)
+    gu.put(1, FM1)
+    gv.put(1, FP2)
+    pairs(2)
+    gv.put(0, FP3)
+    gu.put(0, FP1)
+    gv.put(0, FM3)
+    gv.put(0, FM1)
+    gv.put(1, FM3)
+    one[2].em()
+    gu.put(0, FM1)
+    one[2].ep()
+    one[2].dm()
     project(3)
-    gu.put(0, FM2)
-    gv.put(1, FM1)
-    pairs(2)
-    gv.put(1, QP)
     one[2].dp()
-    one[2].dm()
     mix_terms(3)
+    one[1].pass_on()
+    hidden(0)
+    gv.put(0, FP1)
+    hid[0].own_m()
+    gv.put(1, FM0)
+    hid[0].own_p()
+    pairs(3)
     gv.put(0, GP0)
-    gd.put(1, NM)
+    gv.put(0, FM2)
+    gu.put(0, GP2)
+    gv.put(1, GP0)
+    one[3].dp()
+    hid[0].own_c()
     gu.put(0, FM3)
-    gv.put(1, FP2)
-    one[0].pass_on()
-    gu.put(1, GP0)
-    one[2].ep()
-    one[1].pass_on()
-    gd.put(0, NM)
+    gu.put(0, FP3)
+    one[3].dm()
+    hidden(1)
+    gd.put(0, NP)
     gu.put(1, FM3)
-    one[2].em()
+    gu.put(1, FP1)
     one[2].pass_on()
-    pairs(3)
-    gv.put(0, FM2)
-    gv.put(1, FM2)
-    gv.put(0, FP2)
-    gu.put(0, GP2)
-    hidden(0)
-    one[3].dp()
-    one[3].ep()
-    gv.put(1, FM3)
-    hid[0].own_p()
-    gv.put(1, GP0)
-    gu.put(0, FP1)
-    gv.put(0, FM1)
-    one[3].dm()
-    hid[0].own_m()
-    hidden(1)
-    gu.put(1, GP2)
-    gv.put(0, FM3)
-    hid[1].own_c()
-    gd.put(1, QP)
-    gu.put(1, GM1)
+    hid[1].own_p()
+    gv.put(1, GM1)
+    hid[1].own_m()
+    gv.put(1, GP2)
     one[3].em()
-    gv.put(1, FP3)
-    gv.put(0, FP3)
-    gu.put(0, GM3)
-    gu.put(1, FM2)
-    gu.put(1, FP1)
-    one[3].pass_on()
-    hid[1].own_p()
-    gu.put(0, FP3)
-    hid[0].own_c()
-    gu.put(1, GM3)
-    gd.put(1, QM)
-    gu.put(0, GP0)
-    gu.put(0, GM1)
-    hid[1].own_m()
     gu.put(1, FP3)
     hid[0].on_m()
+    one[3].pass_on()
+    hid[1].own_c()
+    gv.put(1, FP1)
+    hid[0].on_p()
+    hid[0].on_cp()
+    gv.put(0, GP2)
+    gu.put(1, GP2)
+    gv.put(0, GM1)
+    one[3].ep()
+    gu.put(1, GM1)
+    hidden(2)
+    hid[2].own_p()
+    gv.put(1, GM3)
+    hid[2].own_m()
     gd.put(0, QP)
-    hidden(2)
-    hid[2].own_m()
-    gv.put(0, GP2)
-    hid[0].on_p()
-    gv.put(0, FP1)
-    gv.put(1, FP1)
+    gu.put(0, GM1)
+    hid[1].on_p()
+    hid[1].on_m()
+    gv.put(0, GM3)
+    hid[1].on_cm()
+    gu.put(0, GM3)
+    hid[0].on_cm()
+    hid[0].far_c()
+    ge.put(1, NM)
+    gu.put(1, GM3)
+    gu.put(0, GP0)
+    gd.put(1, QP)
+    hidden(3)
+    hid[1].on_cp()
+    hid[3].own_m()
+    hid[3].own_c()
+    gd.put(1, QM)
+    hid[3].own_p()
+    hid[2].own_c()
+    ge.put(1, NP)
     gd.put(0, QM)
-    hid[0].on_cm()
-    hid[2].own_p()
-    hid[1].on_m()
-    hid[1].on_p()
-    gv.put(0, GM3)
-    hid[1].on_cp()
-    gv.put(1, GM3)
-    hidden(3)
-    gv.put(1, GP2)
-    gv.put(1, GM1)
+    gd.put(0, FM1)
+    ge.put(0, NM)
+    gd.put(0, FP0)
+    gd.put(1, FM1)
+    gd.put(1, FP0)
+    hid[0].end()
+    gd.put(0, FP2)
     gd.put(1, FP2)
+    gd.put(0, FM2)
     ge.put(0, NP)
-    gv.put(0, GM1)
-    hid[0].far_c()
-    hid[3].own_c()
-    ge.put(1, NP)
-    gd.put(0, FP2)
-    hid[3].own_p()
-    hid[3].own_m()
-    gd.put(0, FP0)
-    ge.put(0, NM)
-    hid[0].on_cp()
-    gd.put(0, FM1)
-    gd.put(1, FP0)
-    hid[2].own_c()
+    hid[2].on_cp()
+    scale(0)
+    hid[1].far_c()
     hid[2].on_p()
-    gd.put(1, FM1)
-    ge.put(1, NM)
-    hid[1].on_cm()
-    hid[0].end()
-    hid[2].on_cm()
-    gd.put(1, FM3)
     hid[2].on_m()
     gd.put(0, FP1)
-    gd.put(0, FP3)
-    scale(0)
-    gd.put(0, FM3)
-    gd.put(1, FM2)
-    gu.end()
-    hid[1].far_c()
-    gd.put(1, FM0)
-    expand(0, 0, 640)
-    hid[3].on_p()
-    gd.put(0, FM2)
-    hid[3].on_cm()
-    gd.put(0, FM0)
-    gd.put(1, FP1)
-    hid[2].on_cp()
-    hid[3].on_cp()
-    hid[3].on_m()
     hid[1].end()
     scale(1)
-    expand(1, 0, 640)
+    hid[3].on_m()
+    gd.put(1, FM2)
+    hid[2].on_cm()
+    hid[3].on_p()
+    hid[3].on_cp()
+    hid[3].on_cm()
+    gd.put(1, FP1)
+    gv.end()
+    gu.end()
+    expand(0)
+    gd.put(0, FP3)
+    gd.put(1, FM3)
+    gd.put(0, FM3)
     hid[2].far_c()
+    gd.put(1, FM0)
+    ge.put(0, QM)
     gd.put(1, FP3)
-    gv.end()
-    expand(0, 640, 1408)
-    expand(1, 640, 1408)
+    ge.put(1, QM)
+    gd.put(0, FM0)
+    expand(1)
+    gd.put(1, GP0)
     activate(0)
-    ge.put(0, QM)
-    ge.put(1, QM)
+    hid[2].end()
+    gd.put(0, GM1)
+    gd.put(1, GM1)
+    gd.put(0, GP0)
     ge.put(1, QP)
-    gd.put(0, GM1)
-    hid[2].end()
+    scale(2)
+    gd.put(1, GP2)
+    hid[3].far_c()
+    expand(2)
     gd.put(0, GP2)
+    gd.put(1, GM3)
+    gd.put(0, GM3)
     ge.put(0, QP)
-    gd.put(1, GP2)
-    scale(2)
-    hid[3].far_c()
-    gd.put(1, GM1)
-    expand(2, 0, 640)
-    gd.put(1, GM3)
-    gd.put(1, GP0)
-    gd.put(0, GP0)
-    ge.put(1, FM1)
+    ge.put(1, FM0)
+    ge.put(0, FM0)
+    ge.put(1, FP2)
     activate(1)
-    ge.put(0, FP2)
-    ge.put(0, FP0)
-    gd.put(0, GM3)
-    expand(2, 640, 1408)
-    ge.put(1, FP2)
     hid[3].end()
     scale(3)
+    ge.put(1, FM1)
     ge.put(0, FM1)
+    ge.put(1, FP0)
+    ge.put(0, FP2)
     activate(2)
+    ge.put(0, FP0)
+    expand(3)
+    ge.put(1, FM3)
     ge.put(0, FM3)
-    ge.put(1, FM3)
+    activate(3)
+    ge.put(0, FP1)
+    ge.put(1, FP1)
+    gd.end()
+    down_terms(0, 0)
+    ge.put(1, FP3)
+    ge.put(0, GP2)
+    ge.put(0, FM2)
     ge.put(1, FM2)
-    ge.put(0, FM0)
-    ge.put(1, FP0)
-    ge.put(0, FM2)
-    ge.put(1, FP3)
-    ge.put(1, FM0)
-    ge.put(0, FP1)
-    expand(3, 0, 640)
-    ge.put(1, FP1)
+    down_terms(0, 1)
+    ge.put(1, GP2)
+    ge.put(1, GM1)
+    ge.put(0, GP0)
     ge.put(0, FP3)
-    expand(3, 640, 1408)
-    activate(3)
-    gd.end()
-    down_terms(0, 0, 1)
-    down_terms(0, 0, 2)
-    down_terms(0, 0, 0)
-    down_terms(0, 1, 0)
+    ge.put(1, GP0)
     ge.put(0, GM1)
-    ge.put(1, GM1)
-    ge.put(0, GP2)
-    ge.put(1, GP2)
-    down_terms(0, 1, 1)
-    down_terms(0, 1, 2)
+    down_terms(0, 2)
     ge.put(0, GM3)
-    down_terms(0, 2, 2)
     ge.put(1, GM3)
-    ge.put(0, GP0)
-    pair_first(0, 1)
+    pair_all(0, 0)
+    two[0].dm()
+    two[0].dp()
     two[1].dp()
     two[1].dm()
-    ge.put(1, GP0)
-    down_terms(0, 2, 1)
-    down_terms(0, 2, 0)
-    pair_first(0, 0)
-    two[0].dp()
-    pair_first(0, 2)
-    two[0].dm()
     two[2].dp()
     two[2].dm()
-    down_terms(0, 3, 1)
     pair_all(0, 1)
-    down_terms(0, 3, 2)
-    two[1].ep()
-    two[0].ep()
+    two[2].ep()
     pair_all(0, 2)
     two[0].em()
+    two[1].ep()
+    two[2].em()
     two[1].em()
-    down_terms(0, 3, 0)
+    down_terms(0, 3)
     ge.end()
-    two[2].ep()
-    two[2].em()
+    two[0].ep()
+    down_terms(1, 0)
     two[1].pass_on()
-    down_terms(1, 0, 1)
-    down_terms(1, 0, 0)
-    down_terms(1, 0, 2)
-    down_terms(1, 1, 0)
     two[0].pass_on()
-    down_terms(1, 1, 1)
+    down_terms(1, 1)
     two[2].pass_on()
+    down_terms(1, 2)
+    pair_all(1, 0)
+    tri[0].dp()
+    tri[0].dm()
     pair_all(0, 3)
-    down_terms(1, 2, 1)
-    pair_first(1, 1)
-    down_terms(1, 1, 2)
+    tri[2].dm()
+    tri[2].dp()
+    down_terms(1, 3)
     tri[1].dm()
     tri[1].dp()
-    down_terms(1, 2, 0)
-    pair_first(1, 2)
-    down_terms(1, 2, 2)
-    tri[2].dm()
-    pair_first(1, 0)
-    tri[0].dp()
-    down_terms(1, 3, 1)
-    tri[0].dm()
-    down_terms(1, 3, 0)
     pair_all(1, 1)
     tri[0].ep()
     pair_all(1, 2)
+    tri[2].ep()
     tri[0].em()
-    tri[2].dp()
-    tri[2].ep()
-    down_terms(1, 3, 2)
     tri[2].em()
     tri[1].ep()
+    early(2)
+    pair_all(1, 3)
     tri[1].em()
+    tri[0].pass_on()
+    early(1)
     tri[1].pass_on()
-    pair_all(1, 3)
-    tri[0].pass_on()
+    early(0)
     tri[2].pass_on()
+    finish(0)
     finish(1)
-    finish(0)
     finish(2)
     for gather in (gp, gm, gu, gv, gd, ge):
         gather.sent()
@@ -944,6 +921,7 @@
             pltpu.VMEM((3, 2, 704), F32),
             pltpu.VMEM((2, 704), F32),
             pltpu.VMEM((SEQ, 1), F32),
+            pltpu.VMEM((SEQ, 256), F32),
             pltpu.VMEM((SEQ, D), BF16),
             pltpu.VMEM((SEQ, D), BF16),
             pltpu.VMEM((SEQ, D), BF16),

time: 91.6 us -> 90.8 us (level)
  Pallas kernels: 90.8 us -> 89.7 us
    pallas_call x1, Pallas kernels: 90.8 us -> 89.7 us  [on_device(): pl.pallas_call(kernel, out_shape=pltpu.VMEM((SEQ, 256), BF16), in_specs=[...]
where the time goes in v6:
time: 90.8 us; the launch traced here: 90.4 us
  Pallas kernels  89.7 us (99%)
    pallas_call x1, Pallas kernels, on_device(): pl.pallas_call(kernel, out_shape=pltpu.VMEM((SEQ, 256), BF16), in_specs=[...  89.7 us

profile of v6, /device:TPU:1, one launch (start us, length us, event | category | flops | bytes accessed | tf_op | source)
XLA Modules:
  0.0 90.4 jit_solution(13545326023526528370)
XLA Ops:
  0.0 89.7 %shard_map.136 = bf16[768,256]{1,0:T(8,128)(2,1)S(1)} custom-call(bf16[768,256]{1,0:T(8,128)(2,1)} %tokens.1, f32[1,2048]{1,0:T(1,128)} %bitcast.9, bf16[128,256]{1,0:T(8,128)(2,1)} %outer_gate.1, bf16[128,256]{1,0:T(8,128)(2,1)} %inner_gate.1, bf16[128,256]{1,0:T(8,128)(2,1)} %signal_in.1, f32[3,256]{1,0:T(4,128)} %mix_taps.1, f32[1,256]{1,0:T(1,128)} %bitcast.11, ...), custom_call_target="tpu_custom_call" | custom-call | tf_op jit(solution)/shard_map/pallas_call | solution.py:911
  89.7 0.7 copy.16

commit v7 on v6

--- a/solution.py
+++ b/solution.py
@@ -15,7 +15,7 @@
 R = SEQ // CHUNKS
 PIECES = 3
 Q = SEQ // PIECES
-RECEIVES = 112
+RECEIVES = 92
 GROUPS = 12
 NP, NM, QP, QM, FP0, FM0, FP1, FM1, FP2, FM2, FP3, FM3, GP0, GM1, GP2, GM3 = range(16)
 ROUTE = {
@@ -203,12 +203,12 @@
                 size = size // 2
                 start = start + half * size
             ref = self.buf.at[pl.ds(start, size), pl.ds(at(256 * (2 * near(y, dy) + c), 256), 256)]
-            send(ref, ref, (self.group, self.r, key), self.group, dev)
+            send(ref, ref, (6, self.r, key), self.group, dev)
 
         def get(self, key, blocks=1):
             if key not in self.got:
                 self.got.add(key)
-                arrive(self.buf.at[pl.ds(self.r * R, R), pl.ds(0, 256 * blocks)], (self.group, self.r, key))
+                arrive(self.buf.at[pl.ds(self.r * R, R), pl.ds(0, 256 * blocks)], (6, self.r, key))
 
         def own_p(self):
             self.put(0, 0, yp)
@@ -248,7 +248,8 @@
 
     class Sums:
         def __init__(self, group, r, start, size, keep, mine, leave, mid, fin):
-            self.group, self.r, self.start, self.size = group, r, start, size
+            self.group, self.start, self.size = group, start, size
+            self.r = (9 if r < CHUNKS else 11, r)
             self.keep, self.mine, self.leave, self.mid, self.fin = keep, mine, leave, mid, fin
 
         def pair(self, k):
@@ -267,7 +268,7 @@
                 self.keep[k, lines] = total
 
         def go(self, k, half, dst, key, dev):
-            send(self.leave.at[k, half], dst, (self.group, self.r, key), self.group, dev)
+            send(self.leave.at[k, half], dst, (*self.r, key), self.group, dev)
 
         def halves(self):
             half = self.size // 2
@@ -290,14 +291,14 @@
         def pass_on(self):
             half = self.size // 2
             low, high = self.halves()
-            arrive(self.mid, (self.group, self.r, 2))
+            arrive(self.mid, (*self.r, 2))
             self.leave[1, low] = (self.keep[1, pl.ds(self.start, half)] + self.mid[0].astype(F32)).astype(BF16)
             self.go(1, low, self.fin.at[0, low], 3, yp)
             self.leave[2, high] = (self.keep[2, pl.ds(self.start + half, half)] + self.mid[1].astype(F32)).astype(BF16)
             self.go(2, high, self.fin.at[1, high], 3, ym)
 
         def total(self):
-            arrive(self.fin, (self.group, self.r, 3))
+            arrive(self.fin, (*self.r, 3))
             return self.keep[3, pl.ds(self.start, self.size)] + self.fin[0].astype(F32) + self.fin[1].astype(F32)
 
     one = [
@@ -338,11 +339,18 @@
             term = across(act[:, 0:640], downw2[lines, :]) + across(act[:, 768:896], downw[lines, 640:768])
         low, high = term[:, 0:128], term[:, 128:256]
         psend2[n, k] = jnp.where(c == 0, high, low).astype(BF16)
-        send(psend2.at[n, k], precv2.at[n, k], (10, n, k), 10, pc)
+        for r in range(PIECES if k == 0 else 1):
+            here = pl.ds(r * Q, Q if k == 0 else SEQ)
+            send(psend2.at[n, k, here], precv2.at[n, k, here], (10, n, k, r), 10, pc)
         keep2[n, k] = jnp.where(c == 0, low, high)
 
+    def pair_first(n, r):
+        here = pl.ds(r * Q, Q)
+        arrive(precv2.at[n, 0, here], (10, n, 0, r))
+        (two, tri)[n][r].pair(0)
+
     def pair_all(n, k):
-        arrive(precv2.at[n, k], (10, n, k))
+        arrive(precv2.at[n, k], (10, n, k, 0))
         for r in range(PIECES):
             (two, tri)[n][r].pair(k)
 
@@ -501,382 +509,386 @@
     pl.semaphore_wait(barrier, 7)
 
     place(1, 4)
+    gp.put(1, NP)
+    gp.put(1, NM)
+    gp.put(0, NM)
     gp.put(0, NP)
-    gp.put(1, NM)
-    gp.put(1, NP)
-    gp.put(0, NM)
     place(4, 5)
+    gm.put(1, NM)
     place(0, 1)
-    gm.put(1, FM0)
+    gm.put(0, NP)
+    tok[3].own_m()
+    tok[1].own_p()
     gm.put(0, NM)
-    gm.put(0, NP)
-    lay_up()
-    tok[2].own_m()
     gm.put(1, NP)
-    gm.put(0, FP0)
-    gm.put(1, NM)
+    tok[2].own_p()
+    gp.put(0, FM0)
     gp.put(1, FM0)
     gp.put(0, FP0)
+    gp.put(1, FP0)
+    tok[1].own_m()
+    tok[2].own_m()
+    gp.put(0, QP)
+    tok[1].own_c()
+    gp.put(0, FP2)
+    gp.put(0, QM)
+    gp.put(0, FM1)
+    tok[0].own_c()
+    gm.put(1, QM)
+    tok[3].own_c()
+    tok[2].own_c()
+    gp.put(1, FP2)
+    gp.put(1, QM)
+    gp.put(1, QP)
+    gm.put(0, QM)
+    gm.put(1, QP)
+    gm.put(0, QP)
+    gp.put(1, FM1)
+    gp.put(1, FM2)
+    gm.put(0, FP0)
     tok[0].own_p()
-    tok[1].own_p()
-    gp.put(0, FM0)
+    lay_up()
+    gp.put(0, FP1)
+    tok[0].own_m()
+    tok[3].own_p()
+    gm.put(1, FP2)
+    gm.put(0, FM0)
     gm.put(1, FP0)
-    gp.put(1, FP0)
-    tok[0].own_m()
-    tok[0].own_c()
-    tok[2].own_c()
-    tok[2].own_p()
-    tok[1].own_c()
-    gm.put(0, FM0)
-    gp.put(1, QP)
-    tok[1].own_m()
-    tok[3].own_p()
-    gm.put(1, QP)
-    tok[0].on_p()
-    gm.put(1, FP1)
-    gp.put(1, QM)
-    gp.put(0, FM1)
+    gm.put(0, FP2)
+    gp.put(1, GP0)
     gm.put(1, FM1)
-    gm.put(0, FP2)
-    gm.put(1, QM)
-    gp.put(0, QP)
-    tok[3].own_m()
-    gp.put(0, QM)
-    gp.put(0, FP2)
-    gm.put(1, FP2)
-    gm.put(0, QM)
-    tok[1].on_p()
-    tok[0].on_m()
+    gp.put(0, GP0)
+    gp.put(0, FM2)
+    tok[2].on_cm()
+    tok[2].on_p()
     tok[2].on_m()
-    gp.put(1, FP2)
-    gp.put(0, FM2)
-    gp.put(1, FM1)
-    gm.put(0, FM2)
-    gp.put(0, FP1)
-    gp.put(0, GP0)
-    tok[0].on_cm()
-    tok[0].on_cp()
-    gm.put(1, FM2)
-    gm.put(0, QP)
-    gp.put(1, FM3)
+    gp.put(0, FM3)
+    tok[2].on_cp()
     gp.put(0, FP3)
+    gm.put(0, FM3)
     tok[1].on_cm()
     gp.put(1, FP3)
-    tok[2].on_cp()
-    gp.put(1, GP0)
-    tok[3].own_c()
-    gm.put(0, GP0)
+    gm.put(0, FP3)
+    gm.put(1, FM2)
     gm.put(0, FM1)
-    tok[3].on_cp()
-    gp.put(0, FM3)
-    gp.put(1, FM2)
+    gp.put(1, GP2)
+    gp.put(1, FM3)
+    tok[0].on_cm()
+    tok[0].on_p()
+    tok[1].on_p()
+    gp.put(0, GP2)
+    gp.put(0, GM1)
+    tok[1].on_m()
     gm.put(1, FM3)
-    tok[2].on_cm()
+    gm.put(0, GP2)
+    tok[2].far_c()
+    gp.put(1, GM1)
+    gp.put(1, FP1)
     gm.put(1, GP2)
-    tok[3].on_m()
-    tok[3].on_p()
-    tok[0].far_c()
-    gp.put(1, GM1)
-    gm.put(0, FM3)
-    gm.put(0, GP2)
-    tok[2].on_p()
-    gp.put(1, GP2)
-    tok[3].on_cm()
-    gp.put(1, FP1)
-    gp.put(0, GM1)
-    gm.put(1, FP3)
-    tok[0].end()
-    tok[1].on_m()
-    lay_down()
-    norm(0)
-    tok[1].on_cp()
-    gp.put(0, GP2)
+    tok[0].on_m()
     gp.put(1, GM3)
+    tok[2].end()
     gp.put(0, GM3)
     gm.put(0, GM1)
+    lay_down()
     gm.put(0, FP1)
+    gm.put(1, FM0)
+    tok[1].on_cp()
+    gm.put(1, FP1)
+    gm.put(1, GM1)
+    gm.put(0, GP0)
+    gm.put(1, FP3)
     gm.put(1, GM3)
-    gm.put(0, FP3)
-    tok[2].far_c()
-    gm.put(1, GM1)
+    tok[1].far_c()
+    gv.put(1, NP)
     gm.put(1, GP0)
     gv.put(0, NM)
+    tok[3].on_cm()
+    tok[0].on_cp()
+    gm.put(0, FM2)
+    norm(2)
+    tok[3].on_m()
+    gu.put(1, NP)
+    tok[0].far_c()
+    tok[1].end()
+    gm.put(0, GM3)
+    tok[3].on_p()
+    gu.put(0, NP)
+    norm(1)
+    gv.put(0, NP)
+    gu.put(1, NM)
+    tok[0].end()
+    gu.put(0, NM)
+    gv.put(1, NM)
+    gu.put(1, FM0)
+    norm(0)
+    gd.put(0, NP)
+    gd.put(1, NP)
+    gv.put(1, FP0)
+    gp.end()
+    gu.put(1, FP0)
+    gv.put(1, FM0)
+    gd.put(1, NM)
+    project(0)
+    gu.put(0, FP0)
+    gv.put(0, FP0)
+    project(1)
+    gm.end()
     tok[3].far_c()
-    gm.put(0, GM3)
-    gv.put(1, NP)
-    tok[1].far_c()
-    gu.put(1, NP)
-    gv.put(0, NP)
-    gv.put(0, FP0)
-    gv.put(1, NM)
-    tok[2].end()
-    gd.put(1, NM)
-    gu.put(0, NM)
-    gu.put(1, NM)
-    gu.put(0, NP)
-    tok[1].end()
+    mix_terms(0)
+    mix_terms(1)
+    gv.put(0, FM0)
+    tok[3].on_cp()
+    project(2)
+    pairs(0)
+    one[0].dp()
+    gu.put(1, QP)
+    one[0].ep()
+    gv.put(0, FM2)
+    gv.put(1, FM1)
+    one[0].dm()
+    gv.put(1, FP1)
+    mix_terms(2)
+    pairs(1)
+    gu.put(0, QP)
+    gv.put(0, FM1)
+    gv.put(1, QP)
+    gu.put(0, QM)
+    one[1].ep()
+    tok[3].end()
+    one[1].dm()
+    gv.put(0, QM)
+    gv.put(0, FP2)
+    norm(3)
+    one[0].em()
+    gv.put(0, QP)
+    gv.put(1, FP2)
+    gu.put(1, FM2)
+    gv.put(1, QM)
+    one[1].dp()
+    one[1].em()
+    gu.put(0, FP1)
+    project(3)
+    pairs(2)
+    gu.put(1, QM)
+    one[0].pass_on()
+    gu.put(0, FP2)
+    one[2].em()
+    one[2].dp()
+    one[2].dm()
+    mix_terms(3)
+    gv.put(0, GP0)
+    gu.put(0, GP0)
+    gu.put(1, GP0)
+    gv.put(1, FM2)
+    one[2].ep()
+    gd.put(0, NM)
+    one[1].pass_on()
+    gu.put(0, FM1)
+    pairs(3)
+    gu.put(1, FP2)
     gu.put(0, FM0)
-    gu.put(1, FP0)
-    norm(2)
-    gd.put(0, NM)
-    gv.put(1, FP0)
-    norm(1)
-    gp.end()
-    project(0)
-    gm.end()
-    mix_terms(0)
-    tok[3].end()
-    project(1)
-    gv.put(1, QM)
-    gv.put(0, QM)
-    gu.put(0, FP0)
-    gv.put(1, QP)
-    gd.put(1, NP)
-    gv.put(1, FM2)
-    mix_terms(1)
-    gv.put(1, FM1)
-    gv.put(0, FM0)
-    pairs(0)
-    gu.put(1, QP)
-    gu.put(1, FM0)
-    one[0].dm()
-    one[0].em()
-    one[0].dp()
-    gv.put(0, QP)
-    gu.put(0, QP)
-    project(2)
-    one[0].ep()
-    gv.put(0, FP2)
-    mix_terms(2)
+    one[3].ep()
+    one[3].dp()
     gu.put(0, FM2)
-    pairs(1)
-    one[1].dm()
-    gu.put(1, FP2)
-    gu.put(1, FM2)
-    one[1].ep()
-    one[1].em()
-    gu.put(0, QM)
-    gu.put(0, FP2)
-    one[1].dp()
-    norm(3)
-    one[0].pass_on()
-    gv.put(1, FP3)
-    gu.put(1, GP0)
-    gu.put(1, QM)
+    one[3].dm()
     gu.put(1, FM1)
-    gv.put(1, FP2)
-    pairs(2)
-    gv.put(0, FP3)
-    gu.put(0, FP1)
+    hidden(0)
+    hid[0].own_p()
     gv.put(0, FM3)
-    gv.put(0, FM1)
-    gv.put(1, FM3)
-    one[2].em()
-    gu.put(0, FM1)
-    one[2].ep()
-    one[2].dm()
-    project(3)
-    one[2].dp()
-    mix_terms(3)
-    one[1].pass_on()
-    hidden(0)
-    gv.put(0, FP1)
-    hid[0].own_m()
-    gv.put(1, FM0)
-    hid[0].own_p()
-    pairs(3)
-    gv.put(0, GP0)
-    gv.put(0, FM2)
-    gu.put(0, GP2)
-    gv.put(1, GP0)
-    one[3].dp()
     hid[0].own_c()
     gu.put(0, FM3)
-    gu.put(0, FP3)
-    one[3].dm()
+    gv.put(1, FM3)
+    gu.put(1, FM3)
+    hid[0].own_m()
+    gv.put(0, FP1)
+    gv.put(1, GP0)
     hidden(1)
-    gd.put(0, NP)
-    gu.put(1, FM3)
-    gu.put(1, FP1)
+    gv.put(1, GP2)
+    gu.put(1, FP3)
+    hid[1].own_m()
+    hid[1].own_p()
     one[2].pass_on()
-    hid[1].own_p()
-    gv.put(1, GM1)
-    hid[1].own_m()
-    gv.put(1, GP2)
-    one[3].em()
-    gu.put(1, FP3)
-    hid[0].on_m()
     one[3].pass_on()
     hid[1].own_c()
-    gv.put(1, FP1)
+    gu.put(1, FP1)
     hid[0].on_p()
-    hid[0].on_cp()
+    gv.put(1, FP3)
+    gu.put(1, GM1)
     gv.put(0, GP2)
     gu.put(1, GP2)
-    gv.put(0, GM1)
-    one[3].ep()
-    gu.put(1, GM1)
+    gd.put(0, QP)
+    gu.put(0, GM1)
+    ge.put(0, NP)
+    one[3].em()
+    gv.put(1, GM3)
+    gu.put(0, FP3)
+    gv.put(0, FP3)
+    gv.put(0, GM3)
+    hid[1].on_p()
+    hid[1].on_cm()
+    hid[0].on_m()
+    gv.put(1, GM1)
+    hid[1].on_m()
     hidden(2)
     hid[2].own_p()
-    gv.put(1, GM3)
+    gv.put(0, GM1)
+    hid[0].on_cm()
     hid[2].own_m()
-    gd.put(0, QP)
-    gu.put(0, GM1)
-    hid[1].on_p()
-    hid[1].on_m()
-    gv.put(0, GM3)
-    hid[1].on_cm()
+    hidden(3)
+    gd.put(1, FP1)
+    hid[3].own_p()
+    hid[0].on_cp()
+    gd.put(1, FP0)
+    hid[0].far_c()
+    hid[3].own_m()
+    gu.put(1, GM3)
     gu.put(0, GM3)
-    hid[0].on_cm()
-    hid[0].far_c()
     ge.put(1, NM)
-    gu.put(1, GM3)
-    gu.put(0, GP0)
-    gd.put(1, QP)
-    hidden(3)
     hid[1].on_cp()
-    hid[3].own_m()
-    hid[3].own_c()
+    hid[2].own_c()
     gd.put(1, QM)
-    hid[3].own_p()
-    hid[2].own_c()
+    gu.put(0, GP2)
+    gd.put(1, FP2)
+    hid[1].far_c()
     ge.put(1, NP)
     gd.put(0, QM)
+    ge.put(0, NM)
+    hid[0].end()
     gd.put(0, FM1)
-    ge.put(0, NM)
+    gd.put(1, QP)
+    gd.put(1, FM1)
+    hid[2].on_p()
+    gd.put(0, FM2)
+    gd.put(1, FM0)
+    hid[2].on_cp()
+    hid[3].own_c()
+    gd.put(0, FP2)
+    hid[2].on_m()
     gd.put(0, FP0)
-    gd.put(1, FM1)
-    gd.put(1, FP0)
-    hid[0].end()
-    gd.put(0, FP2)
-    gd.put(1, FP2)
-    gd.put(0, FM2)
-    ge.put(0, NP)
-    hid[2].on_cp()
     scale(0)
-    hid[1].far_c()
-    hid[2].on_p()
-    hid[2].on_m()
-    gd.put(0, FP1)
+    hid[2].on_cm()
+    gv.end()
+    hid[3].on_p()
     hid[1].end()
     scale(1)
+    gd.put(0, FP1)
+    hid[3].on_cm()
     hid[3].on_m()
-    gd.put(1, FM2)
-    hid[2].on_cm()
-    hid[3].on_p()
     hid[3].on_cp()
-    hid[3].on_cm()
-    gd.put(1, FP1)
-    gv.end()
     gu.end()
     expand(0)
+    hid[2].far_c()
+    gd.put(1, FM3)
+    ge.put(0, QM)
+    ge.put(1, QP)
+    gd.put(0, FM3)
+    ge.put(1, QM)
+    gd.put(1, FM2)
+    gd.put(0, FM0)
     gd.put(0, FP3)
-    gd.put(1, FM3)
-    gd.put(0, FM3)
-    hid[2].far_c()
-    gd.put(1, FM0)
-    ge.put(0, QM)
+    ge.put(0, QP)
+    activate(0)
     gd.put(1, FP3)
-    ge.put(1, QM)
-    gd.put(0, FM0)
     expand(1)
+    hid[2].end()
+    gd.put(1, GM1)
+    gd.put(0, GM1)
+    scale(2)
     gd.put(1, GP0)
-    activate(0)
-    hid[2].end()
-    gd.put(0, GM1)
-    gd.put(1, GM1)
+    hid[3].far_c()
     gd.put(0, GP0)
-    ge.put(1, QP)
-    scale(2)
-    gd.put(1, GP2)
-    hid[3].far_c()
     expand(2)
     gd.put(0, GP2)
+    gd.put(1, GP2)
+    gd.put(0, GM3)
     gd.put(1, GM3)
-    gd.put(0, GM3)
-    ge.put(0, QP)
-    ge.put(1, FM0)
+    activate(1)
+    ge.put(0, FM3)
+    ge.put(0, FM1)
     ge.put(0, FM0)
     ge.put(1, FP2)
-    activate(1)
+    ge.put(0, FP2)
+    ge.put(0, FP3)
+    ge.put(1, FM3)
+    ge.put(1, FP1)
     hid[3].end()
+    ge.put(1, FM1)
     scale(3)
-    ge.put(1, FM1)
-    ge.put(0, FM1)
     ge.put(1, FP0)
-    ge.put(0, FP2)
     activate(2)
     ge.put(0, FP0)
+    ge.put(1, FP3)
     expand(3)
-    ge.put(1, FM3)
-    ge.put(0, FM3)
+    ge.put(1, FM2)
     activate(3)
-    ge.put(0, FP1)
-    ge.put(1, FP1)
+    ge.put(1, FM0)
     gd.end()
     down_terms(0, 0)
-    ge.put(1, FP3)
+    ge.put(0, FM2)
     ge.put(0, GP2)
-    ge.put(0, FM2)
-    ge.put(1, FM2)
     down_terms(0, 1)
-    ge.put(1, GP2)
-    ge.put(1, GM1)
-    ge.put(0, GP0)
-    ge.put(0, FP3)
-    ge.put(1, GP0)
-    ge.put(0, GM1)
-    down_terms(0, 2)
     ge.put(0, GM3)
     ge.put(1, GM3)
-    pair_all(0, 0)
+    ge.put(0, FP1)
+    ge.put(1, GP2)
+    down_terms(0, 2)
+    pair_first(0, 0)
     two[0].dm()
     two[0].dp()
+    ge.put(1, GM1)
+    ge.put(0, GM1)
+    ge.put(1, GP0)
+    ge.put(0, GP0)
+    pair_first(0, 1)
     two[1].dp()
     two[1].dm()
+    pair_first(0, 2)
+    down_terms(0, 3)
+    two[2].dm()
     two[2].dp()
-    two[2].dm()
     pair_all(0, 1)
+    pair_all(0, 2)
+    two[1].em()
+    two[2].em()
     two[2].ep()
-    pair_all(0, 2)
+    two[1].ep()
     two[0].em()
-    two[1].ep()
-    two[2].em()
-    two[1].em()
-    down_terms(0, 3)
+    two[0].pass_on()
+    two[0].ep()
     ge.end()
-    two[0].ep()
     down_terms(1, 0)
     two[1].pass_on()
-    two[0].pass_on()
     down_terms(1, 1)
     two[2].pass_on()
     down_terms(1, 2)
-    pair_all(1, 0)
+    pair_first(1, 0)
+    tri[0].dm()
     tri[0].dp()
-    tri[0].dm()
+    pair_first(1, 2)
+    pair_first(1, 1)
+    tri[1].dp()
+    tri[2].dp()
+    tri[2].dm()
+    down_terms(1, 3)
+    pair_all(1, 1)
+    tri[1].ep()
+    tri[0].ep()
+    tri[1].dm()
     pair_all(0, 3)
-    tri[2].dm()
-    tri[2].dp()
-    down_terms(1, 3)
-    tri[1].dm()
-    tri[1].dp()
-    pair_all(1, 1)
-    tri[0].ep()
     pair_all(1, 2)
+    tri[2].em()
+    tri[0].em()
+    early(0)
+    tri[1].em()
     tri[2].ep()
-    tri[0].em()
-    tri[2].em()
-    tri[1].ep()
+    tri[0].pass_on()
+    tri[1].pass_on()
     early(2)
+    tri[2].pass_on()
     pair_all(1, 3)
-    tri[1].em()
-    tri[0].pass_on()
+    finish(0)
     early(1)
-    tri[1].pass_on()
-    early(0)
-    tri[2].pass_on()
-    finish(0)
     finish(1)
     finish(2)
     for gather in (gp, gm, gu, gv, gd, ge):

time: 90.8 us -> 90.8 us (level)
  no operation moved by 1% of the time
where the time goes in v7:
time: 90.8 us; the launch traced here: 90.4 us
  Pallas kernels  89.7 us (99%)
    pallas_call x1, Pallas kernels, on_device(): pl.pallas_call(kernel, out_shape=pltpu.VMEM((SEQ, 256), BF16), in_specs=[...  89.7 us

profile of v7, /device:TPU:1, one launch (start us, length us, event | category | flops | bytes accessed | tf_op | source)
XLA Modules:
  0.0 90.4 jit_solution(13486977911870607026)
XLA Ops:
  0.0 89.7 %shard_map.136 = bf16[768,256]{1,0:T(8,128)(2,1)S(1)} custom-call(bf16[768,256]{1,0:T(8,128)(2,1)} %tokens.1, f32[1,2048]{1,0:T(1,128)} %bitcast.9, bf16[128,256]{1,0:T(8,128)(2,1)} %outer_gate.1, bf16[128,256]{1,0:T(8,128)(2,1)} %inner_gate.1, bf16[128,256]{1,0:T(8,128)(2,1)} %signal_in.1, f32[3,256]{1,0:T(4,128)} %mix_taps.1, f32[1,256]{1,0:T(1,128)} %bitcast.11, ...), custom_call_target="tpu_custom_call" | custom-call | tf_op jit(solution)/shard_map/pallas_call | solution.py:923
  89.7 0.7 copy.16
